TPU v7x, 256 devices: a 4x2x16 block of a 4x16x16 slice. The times are simulated.
256 devices in a mesh: grp: 2 (over y), sp: 32 (over z, core), tp: 4 (over x).
Axes of the slice: x: 4, y: 2, z: 16, core: 2. Of those that a mesh axis runs over, the one named last changes fastest.
The devices are a block of a 4x16x16 slice.
Arguments:
- resid_in: bfloat16 [16384, 2048], P(('grp', 'sp', 'tp')), parts along dimension 0, may hold values from -6 to 6
- query_narrow: bfloat16 [16384, 8, 128], P(('grp', 'sp'), 'tp'), parts along dimension 0, may hold values from -512 to 512
- key_narrow: bfloat16 [16384, 4, 128], P(('grp', 'sp'), 'tp'), parts along dimension 0, may hold values from -512 to 512
- value_narrow: bfloat16 [16384, 4, 128], P(('grp', 'sp'), 'tp'), parts along dimension 0, may hold values from -6 to 6
- query_wide: bfloat16 [16384, 8, 256], P(('grp', 'sp'), 'tp'), parts along dimension 0, may hold values from -512 to 512
- key_wide: bfloat16 [16384, 4, 256], P(('grp', 'sp'), 'tp'), parts along dimension 0, may hold values from -512 to 512
- value_wide: bfloat16 [16384, 4, 128], P(('grp', 'sp'), 'tp'), parts along dimension 0, may hold values from -6 to 6
- lambda_narrow: float32 [8], P('tp'), may hold values from 0.3 to 0.8
- lambda_wide: float32 [8], P('tp'), may hold values from 0.3 to 0.8
- head_gain: float32 [128], replicated, may hold values from 0.1 to 1.9
- out_narrow: bfloat16 [1024, 2048], P('tp'), may hold values from -0.125 to 0.125
- out_wide: bfloat16 [1024, 2048], P('tp'), may hold values from -0.125 to 0.125
- norm_gain: bfloat16 [2048], replicated, may hold values from 0.099609375 to 1.8984375
- up_weight: bfloat16 [2048, 8192], P('sp', 'tp'), may hold values from -0.125 to 0.125
- down_weight: bfloat16 [8192, 2048], P('tp', 'sp'), may hold values from -0.0625 to 0.0625
Outputs:
- mixed_out: bfloat16 [16384, 2048], P(('grp', 'sp', 'tp')), parts along dimension 0
There are 2 independent parts, one for each index of `grp`. A program takes and returns all parts, laid end to end along the dimension named above; an argument that names none is the same for every part. Nothing has to cross between parts.
All inputs are finite; a program needn't handle non-finite values.
Results may differ from a plain program's by a relative error of at most 0.018.
Values may be sent and summed in bfloat16 or wider, within the bound.
No kernel may reach another device: no remote copies, remote signals or barrier semaphores. Data moves between devices by JAX's collectives and lax.ppermute only.
A program may use at most 128 MiB of HBM per device.

v0:
```python
import math

import jax
import jax.numpy as jnp
from jax import lax
from jax.sharding import PartitionSpec as P

NORM_EPS = 1e-06
OUT_SCALE = 0.8


def sent_together(arrays, axis, dim, along):
    ends, at = ([], 0)
    for a in arrays[:-1]:
        at += a.shape[along]
        ends.append(at)
    both = jnp.concatenate(arrays, axis=along)
    return tuple(jnp.split(lax.all_gather(both, axis, axis=dim, tiled=True), ends, axis=along))


def split_up(array, dim, peers):
    before, after = (array.shape[:dim], array.shape[dim + 1 :])
    return jnp.moveaxis(array.reshape(*before, peers, -1, *after), dim, 0)


def sent_and_summed(array, axis, dim):
    peers = lax.axis_size(axis)
    parts = lax.all_to_all(split_up(array, dim, peers), axis, 0, 0, tiled=True)
    return jnp.sum(parts.astype(jnp.float32), axis=0)


def laid_out(parts, dim):
    parts = jnp.moveaxis(parts, 0, dim)
    lengths = parts.shape
    return parts.reshape(*lengths[:dim], lengths[dim] * lengths[dim + 1], *lengths[dim + 2 :])


def copy_for_each(array, axis):
    copies = jnp.broadcast_to(array, (lax.axis_size(axis), *array.shape))
    return lax.all_to_all(copies, axis, split_axis=0, concat_axis=0, tiled=True)


def collect(array, axis, dim):
    return laid_out(copy_for_each(array, axis), dim)


def empty_state(query, key_head_stack, value_width):
    row_count, head_count = (query.shape[0], query.shape[1])
    group_size = head_count // key_head_stack
    row_top = jnp.full((key_head_stack, group_size, 2, row_count), -jnp.inf, jnp.float32)
    row_total = jnp.zeros((key_head_stack, group_size, 2, row_count), jnp.float32)
    weighted_values = jnp.zeros(
        (key_head_stack, group_size, 2, row_count, value_width), jnp.float32
    )
    return (row_top, row_total, weighted_values)


def absorb(states, query, key_rows, values):
    row_count, head_count = (query.shape[0], query.shape[1])
    key_head_stack = key_rows.shape[1]
    half_width = key_rows.shape[2] // 2
    group_size = head_count // key_head_stack
    value_width = values.shape[2]
    amount = key_rows.shape[0]
    block_rows = math.gcd(amount, 512)
    rotation_count = amount // block_rows
    grouped = query.reshape(row_count, key_head_stack, group_size, 2, half_width)
    key_block_list = key_rows.reshape(rotation_count, block_rows, key_head_stack, 2, half_width)
    value_blocks = values.reshape(rotation_count, block_rows, key_head_stack, value_width)

    def visit(running, kv_pair):
        row_top, row_total, weighted_values = running
        key_blk, value_blk = kv_pair
        scores = jnp.einsum(
            "tkgcd,skcd->kgcts", grouped, key_blk, preferred_element_type=jnp.float32
        ) * half_width ** (-0.5)
        new_top = jnp.maximum(row_top, jnp.max(scores, axis=-1))
        rescale = jnp.exp(row_top - new_top)
        powers = jnp.exp(scores - new_top[..., None])
        row_total = row_total * rescale + jnp.sum(powers, axis=-1)
        weighted_values = weighted_values * rescale[..., None] + jnp.einsum(
            "iodph,hie->iodpe",
            powers.astype(jnp.bfloat16),
            value_blk,
            preferred_element_type=jnp.float32,
        )
        return ((new_top, row_total, weighted_values), None)

    outcome, _ = lax.scan(visit, states, (key_block_list, value_blocks))
    return outcome


def finish(states, lambdas, gain_vec):
    row_top, row_total, weighted_values = states
    key_head_stack, group_size, row_count = (row_top.shape[0], row_top.shape[1], row_top.shape[3])
    value_width = weighted_values.shape[4]
    first_map = weighted_values[:, :, 0] / row_total[:, :, 0, :, None]
    second_map = weighted_values[:, :, 1] / row_total[:, :, 1, :, None]
    mixed = first_map - lambdas.reshape(key_head_stack, group_size)[:, :, None, None] * second_map
    normed = (
        mixed
        * lax.rsqrt(jnp.mean(mixed * mixed, axis=-1, keepdims=True) + NORM_EPS)
        * gain_vec
        * OUT_SCALE
    )
    normed = normed.astype(jnp.bfloat16).transpose(2, 0, 1, 3)
    return normed.reshape(row_count, key_head_stack * group_size * value_width)


def attend(
    query_narrow,
    key_narrow,
    value_narrow,
    query_wide,
    key_wide,
    value_wide,
    lambda_narrow,
    lambda_wide,
    head_gain,
):
    initial = (
        empty_state(query_narrow, key_narrow.shape[1], value_narrow.shape[2]),
        empty_state(query_wide, key_wide.shape[1], value_wide.shape[2]),
    )
    narrow_keys, narrow_values, wide_keys, wide_values = sent_together(
        (key_narrow, value_narrow, key_wide, value_wide), "sp", 0, 2
    )
    narrow_state = absorb(initial[0], query_narrow, narrow_keys, narrow_values)
    wide_state = absorb(initial[1], query_wide, wide_keys, wide_values)
    return (
        finish(narrow_state, lambda_narrow, head_gain),
        finish(wide_state, lambda_wide, head_gain),
    )


def shards(
    resid_in,
    query_narrow,
    key_narrow,
    value_narrow,
    query_wide,
    key_wide,
    value_wide,
    lambda_narrow,
    lambda_wide,
    head_gain,
    out_narrow,
    out_wide,
    norm_gain,
    up_weight,
    down_weight,
):
    att_narrow, att_wide = attend(
        query_narrow,
        key_narrow,
        value_narrow,
        query_wide,
        key_wide,
        value_wide,
        lambda_narrow,
        lambda_wide,
        head_gain,
    )
    projected = sent_and_summed(
        (
            jnp.dot(att_narrow, out_narrow, preferred_element_type=jnp.float32)
            + jnp.dot(att_wide, out_wide, preferred_element_type=jnp.float32)
        ).astype(jnp.bfloat16),
        "tp",
        0,
    )
    middle = (resid_in.astype(jnp.float32) + projected).astype(jnp.bfloat16)
    middle_f32 = middle.astype(jnp.float32)
    normed = middle_f32 * lax.rsqrt(
        jnp.mean(middle_f32 * middle_f32, axis=-1, keepdims=True) + NORM_EPS
    )
    normed = (normed * norm_gain.astype(jnp.float32)).astype(jnp.bfloat16)
    whole_rows = collect(normed, "tp", 0)
    up_collected = lax.all_gather(up_weight, "sp", axis=0, tiled=True)
    lifted = jnp.dot(whole_rows, up_collected, preferred_element_type=jnp.float32)
    activated = jnp.square(jax.nn.relu(lifted)).astype(jnp.bfloat16)
    partials = jnp.dot(
        activated,
        lax.all_gather(down_weight, "sp", axis=1, tiled=True),
        preferred_element_type=jnp.float32,
    )
    mixer_out = sent_and_summed(partials.astype(jnp.bfloat16), "tp", 0)
    return (middle_f32 + mixer_out).astype(jnp.bfloat16)


def solution(mesh):
    placed = (
        P(("grp", "sp", "tp"), None),
        P(("grp", "sp"), "tp", None),
        P(("grp", "sp"), "tp", None),
        P(("grp", "sp"), "tp", None),
        P(("grp", "sp"), "tp", None),
        P(("grp", "sp"), "tp", None),
        P(("grp", "sp"), "tp", None),
        P("tp"),
        P("tp"),
        P(),
        P("tp", None),
        P("tp", None),
        P(),
        P("sp", "tp"),
        P("tp", "sp"),
    )
    return jax.shard_map(
        shards, mesh=mesh, in_specs=placed, out_specs=P(("grp", "sp", "tp"), None), check_vma=False
    )
```

profile of v0, /device:TPU:40, one launch (start us, length us, event | category | flops | bytes accessed | tf_op | source)
XLA Modules:
  0.0 384.9 jit_solution(5291192769765145764)
XLA Ops:
  6.6 1.8 pad_maximum_fusion
  11.5 90.5 %all-gather.4.cloned.1.call-done = bf16[8192,1,640]{2,0,1:T(8,128)(2,1)} async-done(((bf16[256,1,640]{2,0,1:T(8,128)(2,1)}), bf16[8192,1,640]{2,0,1:T(8,128)(2,1)}) %all-gather.4.cloned.1.call-update) | async-done | bytes 10485776 | tf_op jit(solution)/shard_map/all_gather | solution.py:18
  102.0 5.2 %fusion.45 = (bf16[8192,1,128]{2,0,1:T(8,128)(2,1)}, bf16[8192,1,128]{2,0,1:T(8,128)(2,1)}, bf16[8192,1,128]{2,0,1:T(8,128)(2,1)S(1)}) fusion(bf16[8192,1,640]{2,0,1:T(8,128)(2,1)} %all-gather.4.cloned.1.call-done), kind=kLoop, calls=%fused_computation.88 | loop fusion | bytes 12582912 | tf_op jit(solution)/shard_map/split | solution.py:18
  107.3 3.2 reshape.284
  110.5 10.6 %copy.29 = bf16[16,512,1,2,64]{1,4,3,2,0:T(8,128)(2,1)} copy(bf16[16,512,1,2,64]{4,3,1,0,2:T(2,128)(2,1)} %reshape.284) | data formatting | bytes 4194304
  121.1 89.1 %while.30 = (s32[]{:T(128)}, f32[1,2,2,256]{3,1,2,0:T(2,128)S(1)}, f32[1,2,2,256]{3,1,2,0:T(2,128)}, f32[1,2,2,256,128]{4,3,2,1,0:T(8,128)}, bf16[16,512,1,2,64]...) while((s32[]{:T(128)}, f32[1,2,2,256]{3,1,2,0:T(2,128)S(1)}, ...), condition=%wide.region_3.4_spmd.clone, body=%wide.region_0.3_spmd.clone.sunk | while | flops 204871680 | bytes 12031193 | solution.py:89
  121.1 1.4 bitcast_reduce_fusion.4
  123.5 1.6 fusion.68
  126.6 1.4 bitcast_reduce_fusion.4
  129.1 1.6 fusion.68
  132.2 1.4 bitcast_reduce_fusion.4
  134.7 1.6 fusion.68
  140.3 1.6 fusion.68
  143.4 1.4 bitcast_reduce_fusion.4
  145.8 1.6 fusion.68
  148.9 1.4 bitcast_reduce_fusion.4
  151.4 1.6 fusion.68
  154.5 1.4 bitcast_reduce_fusion.4
  157.0 1.6 fusion.68
  160.1 1.4 bitcast_reduce_fusion.4
  162.5 1.6 fusion.68
  165.6 1.4 bitcast_reduce_fusion.4
  168.1 1.6 fusion.68
  171.2 1.4 bitcast_reduce_fusion.4
  173.7 1.6 fusion.68
  176.8 1.4 bitcast_reduce_fusion.4
  179.2 1.6 fusion.68
  182.3 1.4 bitcast_reduce_fusion.4
  184.8 1.6 fusion.68
  187.9 1.4 bitcast_reduce_fusion.4
  190.3 1.6 fusion.68
  193.4 1.4 bitcast_reduce_fusion.4
  195.9 1.6 fusion.68
  199.0 1.4 bitcast_reduce_fusion.4
  201.4 1.7 fusion.68
  204.6 1.4 bitcast_reduce_fusion.4
  207.1 1.6 fusion.68
  210.2 2.0 copy.31
  212.2 4.6 %split.18 = bf16[8192,1,256]{2,0,1:T(8,128)(2,1)} slice(bf16[8192,1,640]{2,0,1:T(8,128)(2,1)} %all-gather.4.cloned.1.call-done), slice={[0:8192], [0:1], [256:512]} | slice | bytes 8388608 | tf_op jit(solution)/shard_map/split | solution.py:18
  216.8 7.0 %reshape.285 = bf16[16,512,1,2,128]{4,3,1,0,2:T(2,128)(2,1)} reshape(bf16[8192,1,256]{2,0,1:T(8,128)(2,1)} %split.18) | data formatting | bytes 8388608 | tf_op jit(solution)/shard_map/reshape | solution.py:68
  223.8 82.0 %while.31 = (s32[]{:T(128)}, f32[1,2,2,256]{3,1,2,0:T(2,128)S(1)}, f32[1,2,2,256]{3,1,2,0:T(2,128)S(1)}, f32[1,2,2,256,128]{4,3,2,1,0:T(8,128)}, bf16[16,512,1,2...) while((s32[]{:T(128)}, f32[1,2,2,256]{3,1,2,0:T(2,128)S(1)}, ...), condition=%wide.region_8.9_spmd.clone, body=%wide.region_5.0_spmd.clone.sunk | while | flops 271980544 | bytes 12784293 | solution.py:89
  226.4 1.6 fusion.73
  231.6 1.6 fusion.73
  236.7 1.6 fusion.73
  241.9 1.6 fusion.73
  247.0 1.6 fusion.73
  252.1 1.6 fusion.73
  257.2 1.6 fusion.73
  262.4 1.6 fusion.73
  267.5 1.6 fusion.73
  272.6 1.6 fusion.73
  277.7 1.6 fusion.73
  282.8 1.6 fusion.73
  288.0 1.6 fusion.73
  293.1 1.6 fusion.73
  298.2 1.6 fusion.73
  303.3 1.6 fusion.73
  309.5 1.4 fusion.29
  311.0 4.5 %all-to-all-start = ((bf16[4,64,2048]{2,1,0:T(8,128)(2,1)}), bf16[4,64,2048]{2,1,0:T(8,128)(2,1)S(1)}, u32[]{:S(2)}, u32[]{:S(2)}) async-start(bf16[4,64,2048]{2,1,0:T(8,128)(2,1)} %bitcast.16), calls=%async_computation | async-start | bytes 2097152 | tf_op jit(solution)/shard_map/all_to_all | solution.py:28
  315.4 15.6 %all-to-all-done = bf16[4,64,2048]{2,1,0:T(8,128)(2,1)S(1)} async-done(((bf16[4,64,2048]{2,1,0:T(8,128)(2,1)}), bf16[4,64,2048]{2,1,0:T(8,128)(2,1)S(1)}, u32[]{:S(2)}, u32[]{:S(2)}) %all-to-all-start) | async-done | bytes 1048608 | tf_op jit(solution)/shard_map/all_to_all | solution.py:28
  332.6 3.8 all-to-all-start.1
  336.5 14.4 %all-to-all-done.1 = bf16[4,64,2048]{2,1,0:T(8,128)(2,1)S(1)} async-done(((bf16[4,64,2048]{2,1,0:T(8,128)(2,1)}), bf16[4,64,2048]{2,1,0:T(8,128)(2,1)S(1)}, u32[]{:S(2)}, u32[]{:S(2)}) %all-to-all-start.1) | async-done | bytes 1048608 | tf_op jit(solution)/shard_map/all_to_all | solution.py:40
  350.9 10.3 %convolution_convert_fusion = bf16[256,2048]{1,0:T(8,128)(2,1)S(1)} fusion(bf16[2048,2048]{0,1:T(8,128)(2,1)} %all-gather.8.cloned.1.call-done, bf16[256,2048]{1,0:T(8,128)(2,1)S(1)} %bitcast.204, bf16[2048,2048]{1,0:T(8,128)(2,1)} %all-gather.6.cloned.1.call-done), kind=kOutput, calls=%fused_computation.52 | convolution fusion | flops 4297064448 | bytes 18874368 | tf_op jit(solution)/shard_map/dot_general | solution.py:182
  361.2 16.3 %all_to_all.15 = bf16[4,64,2048]{2,1,0:T(8,128)(2,1)S(1)} all-to-all(bf16[4,64,2048]{2,1,0:T(8,128)(2,1)S(1)} %bitcast.205), channel_id=1, replica_groups=mesh['grp'=2,'sp'=32,'tp'=4] {'tp'}, dimensions={0} | all-to-all | bytes 2097152 | tf_op jit(solution)/shard_map/all_to_all | solution.py:28
  (437 shorter events, 104.3 us)
Async XLA Ops:
  6.5 301.9 %copy-start = (bf16[256,2048]{1,0:T(8,128)(2,1)S(1)}, bf16[256,2048]{1,0:T(8,128)(2,1)}, u32[]{:S(2)}) copy-start(bf16[256,2048]{1,0:T(8,128)(2,1)} %param.29) | copy-start | bytes 3145732
  6.6 4.6 %copy-start.6 = (bf16[256,2,256]{2,1,0:T(2,128)(2,1)S(1)}, bf16[256,2,256]{2,1,0:T(2,128)(2,1)}, u32[]{:S(2)}) copy-start(bf16[256,2,256]{2,1,0:T(2,128)(2,1)} %param.23) | copy-start | bytes 786436
  6.6 95.5 %all-gather.4.cloned.1.call-start = ((), (), s32[]{:S(2)}) async-start(), calls=%async_computation.3 | async-start | bytes 10813440 | tf_op jit(solution)/shard_map/all_gather | solution.py:18
  8.5 328.0 %all-gather.6.cloned.1.call-start = ((), (), s32[]{:S(2)}) async-start(), calls=%async_computation.4 | async-start | bytes 8650752 | tf_op jit(solution)/shard_map/all_gather | solution.py:179
  9.3 327.2 %all-gather.8.cloned.1.call-start = ((), (), s32[]{:S(2)}) async-start(), calls=%async_computation.5 | async-start | bytes 8650752 | tf_op jit(solution)/shard_map/all_gather | solution.py:184
  122.5 1.1 copy-start.4
  122.5 3.5 copy-start.8
  128.1 1.0 copy-start.4
  128.1 3.5 copy-start.8
  130.8 0.8 copy-start.5
  133.6 1.0 copy-start.4
  133.7 3.5 copy-start.8
  136.3 0.8 copy-start.5
  139.2 1.1 copy-start.4
  139.2 3.5 copy-start.8
  144.8 1.0 copy-start.4
  144.8 3.5 copy-start.8
  150.3 1.1 copy-start.4
  150.4 3.5 copy-start.8
  155.9 1.0 copy-start.4
  155.9 3.5 copy-start.8
  161.5 1.0 copy-start.4
  161.5 3.5 copy-start.8
  167.0 1.1 copy-start.4
  167.1 3.5 copy-start.8
  172.6 1.0 copy-start.4
  172.6 3.5 copy-start.8
  178.2 1.0 copy-start.4
  178.2 3.5 copy-start.8
  183.7 1.0 copy-start.4
  183.8 3.5 copy-start.8
  189.3 1.0 copy-start.4
  189.3 3.5 copy-start.8
  194.8 1.0 copy-start.4
  194.9 3.5 copy-start.8
  200.4 1.0 copy-start.4
  200.4 3.5 copy-start.8
  206.0 1.1 copy-start.4
  206.0 3.5 copy-start.8
  223.8 83.3 %copy-start.10 = (f32[1,2,2,256]{3,1,2,0:T(2,128)S(1)}, f32[1,2,2,256]{3,1,2,0:T(2,128)}, u32[]{:S(2)}) copy-start(f32[1,2,2,256]{3,1,2,0:T(2,128)} %get-tuple-element.82) | copy-start | bytes 12292
  223.8 83.3 %copy-start.12 = (f32[2]{0:T(128)S(1)}, f32[2]{0:T(128)}, u32[]{:S(2)}) copy-start(f32[2]{0:T(128)} %param.27) | copy-start | bytes 28
  223.8 83.3 %copy-start.13 = (f32[2]{0:T(128)S(1)}, f32[2]{0:T(128)}, u32[]{:S(2)}) copy-start(f32[2]{0:T(128)} %param.26) | copy-start | bytes 28
  225.4 1.0 copy-start.2
  230.5 1.1 copy-start.2
  235.7 1.0 copy-start.2
  240.8 1.1 copy-start.2
  246.0 1.0 copy-start.2
  251.1 1.0 copy-start.2
  256.2 1.0 copy-start.2
  261.3 1.0 copy-start.2
  266.4 1.0 copy-start.2
  271.6 1.0 copy-start.2
  276.7 1.0 copy-start.2
  281.8 1.0 copy-start.2
  286.9 1.0 copy-start.2
  292.0 1.0 copy-start.2
  297.2 1.0 copy-start.2
  302.3 1.0 copy-start.2
  305.8 2.6 copy-start.14
  308.3 1.2 copy-start.1
  311.0 4.5 %copy-start.11 = (bf16[2048]{0:T(1024)(128)(2,1)S(1)}, bf16[2048]{0:T(1024)(128)(2,1)}, u32[]{:S(2)}) copy-start(bf16[2048]{0:T(1024)(128)(2,1)} %param.31) | copy-start | bytes 12292
  311.0 20.2 %copy-start.7 = (bf16[64,2048]{1,0:T(8,128)(2,1)S(1)}, bf16[64,2048]{1,0:T(8,128)(2,1)}, u32[]{:S(2)}) copy-start(bf16[64,2048]{1,0:T(8,128)(2,1)} %param.19) | copy-start | bytes 786436
  311.0 20.0 %all-to-all-start = ((bf16[4,64,2048]{2,1,0:T(8,128)(2,1)}), bf16[4,64,2048]{2,1,0:T(8,128)(2,1)S(1)}, u32[]{:S(2)}, u32[]{:S(2)}) async-start(bf16[4,64,2048]{2,1,0:T(8,128)(2,1)} %bitcast.16), calls=%async_computation | async-start | bytes 2097152 | tf_op jit(solution)/shard_map/all_to_all | solution.py:28
  332.6 18.2 %all-to-all-start.1 = ((bf16[4,64,2048]{2,1,0:T(8,128)(2,1)}), bf16[4,64,2048]{2,1,0:T(8,128)(2,1)S(1)}, u32[]{:S(2)}, u32[]{:S(2)}) async-start(bf16[4,64,2048]{2,1,0:T(8,128)(2,1)} %broadcast_in_dim.4), calls=%async_computation.1 | async-start | bytes 2097152 | tf_op jit(solution)/shard_map/all_to_all | solution.py:40
  (46 other events, 33.9 us)
Sparse Core Ops, SparseCore 0:
  9.2 92.7 all-gather.3
  103.9 73.4 all-gather.5
  179.3 73.6 all-gather.7
where the time goes:
time: 388 us; the launch traced here: 385 us
  waiting for transfers between devices  122 us (31%)
  local copies, waits for them, and re-layouts  109 us (28%)
  matrix products  94.4 us (24%)
  other arithmetic  18.6 us (5%)
  blocking collectives  16.3 us (4%)
  between operations  13.4 us (3%)
  starting transfers between devices  8.37 us (2%)
    all_gather x1, waiting for transfers between devices, sent_together(): lax.all_gather(both, axis, axis=dim, tiled=True)  90.5 us
    while x224, local copies, waits for them, and re-layouts  54.1 us
    dot_general x32, matrix products, visit(): jnp.einsum('iodph,hie->iodpe', powers.astype(jnp.bfloat16), value_blk, pr...  52.6 us
    dot_general x32, matrix products, visit(): jnp.einsum('tkgcd,skcd->kgcts', grouped, key_blk, preferred_element_type=...  29.6 us
    dynamic_slice x16, local copies, waits for them, and re-layouts, absorb(): outcome, _ = lax.scan(visit, states, (key_block_list, value_blocks))  18.2 us
    all_to_all x1, blocking collectives, sent_and_summed(): parts = lax.all_to_all(split_up(array, dim, peers), axis, 0, 0, tiled=True)  16.3 us
    all_to_all x1, waiting for transfers between devices, sent_and_summed(): parts = lax.all_to_all(split_up(array, dim, peers), axis, 0, 0, tiled=True)  15.6 us
    all_to_all x1, waiting for transfers between devices, copy_for_each(): return lax.all_to_all(copies, axis, split_axis=0, concat_axis=0, tiled=True)  14.4 us
  transfers between devices with their start and end apart: 5, of which 3 were waited for; matrix products, arithmetic and copies ran while one was open for 40% of the time, Pallas kernels for 0%

commit v1 on v0

v1 whole, which is shorter than its diff:
```python
import functools
import math

import jax
import jax.numpy as jnp
from jax import lax
from jax.experimental import pallas as pl
from jax.experimental.pallas import tpu as pltpu
from jax.sharding import PartitionSpec as P

NORM_EPS = 1e-06
OUT_SCALE = 0.8
LOG2E = math.log2(math.e)
LAST_DIMS = (((1,), (1,)), ((), ()))
VMEM_LIMIT = 60 * 2**20


def split_up(array, dim, peers):
    before, after = (array.shape[:dim], array.shape[dim + 1 :])
    return jnp.moveaxis(array.reshape(*before, peers, -1, *after), dim, 0)


def sent_and_summed(array, axis, dim):
    peers = lax.axis_size(axis)
    parts = lax.all_to_all(split_up(array, dim, peers), axis, 0, 0, tiled=True)
    return jnp.sum(parts.astype(jnp.float32), axis=0)


def copy_for_each(array, axis):
    copies = jnp.broadcast_to(array, (lax.axis_size(axis), *array.shape))
    return lax.all_to_all(copies, axis, split_axis=0, concat_axis=0, tiled=True)


def attend_kernel(
    qn_ref, qw_ref, kv_ref, lam_ref, gain_ref, out_ref, q_s, m_s, acc_s, v_s, *, dn, dw, dv, steps
):
    step = pl.program_id(0)
    rows = qn_ref.shape[0]

    @pl.when(step == 0)
    def _():
        m_s[...] = jnp.full_like(m_s, -jnp.inf)
        acc_s[...] = jnp.zeros_like(acc_s)
        v_s[...] = jnp.ones_like(v_s)
        lane = lax.broadcasted_iota(jnp.int32, (rows, 2 * dn), 1)
        for h in range(2):
            q = qn_ref[:, h * 2 * dn : (h + 1) * 2 * dn]
            for c in range(2):
                keep = (lane < dn) if c == 0 else (lane >= dn)
                q_s[h * 2 + c] = jnp.where(keep, q, jnp.zeros_like(q))
                q_s[4 + h * 2 + c] = qw_ref[:, (h * 2 + c) * dw : (h * 2 + c + 1) * dw]

    at_vn = 2 * dn
    at_kw = at_vn + dv
    at_vw = at_kw + 2 * dw
    v_s[0, :, :dv] = kv_ref[:, at_vn : at_vn + dv]
    v_s[1, :, :dv] = kv_ref[:, at_vw : at_vw + dv]
    for u in range(8):
        wide, c = u >= 4, u % 2
        at = at_kw + c * dw if wide else 0
        width = dw if wide else 2 * dn
        scale = (dw if wide else dn) ** -0.5 * LOG2E
        s = lax.dot_general(
            q_s[u], kv_ref[:, at : at + width], LAST_DIMS, preferred_element_type=jnp.float32
        )
        m_old = m_s[u]
        m_new = jnp.maximum(m_old, jnp.max(s, axis=1, keepdims=True))
        powers = jnp.exp2((s - m_new) * scale).astype(jnp.bfloat16)
        rescale = jnp.exp2((m_old - m_new) * scale)
        m_s[u] = m_new
        acc_s[u] = acc_s[u] * rescale + jnp.dot(
            powers, v_s[int(wide)], preferred_element_type=jnp.float32
        )

    @pl.when(step == steps - 1)
    def _():
        for h in range(4):
            first, second = acc_s[2 * h], acc_s[2 * h + 1]
            o = first[:, :dv] / first[:, dv:] - lam_ref[h] * (second[:, :dv] / second[:, dv:])
            square = jnp.mean(o * o, axis=-1, keepdims=True)
            o = o * lax.rsqrt(square + NORM_EPS) * gain_ref[...] * OUT_SCALE
            out_ref[:, h * dv : (h + 1) * dv] = o.astype(out_ref.dtype)


def attention(qn, qw, kv, lam, gain):
    rows = qn.shape[0]
    keys, width = kv.shape
    dv = gain.shape[1]
    dn, dw = qn.shape[1] // 4, qw.shape[1] // 4
    block = math.gcd(keys, 2048)
    steps = keys // block
    return pl.pallas_call(
        functools.partial(attend_kernel, dn=dn, dw=dw, dv=dv, steps=steps),
        grid=(steps,),
        in_specs=[
            pl.BlockSpec(qn.shape, lambda i: (0, 0)),
            pl.BlockSpec(qw.shape, lambda i: (0, 0)),
            pl.BlockSpec((block, width), lambda i: (i, 0)),
            pl.BlockSpec(memory_space=pltpu.SMEM),
            pl.BlockSpec(gain.shape, lambda i: (0, 0)),
        ],
        out_specs=pl.BlockSpec((rows, 4 * dv), lambda i: (0, 0)),
        out_shape=jax.ShapeDtypeStruct((rows, 4 * dv), jnp.bfloat16),
        scratch_shapes=[
            pltpu.VMEM((8, rows, 128), jnp.bfloat16),
            pltpu.VMEM((8, rows, 1), jnp.float32),
            pltpu.VMEM((8, rows, 2 * dv), jnp.float32),
            pltpu.VMEM((2, block, 2 * dv), jnp.bfloat16),
        ],
        compiler_params=pltpu.CompilerParams(
            dimension_semantics=("arbitrary",), vmem_limit_bytes=VMEM_LIMIT
        ),
        cost_estimate=pl.CostEstimate(
            flops=16 * rows * keys * 256, bytes_accessed=keys * width * 2, transcendentals=8 * rows * keys
        ),
        name="attend",
    )(qn, qw, kv, lam, gain)


def mixer_kernel(x_ref, w_ref, out_ref, lifted, activated, *, half):
    step = pl.program_id(0)
    depth = w_ref.shape[0] * w_ref.shape[2]
    w = w_ref[...].reshape(depth, w_ref.shape[3])

    @pl.when(step < half)
    def _():
        at = pl.multiple_of(step * depth, depth)
        part = jnp.dot(x_ref[:, pl.ds(at, depth)], w, preferred_element_type=jnp.float32)

        @pl.when(step == 0)
        def _():
            lifted[...] = part

        @pl.when(step > 0)
        def _():
            lifted[...] += part

    @pl.when(step == half - 1)
    def _():
        up = jnp.maximum(lifted[...], 0.0)
        activated[...] = (up * up).astype(jnp.bfloat16)

    @pl.when(step >= half)
    def _():
        out_ref[...] = lax.dot_general(
            activated[...], w, LAST_DIMS, preferred_element_type=jnp.float32
        ).astype(jnp.bfloat16)


def mixer(x, w):
    rows, d = x.shape
    shards, _, each, hidden = w.shape
    group = math.gcd(shards, 8)
    half = shards // group
    depth = group * each
    return pl.pallas_call(
        functools.partial(mixer_kernel, half=half),
        grid=(2 * half,),
        in_specs=[
            pl.BlockSpec((rows, d), lambda i: (0, 0)),
            pl.BlockSpec((group, 1, each, hidden), lambda i: (i % half, i // half, 0, 0)),
        ],
        out_specs=pl.BlockSpec((rows, depth), lambda i: (0, jnp.maximum(i - half, 0))),
        out_shape=jax.ShapeDtypeStruct((rows, d), jnp.bfloat16),
        scratch_shapes=[
            pltpu.VMEM((rows, hidden), jnp.float32),
            pltpu.VMEM((rows, hidden), jnp.bfloat16),
        ],
        compiler_params=pltpu.CompilerParams(
            dimension_semantics=("arbitrary",), vmem_limit_bytes=VMEM_LIMIT
        ),
        cost_estimate=pl.CostEstimate(
            flops=4 * rows * d * hidden, bytes_accessed=4 * d * hidden, transcendentals=0
        ),
        name="mixer",
    )(x, w)


def shards(
    resid_in,
    query_narrow,
    key_narrow,
    value_narrow,
    query_wide,
    key_wide,
    value_wide,
    lambda_narrow,
    lambda_wide,
    head_gain,
    out_narrow,
    out_wide,
    norm_gain,
    up_weight,
    down_weight,
):
    rows = query_narrow.shape[0]
    own = jnp.concatenate(
        [a.reshape(rows, -1) for a in (key_narrow, value_narrow, key_wide, value_wide)], axis=1
    )
    kv = lax.all_gather(own, "sp", axis=0, tiled=True)
    own_weights = jnp.stack([up_weight, down_weight.T])
    weights = lax.all_gather(own_weights, "sp", axis=0, tiled=False)
    attended = attention(
        query_narrow.reshape(rows, -1),
        query_wide.reshape(rows, -1),
        kv,
        jnp.concatenate([lambda_narrow, lambda_wide]),
        head_gain.reshape(1, -1),
    )
    out_rows = jnp.concatenate([out_narrow, out_wide], axis=0)
    projected = sent_and_summed(
        jnp.dot(attended, out_rows, preferred_element_type=jnp.float32).astype(jnp.bfloat16), "tp", 0
    )
    middle = (resid_in.astype(jnp.float32) + projected).astype(jnp.bfloat16)
    middle_f32 = middle.astype(jnp.float32)
    normed = middle_f32 * lax.rsqrt(
        jnp.mean(middle_f32 * middle_f32, axis=-1, keepdims=True) + NORM_EPS
    )
    normed = (normed * norm_gain.astype(jnp.float32)).astype(jnp.bfloat16)
    whole_rows = copy_for_each(normed, "tp").reshape(-1, normed.shape[1])
    mixer_out = sent_and_summed(mixer(whole_rows, weights), "tp", 0)
    return (middle_f32 + mixer_out).astype(jnp.bfloat16)


def solution(mesh):
    placed = (
        P(("grp", "sp", "tp"), None),
        P(("grp", "sp"), "tp", None),
        P(("grp", "sp"), "tp", None),
        P(("grp", "sp"), "tp", None),
        P(("grp", "sp"), "tp", None),
        P(("grp", "sp"), "tp", None),
        P(("grp", "sp"), "tp", None),
        P("tp"),
        P("tp"),
        P(),
        P("tp", None),
        P("tp", None),
        P(),
        P("sp", "tp"),
        P("tp", "sp"),
    )
    return jax.shard_map(
        shards, mesh=mesh, in_specs=placed, out_specs=P(("grp", "sp", "tp"), None), check_vma=False
    )
```

time: 388 us -> 247 us (0.64)
  local copies, waits for them, and re-layouts: 109 us -> 1.54 us
  matrix products: 94.4 us -> 2.67 us
  Pallas kernels: 0 us -> 39.7 us
  blocking collectives: 16.3 us -> 37.6 us
  waiting for transfers between devices: 122 us -> 140 us
  other arithmetic: 18.6 us -> 5.7 us
    dot_general x67 -> x1, matrix products: 94.4 us -> 2.67 us  [shards(): jnp.dot(attended, out_rows, preferred_element_type=jnp.float32)]
    while x226 -> x0, local copies, waits for them, and re-layouts: 57.4 us -> none
    pallas_call x0 -> x2, Pallas kernels: none -> 39.7 us  [the longest x1 26.8 us: attention(): pl.pallas_call(functools.partial(attend_kernel, dn=dn, dw=dw, dv=dv, step...]
    all_gather x3 -> x2, waiting for transfers between devices: 90.5 us -> 125 us  [the longest x1 89.5 us: shards(): kv = lax.all_gather(own, 'sp', axis=0, tiled=True)]
    dynamic_slice x16 -> x0, local copies, waits for them, and re-layouts: 18.2 us -> none  [absorb(): outcome, _ = lax.scan(visit, states, (key_block_list, value_blocks))]
    all_to_all x0 -> x1, blocking collectives: none -> 17.8 us  [copy_for_each(): return lax.all_to_all(copies, axis, split_axis=0, concat_axis=0, tiled=True)]
    all_to_all x1 -> x0, waiting for transfers between devices: 14.4 us -> none  [copy_for_each(): return lax.all_to_all(copies, axis, split_axis=0, concat_axis=0, tiled=True)]
    unnamed x23 -> x18, local copies, waits for them, and re-layouts: 12.6 us -> 1.43 us
  transfers between devices with their start and end apart: 5 -> 3, of which waited for: 3 -> 3; matrix products, arithmetic and copies ran while one was open for 40% -> 3% of each run, Pallas kernels for 0% -> 11%
where the time goes in v1:
time: 247 us; the launch traced here: 246 us
  waiting for transfers between devices  140 us (57%)
  Pallas kernels  39.7 us (16%)
  blocking collectives  37.6 us (15%)
  between operations  13.5 us (5%)
  other arithmetic  5.7 us (2%)
  starting transfers between devices  4.49 us (2%)
  matrix products  2.67 us (1%)
    all_gather x1, waiting for transfers between devices, shards(): kv = lax.all_gather(own, 'sp', axis=0, tiled=True)  89.5 us
    all_gather x1, waiting for transfers between devices, shards(): weights = lax.all_gather(own_weights, 'sp', axis=0, tiled=False)  35.3 us
    pallas_call x1, Pallas kernels, attention(): pl.pallas_call(functools.partial(attend_kernel, dn=dn, dw=dw, dv=dv, step...  26.8 us
    all_to_all x1, blocking collectives, sent_and_summed(): parts = lax.all_to_all(split_up(array, dim, peers), axis, 0, 0, tiled=True)  19.8 us
    all_to_all x1, blocking collectives, copy_for_each(): return lax.all_to_all(copies, axis, split_axis=0, concat_axis=0, tiled=True)  17.8 us
    all_to_all x1, waiting for transfers between devices, sent_and_summed(): parts = lax.all_to_all(split_up(array, dim, peers), axis, 0, 0, tiled=True)  15.5 us
    pallas_call x1, Pallas kernels, mixer(): pl.pallas_call(functools.partial(mixer_kernel, half=half), grid=(2 * half...  12.9 us
  transfers between devices with their start and end apart: 3, of which 3 were waited for; matrix products, arithmetic and copies ran while one was open for 3% of the time, Pallas kernels for 11%

profile of v1, /device:TPU:40, one launch (start us, length us, event | category | flops | bytes accessed | tf_op | source)
XLA Modules:
  0.0 245.5 jit_solution(7888438123518681350)
XLA Ops:
  6.5 0.0 copy-start
  6.5 0.0 copy-start.2
  6.6 0.0 copy-start.7
  6.6 0.0 copy-start.6
  6.6 0.1 all-gather.4.cloned.1.call-start
  6.6 1.8 pad_maximum_fusion.1
  8.4 0.1 all-gather.4.cloned.1.call-update
  8.5 0.1 all-gather.6.cloned.1.call-start
  8.5 1.9 pad_maximum_fusion
  10.5 0.1 all-gather.6.cloned.1.call-update
  10.5 0.0 copy-done
  10.5 0.7 copy.17
  11.3 0.0 copy-done.2
  11.3 0.7 copy.19
  11.9 0.0 copy-done.7
  11.9 0.0 copy-done.6
  11.9 0.6 pad_maximum_fusion.2.lam_ref
  12.5 89.5 %all-gather.4.cloned.1.call-done.kv_ref = bf16[8192,640]{1,0:T(8,128)(2,1)} async-done(((bf16[256,640]{1,0:T(8,128)(2,1)}), bf16[8192,640]{1,0:T(8,128)(2,1)}) %all-gather.4.cloned.1.call-update) | async-done | bytes 10485776 | tf_op jit(solution)/shard_map/all_gather | solution.py:200
  102.1 0.0 copy-start.4
  102.1 0.0 copy-start.5
  102.1 26.8 %attend.1 = bf16[256,512]{1,0:T(8,128)(2,1)} custom-call(bf16[256,256]{1,0:T(8,128)(2,1)} %bitcast.29, bf16[256,512]{1,0:T(8,128)(2,1)} %bitcast.24, bf16[8192,640]{1,0:T(8,128)(2,1)} %all-gather.4.cloned.1.call-done.kv_ref, f32[4]{0:T(128)} %pad_maximum_fusion.2.lam_ref, f32[1,128]{1,0:T(1,128)} %bitcast.33), custom_call_target="tpu_custom_call" | custom-call | flops 8589934592 | bytes 10485760 | tf_op jit(solution)/shard_map/attend/pallas_call | solution.py:92
  128.9 0.0 copy-done.4
  128.9 0.0 copy-done.5
  128.9 2.7 %convolution_convert_fusion = bf16[256,2048]{1,0:T(8,128)(2,1)} fusion(bf16[256,512]{1,0:T(8,128)(2,1)} %attend.1, bf16[256,2048]{1,0:T(8,128)(2,1)S(1)} %copy-done.4, bf16[256,2048]{1,0:T(8,128)(2,1)S(1)} %copy-done.5), kind=kOutput, calls=%fused_computation | convolution fusion | flops 541589504 | bytes 3407872 | tf_op jit(solution)/shard_map/dot_general | solution.py:212
  131.6 0.0 copy-start.3
  131.6 0.0 copy-start.1
  131.6 4.4 %all-to-all-start = ((bf16[4,64,2048]{2,1,0:T(8,128)(2,1)}), bf16[4,64,2048]{2,1,0:T(8,128)(2,1)S(1)}, u32[]{:S(2)}, u32[]{:S(2)}) async-start(bf16[4,64,2048]{2,1,0:T(8,128)(2,1)} %bitcast.5), calls=%async_computation | async-start | bytes 2097152 | tf_op jit(solution)/shard_map/all_to_all | solution.py:25
  135.9 0.0 copy-done.3
  136.0 15.5 %all-to-all-done = bf16[4,64,2048]{2,1,0:T(8,128)(2,1)S(1)} async-done(((bf16[4,64,2048]{2,1,0:T(8,128)(2,1)}), bf16[4,64,2048]{2,1,0:T(8,128)(2,1)S(1)}, u32[]{:S(2)}, u32[]{:S(2)}) %all-to-all-start) | async-done | bytes 1048608 | tf_op jit(solution)/shard_map/all_to_all | solution.py:25
  151.4 0.2 convert_reduce_fusion.1
  151.6 0.0 copy-done.1
  151.6 0.2 fusion.3
  151.8 0.1 fusion.5
  151.9 0.1 broadcast_in_dim.2
  152.1 17.8 %all_to_all.15 = bf16[4,64,2048]{2,1,0:T(8,128)(2,1)} all-to-all(bf16[4,64,2048]{2,1,0:T(8,128)(2,1)S(1)} %broadcast_in_dim.2), channel_id=1, replica_groups=mesh['grp'=2,'sp'=32,'tp'=4] {'tp'}, dimensions={0} | all-to-all | bytes 2097152 | tf_op jit(solution)/shard_map/all_to_all | solution.py:31
  169.9 35.3 %all-gather.6.cloned.1.call-done = bf16[64,64,2048]{2,1,0:T(8,128)(2,1)} async-done(((bf16[2,64,2048]{2,1,0:T(8,128)(2,1)}), bf16[64,64,2048]{2,1,0:T(8,128)(2,1)}) %all-gather.6.cloned.1.call-update) | async-done | bytes 16777232 | tf_op jit(solution)/shard_map/all_gather | solution.py:202
  205.1 12.9 %mixer.1 = bf16[256,2048]{1,0:T(8,128)(2,1)} custom-call(bf16[256,2048]{1,0:T(8,128)(2,1)} %bitcast.21, bf16[32,2,64,2048]{3,2,1,0:T(8,128)(2,1)} %bitcast.20), custom_call_target="tpu_custom_call" | custom-call | flops 4294967296 | bytes 16777216 | tf_op jit(solution)/shard_map/mixer/pallas_call | solution.py:156
  218.0 19.8 %all_to_all.16 = bf16[4,64,2048]{2,1,0:T(8,128)(2,1)S(1)} all-to-all(bf16[4,64,2048]{2,1,0:T(8,128)(2,1)} %bitcast.22), channel_id=1, replica_groups=mesh['grp'=2,'sp'=32,'tp'=4] {'tp'}, dimensions={0} | all-to-all | bytes 2097152 | tf_op jit(solution)/shard_map/all_to_all | solution.py:25
  237.8 0.2 convert_reduce_fusion
  237.9 0.8 fusion.6
  (2 shorter events, 0.0 us)
Async XLA Ops:
  6.5 4.0 %copy-start = (bf16[256,2,256]{2,1,0:T(2,128)(2,1)S(1)}, bf16[256,2,256]{2,1,0:T(2,128)(2,1)}, u32[]{:S(2)}) copy-start(bf16[256,2,256]{2,1,0:T(2,128)(2,1)} %param.19) | copy-start | bytes 786436
  6.5 4.7 %copy-start.2 = (bf16[256,2,128]{2,1,0:T(2,128)(2,1)S(1)}, bf16[256,2,128]{2,1,0:T(2,128)(2,1)}, u32[]{:S(2)}) copy-start(bf16[256,2,128]{2,1,0:T(2,128)(2,1)} %param.16) | copy-start | bytes 393220
  6.6 5.4 %copy-start.7 = (f32[2]{0:T(128)S(1)}, f32[2]{0:T(128)}, u32[]{:S(2)}) copy-start(f32[2]{0:T(128)} %param.22) | copy-start | bytes 28
  6.6 5.4 %copy-start.6 = (f32[2]{0:T(128)S(1)}, f32[2]{0:T(128)}, u32[]{:S(2)}) copy-start(f32[2]{0:T(128)} %param.23) | copy-start | bytes 28
  6.6 95.5 %all-gather.4.cloned.1.call-start = ((), (), s32[]{:S(2)}) async-start(), calls=%async_computation.3 | async-start | bytes 10813440 | tf_op jit(solution)/shard_map/all_gather | solution.py:200
  8.5 196.7 %all-gather.6.cloned.1.call-start = ((), (), s32[]{:S(2)}) async-start(), calls=%async_computation.4 | async-start | bytes 17301504 | tf_op jit(solution)/shard_map/all_gather | solution.py:202
  102.1 26.8 %copy-start.4 = (bf16[256,2048]{1,0:T(8,128)(2,1)S(1)}, bf16[256,2048]{1,0:T(8,128)(2,1)}, u32[]{:S(2)}) copy-start(bf16[256,2048]{1,0:T(8,128)(2,1)} %param.26) | copy-start | bytes 3145732
  102.1 26.8 %copy-start.5 = (bf16[256,2048]{1,0:T(8,128)(2,1)S(1)}, bf16[256,2048]{1,0:T(8,128)(2,1)}, u32[]{:S(2)}) copy-start(bf16[256,2048]{1,0:T(8,128)(2,1)} %param.25) | copy-start | bytes 3145732
  131.6 4.4 %copy-start.3 = (bf16[2048]{0:T(1024)(128)(2,1)S(1)}, bf16[2048]{0:T(1024)(128)(2,1)}, u32[]{:S(2)}) copy-start(bf16[2048]{0:T(1024)(128)(2,1)} %param.27) | copy-start | bytes 12292
  131.6 20.0 %copy-start.1 = (bf16[64,2048]{1,0:T(8,128)(2,1)S(1)}, bf16[64,2048]{1,0:T(8,128)(2,1)}, u32[]{:S(2)}) copy-start(bf16[64,2048]{1,0:T(8,128)(2,1)} %param.15) | copy-start | bytes 786436
  131.6 19.9 %all-to-all-start = ((bf16[4,64,2048]{2,1,0:T(8,128)(2,1)}), bf16[4,64,2048]{2,1,0:T(8,128)(2,1)S(1)}, u32[]{:S(2)}, u32[]{:S(2)}) async-start(bf16[4,64,2048]{2,1,0:T(8,128)(2,1)} %bitcast.5), calls=%async_computation | async-start | bytes 2097152 | tf_op jit(solution)/shard_map/all_to_all | solution.py:25
Sparse Core Ops, SparseCore 0:
  9.2 92.7 all-gather.3
  103.9 101.1 all-gather.5

commit v2 on v1

--- a/solution.py
+++ b/solution.py
@@ -8,11 +8,14 @@
 from jax.experimental.pallas import tpu as pltpu
 from jax.sharding import PartitionSpec as P
 
+
 NORM_EPS = 1e-06
 OUT_SCALE = 0.8
 LOG2E = math.log2(math.e)
 LAST_DIMS = (((1,), (1,)), ((), ()))
-VMEM_LIMIT = 60 * 2**20
+VMEM_LIMIT = 28 * 2**20
+EARLY = 8
+BATCHES = ()
 
 
 def split_up(array, dim, peers):
@@ -26,18 +29,61 @@
     return jnp.sum(parts.astype(jnp.float32), axis=0)
 
 
+def after(array, *others):
+    return lax.optimization_barrier((array, *others))[0]
+
+
 def copy_for_each(array, axis):
     copies = jnp.broadcast_to(array, (lax.axis_size(axis), *array.shape))
     return lax.all_to_all(copies, axis, split_axis=0, concat_axis=0, tiled=True)
 
 
+def ring(block, batches):
+    peers = lax.axis_size("sp")
+    chips = peers // 2
+    onward = [(i, (i + 2) % peers) for i in range(peers)]
+    backward = [(i, (i - 2) % peers) for i in range(peers)]
+    ahead, behind = block, block
+    waiting, stacks, places = [block], [], [0]
+    for step in range(1, chips // 2 + 1):
+        ahead = lax.ppermute(ahead, "sp", onward)
+        waiting.append(ahead)
+        places.append(-step % chips)
+        if step < chips - chips // 2:
+            behind = lax.ppermute(behind, "sp", backward)
+            waiting.append(behind)
+            places.append(step)
+        if step in batches or step == chips // 2:
+            stacks.append(stacked(waiting))
+            waiting = []
+    return stacks, places
+
+
+def stack_kernel(*refs):
+    for i, block in enumerate(refs[:-1]):
+        refs[-1][i] = block[...]
+
+
+def stacked(blocks):
+    vmem = pl.BlockSpec(memory_space=pltpu.VMEM)
+    return pl.pallas_call(
+        stack_kernel,
+        in_specs=[vmem] * len(blocks),
+        out_specs=vmem,
+        out_shape=jax.ShapeDtypeStruct((len(blocks), *blocks[0].shape), blocks[0].dtype),
+        compiler_params=pltpu.CompilerParams(vmem_limit_bytes=12 * 2**20),
+        name="stack",
+    )(*blocks)
+
+
 def attend_kernel(
-    qn_ref, qw_ref, kv_ref, lam_ref, gain_ref, out_ref, q_s, m_s, acc_s, v_s, *, dn, dw, dv, steps
+    qn_ref, qw_ref, kv_ref, lam_ref, gain_ref, out_ref, q_s, m_s, acc_s, v_s, *, dn, dw, dv, steps, parts
 ):
-    step = pl.program_id(0)
+    step, part = pl.program_id(0), pl.program_id(1)
     rows = qn_ref.shape[0]
-
-    @pl.when(step == 0)
+    some = pl.ds(pl.multiple_of(part * (rows // parts), rows // parts), rows // parts)
+
+    @pl.when((step == 0) & (part == 0))
     def _():
         m_s[...] = jnp.full_like(m_s, -jnp.inf)
         acc_s[...] = jnp.zeros_like(acc_s)
@@ -53,26 +99,30 @@
     at_vn = 2 * dn
     at_kw = at_vn + dv
     at_vw = at_kw + 2 * dw
-    v_s[0, :, :dv] = kv_ref[:, at_vn : at_vn + dv]
-    v_s[1, :, :dv] = kv_ref[:, at_vw : at_vw + dv]
+
+    @pl.when(part == 0)
+    def _():
+        v_s[0, :, :dv] = kv_ref[:, at_vn : at_vn + dv]
+        v_s[1, :, :dv] = kv_ref[:, at_vw : at_vw + dv]
+
     for u in range(8):
         wide, c = u >= 4, u % 2
         at = at_kw + c * dw if wide else 0
         width = dw if wide else 2 * dn
         scale = (dw if wide else dn) ** -0.5 * LOG2E
         s = lax.dot_general(
-            q_s[u], kv_ref[:, at : at + width], LAST_DIMS, preferred_element_type=jnp.float32
+            q_s[u, some], kv_ref[:, at : at + width], LAST_DIMS, preferred_element_type=jnp.float32
         )
-        m_old = m_s[u]
+        m_old = m_s[u, some]
         m_new = jnp.maximum(m_old, jnp.max(s, axis=1, keepdims=True))
         powers = jnp.exp2((s - m_new) * scale).astype(jnp.bfloat16)
         rescale = jnp.exp2((m_old - m_new) * scale)
-        m_s[u] = m_new
-        acc_s[u] = acc_s[u] * rescale + jnp.dot(
+        m_s[u, some] = m_new
+        acc_s[u, some] = acc_s[u, some] * rescale + jnp.dot(
             powers, v_s[int(wide)], preferred_element_type=jnp.float32
         )
 
-    @pl.when(step == steps - 1)
+    @pl.when((step == steps - 1) & (part == parts - 1))
     def _():
         for h in range(4):
             first, second = acc_s[2 * h], acc_s[2 * h + 1]
@@ -90,16 +140,16 @@
     block = math.gcd(keys, 2048)
     steps = keys // block
     return pl.pallas_call(
-        functools.partial(attend_kernel, dn=dn, dw=dw, dv=dv, steps=steps),
-        grid=(steps,),
+        functools.partial(attend_kernel, dn=dn, dw=dw, dv=dv, steps=steps, parts=2),
+        grid=(steps, 2),
         in_specs=[
-            pl.BlockSpec(qn.shape, lambda i: (0, 0)),
-            pl.BlockSpec(qw.shape, lambda i: (0, 0)),
-            pl.BlockSpec((block, width), lambda i: (i, 0)),
+            pl.BlockSpec(qn.shape, lambda i, j: (0, 0)),
+            pl.BlockSpec(qw.shape, lambda i, j: (0, 0)),
+            pl.BlockSpec((block, width), lambda i, j: (i, 0)),
             pl.BlockSpec(memory_space=pltpu.SMEM),
-            pl.BlockSpec(gain.shape, lambda i: (0, 0)),
-        ],
-        out_specs=pl.BlockSpec((rows, 4 * dv), lambda i: (0, 0)),
+            pl.BlockSpec(gain.shape, lambda i, j: (0, 0)),
+        ],
+        out_specs=pl.BlockSpec((rows, 4 * dv), lambda i, j: (0, 0)),
         out_shape=jax.ShapeDtypeStruct((rows, 4 * dv), jnp.bfloat16),
         scratch_shapes=[
             pltpu.VMEM((8, rows, 128), jnp.bfloat16),
@@ -108,7 +158,7 @@
             pltpu.VMEM((2, block, 2 * dv), jnp.bfloat16),
         ],
         compiler_params=pltpu.CompilerParams(
-            dimension_semantics=("arbitrary",), vmem_limit_bytes=VMEM_LIMIT
+            dimension_semantics=("arbitrary", "arbitrary"), vmem_limit_bytes=VMEM_LIMIT
         ),
         cost_estimate=pl.CostEstimate(
             flops=16 * rows * keys * 256, bytes_accessed=keys * width * 2, transcendentals=8 * rows * keys
@@ -117,7 +167,71 @@
     )(qn, qw, kv, lam, gain)
 
 
-def mixer_kernel(x_ref, w_ref, out_ref, lifted, activated, *, half):
+def early_mixer_kernel(chip_ref, x_ref, *refs, places, batches):
+    weights, (out_ref, x_s, out_s) = refs[:-3], refs[-3:]
+    chips = len(places)
+    each = x_ref.shape[1] // chips
+
+    def columns(at):
+        chip = lax.rem(chip_ref[0] + at, chips)
+        return pl.ds(pl.multiple_of(chip * each, each), each)
+
+    for i, at in enumerate(places):
+        x_s[:, i * each : (i + 1) * each] = x_ref[:, columns(at)]
+    for first in range(0, len(weights), batches):
+        some = weights[first : first + batches]
+        lifted, start = 0.0, 0
+        for w in some:
+            up = w[:, :, 0].reshape(-1, w.shape[4])
+            lifted += jnp.dot(
+                x_s[:, start : start + up.shape[0]], up, preferred_element_type=jnp.float32
+            )
+            start += up.shape[0]
+        lifted = jnp.maximum(lifted, 0.0)
+        activated = (lifted * lifted).astype(jnp.bfloat16)
+        start = 0
+        for w in some:
+            down = w[:, :, 1].reshape(-1, w.shape[4])
+            part = lax.dot_general(
+                activated, down, LAST_DIMS, preferred_element_type=jnp.float32
+            )
+            to = slice(start, start + down.shape[0])
+            out_s[:, to] = part if first == 0 else out_s[:, to] + part
+            start += down.shape[0]
+    for i, at in enumerate(places):
+        out_ref[:, columns(at)] = out_s[:, i * each : (i + 1) * each]
+
+
+def early_mixer(x, weights, places, batches):
+    rows, d = x.shape
+    half = pl.BlockSpec((rows // 2, d), lambda i: (i, 0))
+    hidden = sum(w.shape[4] for w in weights[::batches])
+    chip = (lax.axis_index("sp") // 2).astype(jnp.int32).reshape(1)
+    return pl.pallas_call(
+        functools.partial(early_mixer_kernel, places=places, batches=batches),
+        grid=(2,),
+        in_specs=[
+            pl.BlockSpec(memory_space=pltpu.SMEM),
+            half,
+            *(pl.BlockSpec(memory_space=pltpu.VMEM) for _ in weights),
+        ],
+        out_specs=half,
+        out_shape=jax.ShapeDtypeStruct((rows, d), jnp.float32),
+        scratch_shapes=[
+            pltpu.VMEM((rows // 2, d), jnp.bfloat16),
+            pltpu.VMEM((rows // 2, d), jnp.float32),
+        ],
+        compiler_params=pltpu.CompilerParams(
+            dimension_semantics=("arbitrary",), vmem_limit_bytes=30 * 2**20
+        ),
+        cost_estimate=pl.CostEstimate(
+            flops=4 * rows * d * hidden, bytes_accessed=4 * d * hidden, transcendentals=0
+        ),
+        name="early_mixer",
+    )(chip, x, *weights)
+
+
+def mixer_kernel(x_ref, w_ref, early_ref, out_ref, lifted, activated, *, half):
     step = pl.program_id(0)
     depth = w_ref.shape[0] * w_ref.shape[2]
     w = w_ref[...].reshape(depth, w_ref.shape[3])
@@ -142,12 +256,11 @@
 
     @pl.when(step >= half)
     def _():
-        out_ref[...] = lax.dot_general(
-            activated[...], w, LAST_DIMS, preferred_element_type=jnp.float32
-        ).astype(jnp.bfloat16)
-
-
-def mixer(x, w):
+        part = lax.dot_general(activated[...], w, LAST_DIMS, preferred_element_type=jnp.float32)
+        out_ref[...] = (early_ref[...] + part).astype(jnp.bfloat16)
+
+
+def mixer(x, w, early):
     rows, d = x.shape
     shards, _, each, hidden = w.shape
     group = math.gcd(shards, 8)
@@ -159,6 +272,7 @@
         in_specs=[
             pl.BlockSpec((rows, d), lambda i: (0, 0)),
             pl.BlockSpec((group, 1, each, hidden), lambda i: (i % half, i // half, 0, 0)),
+            pl.BlockSpec((rows, depth), lambda i: (0, jnp.maximum(i - half, 0))),
         ],
         out_specs=pl.BlockSpec((rows, depth), lambda i: (0, jnp.maximum(i - half, 0))),
         out_shape=jax.ShapeDtypeStruct((rows, d), jnp.bfloat16),
@@ -167,13 +281,13 @@
             pltpu.VMEM((rows, hidden), jnp.bfloat16),
         ],
         compiler_params=pltpu.CompilerParams(
-            dimension_semantics=("arbitrary",), vmem_limit_bytes=VMEM_LIMIT
+            dimension_semantics=("arbitrary",), vmem_limit_bytes=20 * 2**20
         ),
         cost_estimate=pl.CostEstimate(
             flops=4 * rows * d * hidden, bytes_accessed=4 * d * hidden, transcendentals=0
         ),
         name="mixer",
-    )(x, w)
+    )(x, w, early)
 
 
 def shards(
@@ -194,12 +308,32 @@
     down_weight,
 ):
     rows = query_narrow.shape[0]
+    sp, grp = lax.axis_size("sp"), lax.axis_size("grp")
+    core, side = lax.axis_index("sp") % 2, lax.axis_index("grp") % 2
+    other_core = [(i, i ^ 1) for i in range(sp)]
+    other_group = [(i, i ^ 1) for i in range(grp)]
     own = jnp.concatenate(
         [a.reshape(rows, -1) for a in (key_narrow, value_narrow, key_wide, value_wide)], axis=1
     )
     kv = lax.all_gather(own, "sp", axis=0, tiled=True)
     own_weights = jnp.stack([up_weight, down_weight.T])
-    weights = lax.all_gather(own_weights, "sp", axis=0, tiled=False)
+    hidden = up_weight.shape[1]
+    share = hidden * EARLY // 16
+    each = share // 4
+    late_weights = lax.all_gather(own_weights[:, :, share:], "sp", axis=0, tiled=False)
+    mine = lax.dynamic_slice_in_dim(own_weights, (2 * side + core) * each, each, 2)
+    theirs = lax.dynamic_slice_in_dim(own_weights, (2 * side + 1 - core) * each, each, 2)
+    theirs = lax.ppermute(theirs, "sp", other_core)
+    chip = jnp.where(core == 0, jnp.stack([mine, theirs]), jnp.stack([theirs, mine]))
+    stacks, places = ring(chip, BATCHES)
+    early_weights = [[], [], [], []]
+    for stack in stacks:
+        swapped = lax.ppermute(stack, "grp", other_group)
+        first = lax.ppermute(stack, "sp", other_core)
+        second = lax.ppermute(swapped, "sp", other_core)
+        for kind, array in zip(early_weights, (stack, first, swapped, second)):
+            kind.append(array)
+    kv = after(kv, *stacks)
     attended = attention(
         query_narrow.reshape(rows, -1),
         query_wide.reshape(rows, -1),
@@ -208,17 +342,17 @@
         head_gain.reshape(1, -1),
     )
     out_rows = jnp.concatenate([out_narrow, out_wide], axis=0)
-    projected = sent_and_summed(
-        jnp.dot(attended, out_rows, preferred_element_type=jnp.float32).astype(jnp.bfloat16), "tp", 0
-    )
+    projected = jnp.dot(attended, out_rows, preferred_element_type=jnp.float32)
+    projected = sent_and_summed(projected.astype(jnp.bfloat16), "tp", 0)
     middle = (resid_in.astype(jnp.float32) + projected).astype(jnp.bfloat16)
     middle_f32 = middle.astype(jnp.float32)
     normed = middle_f32 * lax.rsqrt(
         jnp.mean(middle_f32 * middle_f32, axis=-1, keepdims=True) + NORM_EPS
     )
     normed = (normed * norm_gain.astype(jnp.float32)).astype(jnp.bfloat16)
-    whole_rows = copy_for_each(normed, "tp").reshape(-1, normed.shape[1])
-    mixer_out = sent_and_summed(mixer(whole_rows, weights), "tp", 0)
+    normed = copy_for_each(normed, "tp").reshape(-1, normed.shape[1])
+    early = early_mixer(normed, sum(early_weights, []), places, len(stacks))
+    mixer_out = sent_and_summed(mixer(normed, late_weights, early), "tp", 0)
     return (middle_f32 + mixer_out).astype(jnp.bfloat16)
 
 

time: 247 us -> 233 us (0.943)
  waiting for transfers between devices: 140 us -> 91.7 us
  starting transfers between devices: 4.49 us -> 51.4 us
  blocking collectives: 37.6 us -> 16.2 us
  local copies, waits for them, and re-layouts: 1.54 us -> 11.6 us
    all_gather x1, waiting for transfers between devices: 89.5 us -> 11.5 us  [shards(): kv = lax.all_gather(own, 'sp', axis=0, tiled=True)]
    ppermute x0 -> x19, waiting for transfers between devices: none -> 50.6 us  [the longest x8 49.3 us: ring(): ahead = lax.ppermute(ahead, 'sp', onward)]
    ppermute x0 -> x19, starting transfers between devices: none -> 43.5 us  [the longest x7 39.8 us: ring(): behind = lax.ppermute(behind, 'sp', backward)]
    all_gather x1, waiting for transfers between devices: 35.3 us -> 0.01 us  [shards(): lax.all_gather(own_weights[:, :, share:], 'sp', axis=0, tiled=False)]
    all_to_all x1 -> x0, blocking collectives: 17.8 us -> none  [copy_for_each(): return lax.all_to_all(copies, axis, split_axis=0, concat_axis=0, tiled=True)]
    all_to_all x0 -> x1, waiting for transfers between devices: none -> 14.5 us  [copy_for_each(): return lax.all_to_all(copies, axis, split_axis=0, concat_axis=0, tiled=True)]
    unnamed x18 -> x32, local copies, waits for them, and re-layouts: 1.43 us -> 10.4 us
    pallas_call x0 -> x2, Pallas kernels: none -> 7.93 us  [the longest x1 7.79 us: early_mixer(): pl.pallas_call(functools.partial(early_mixer_kernel, places=places, batch...]
  transfers between devices with their start and end apart: 3 -> 23, of which waited for: 3 -> 13; matrix products, arithmetic and copies ran while one was open for 3% -> 2% of each run, Pallas kernels for 11% -> 15%
where the time goes in v2:
time: 233 us
  waiting for transfers between devices  91.7 us (39%)
  starting transfers between devices  51.4 us (22%)
  Pallas kernels  41.4 us (18%)
  blocking collectives  16.2 us (7%)
  between operations  13.7 us (6%)
  local copies, waits for them, and re-layouts  11.6 us (5%)
  other arithmetic  4.99 us (2%)
    ppermute x8, waiting for transfers between devices, ring(): ahead = lax.ppermute(ahead, 'sp', onward)  49.3 us
    ppermute x7, starting transfers between devices, ring(): behind = lax.ppermute(behind, 'sp', backward)  39.8 us
    pallas_call x1, Pallas kernels, attention(): pl.pallas_call(functools.partial(attend_kernel, dn=dn, dw=dw, dv=dv, step...  27.8 us
    all_to_all x1, blocking collectives, sent_and_summed(): parts = lax.all_to_all(split_up(array, dim, peers), axis, 0, 0, tiled=True)  16.2 us
    all_to_all x1, waiting for transfers between devices, sent_and_summed(): parts = lax.all_to_all(split_up(array, dim, peers), axis, 0, 0, tiled=True)  15 us
    all_to_all x1, waiting for transfers between devices, copy_for_each(): return lax.all_to_all(copies, axis, split_axis=0, concat_axis=0, tiled=True)  14.5 us
    all_gather x1, waiting for transfers between devices, shards(): kv = lax.all_gather(own, 'sp', axis=0, tiled=True)  11.5 us
    unnamed x32, local copies, waits for them, and re-layouts  10.4 us
  transfers between devices with their start and end apart: 23, of which 13 were waited for; matrix products, arithmetic and copies ran while one was open for 2% of the time, Pallas kernels for 15%

profile of v2, /device:TPU:40, one launch (start us, length us, event | category | flops | bytes accessed | tf_op | source)
XLA Modules:
  0.0 232.8 jit_solution(14717310703395905811)
XLA Ops:
  6.6 1.8 pad_maximum_fusion
  8.3 0.1 all-gather.4.cloned.1.call-update
  8.4 0.1 all-gather.6.cloned.1.call-start
  8.5 1.7 pad_maximum_fusion.1
  10.2 0.1 all-gather.6.cloned.1.call-update
  10.3 0.1 collective-permute-start
  10.5 1.2 collective-permute-done
  11.7 0.0 copy-start.7
  11.7 0.0 copy-start.9
  11.7 0.0 copy-start.13
  11.8 0.0 copy-start.14
  11.8 0.0 copy-start.4
  11.8 2.9 %collective-permute-start.1 = (bf16[2,2,64,256]{3,2,1,0:T(8,128)(2,1)S(1)}, bf16[2,2,64,256]{3,2,1,0:T(8,128)(2,1)S(1)}, u32[]{:S(2)}, u32[]{:S(2)}) collective-permute-start(bf16[2,2,64,256]{3,2,1,0:T(8,128)(2,1)S(1)} %maximum_select_fusion.refs_0_), channel_id=1, source_target_pairs={{0,8},{4,12},{8,16},{12,20},{16,24},{20,28},{24,32},{28,36},{32,40... | collective-permute-start | bytes 393224 | tf_op jit(solution)/shard_map/ppermute | solution.py:49
  14.7 19.7 %collective-permute-start.2 = (bf16[2,2,64,256]{3,2,1,0:T(8,128)(2,1)S(1)}, bf16[2,2,64,256]{3,2,1,0:T(8,128)(2,1)S(1)}, u32[]{:S(2)}, u32[]{:S(2)}) collective-permute-start(bf16[2,2,64,256]{3,2,1,0:T(8,128)(2,1)S(1)} %maximum_select_fusion.refs_0_), channel_id=1, source_target_pairs={{0,120},{4,124},{8,0},{12,4},{16,8},{20,12},{24,16},{28,20},{32,24... | collective-permute-start | bytes 393224 | tf_op jit(solution)/shard_map/ppermute | solution.py:53
  34.4 3.7 %collective-permute-done.1.refs_1_ = bf16[2,2,64,256]{3,2,1,0:T(8,128)(2,1)S(1)} collective-permute-done((bf16[2,2,64,256]{3,2,1,0:T(8,128)(2,1)S(1)}, bf16[2,2,64,256]{3,2,1,0:T(8,128)(2,1)S(1)}, u32[]{:S(2)}, u32[]{:S(2)}) %collective-permute-start.1) | collective-permute-done | bytes 131104 | tf_op jit(solution)/shard_map/ppermute | solution.py:49
  38.1 0.0 collective-permute-start.3
  38.1 0.1 collective-permute-done.2.refs_2_
  38.2 3.7 %collective-permute-start.4 = (bf16[2,2,64,256]{3,2,1,0:T(8,128)(2,1)S(1)}, bf16[2,2,64,256]{3,2,1,0:T(8,128)(2,1)S(1)}, u32[]{:S(2)}, u32[]{:S(2)}) collective-permute-start(bf16[2,2,64,256]{3,2,1,0:T(8,128)(2,1)S(1)} %collective-permute-done.2.refs_2_), channel_id=1, source_target_pairs={{0,120},{4,124},{8,0},{12,4},{16,8},{20,12},{24,16},{28,20},{32,24... | collective-permute-start | bytes 393224 | tf_op jit(solution)/shard_map/ppermute | solution.py:53
  41.9 6.1 %collective-permute-done.3.refs_3_ = bf16[2,2,64,256]{3,2,1,0:T(8,128)(2,1)S(1)} collective-permute-done((bf16[2,2,64,256]{3,2,1,0:T(8,128)(2,1)S(1)}, bf16[2,2,64,256]{3,2,1,0:T(8,128)(2,1)S(1)}, u32[]{:S(2)}, u32[]{:S(2)}) %collective-permute-start.3) | collective-permute-done | bytes 131104 | tf_op jit(solution)/shard_map/ppermute | solution.py:49
  48.0 0.0 collective-permute-start.5
  48.0 0.0 collective-permute-done.4.refs_4_
  48.0 3.2 %collective-permute-start.6 = (bf16[2,2,64,256]{3,2,1,0:T(8,128)(2,1)S(1)}, bf16[2,2,64,256]{3,2,1,0:T(8,128)(2,1)S(1)}, u32[]{:S(2)}, u32[]{:S(2)}) collective-permute-start(bf16[2,2,64,256]{3,2,1,0:T(8,128)(2,1)S(1)} %collective-permute-done.4.refs_4_), channel_id=1, source_target_pairs={{0,120},{4,124},{8,0},{12,4},{16,8},{20,12},{24,16},{28,20},{32,24... | collective-permute-start | bytes 393224 | tf_op jit(solution)/shard_map/ppermute | solution.py:53
  51.2 6.4 %collective-permute-done.5.refs_5_ = bf16[2,2,64,256]{3,2,1,0:T(8,128)(2,1)S(1)} collective-permute-done((bf16[2,2,64,256]{3,2,1,0:T(8,128)(2,1)S(1)}, bf16[2,2,64,256]{3,2,1,0:T(8,128)(2,1)S(1)}, u32[]{:S(2)}, u32[]{:S(2)}) %collective-permute-start.5) | collective-permute-done | bytes 131104 | tf_op jit(solution)/shard_map/ppermute | solution.py:49
  57.6 0.0 collective-permute-start.7
  57.6 0.0 collective-permute-done.6.refs_6_
  57.6 3.2 %collective-permute-start.8 = (bf16[2,2,64,256]{3,2,1,0:T(8,128)(2,1)S(1)}, bf16[2,2,64,256]{3,2,1,0:T(8,128)(2,1)S(1)}, u32[]{:S(2)}, u32[]{:S(2)}) collective-permute-start(bf16[2,2,64,256]{3,2,1,0:T(8,128)(2,1)S(1)} %collective-permute-done.6.refs_6_), channel_id=1, source_target_pairs={{0,120},{4,124},{8,0},{12,4},{16,8},{20,12},{24,16},{28,20},{32,24... | collective-permute-start | bytes 393224 | tf_op jit(solution)/shard_map/ppermute | solution.py:53
  60.8 6.2 %collective-permute-done.7.refs_7_ = bf16[2,2,64,256]{3,2,1,0:T(8,128)(2,1)S(1)} collective-permute-done((bf16[2,2,64,256]{3,2,1,0:T(8,128)(2,1)S(1)}, bf16[2,2,64,256]{3,2,1,0:T(8,128)(2,1)S(1)}, u32[]{:S(2)}, u32[]{:S(2)}) %collective-permute-start.7) | collective-permute-done | bytes 131104 | tf_op jit(solution)/shard_map/ppermute | solution.py:49
  67.0 0.0 collective-permute-start.9
  67.1 0.0 collective-permute-done.8.refs_8_
  67.1 3.2 %collective-permute-start.10 = (bf16[2,2,64,256]{3,2,1,0:T(8,128)(2,1)S(1)}, bf16[2,2,64,256]{3,2,1,0:T(8,128)(2,1)S(1)}, u32[]{:S(2)}, u32[]{:S(2)}) collective-permute-start(bf16[2,2,64,256]{3,2,1,0:T(8,128)(2,1)S(1)} %collective-permute-done.8.refs_8_), channel_id=1, source_target_pairs={{0,120},{4,124},{8,0},{12,4},{16,8},{20,12},{24,16},{28,20},{32,24... | collective-permute-start | bytes 393224 | tf_op jit(solution)/shard_map/ppermute | solution.py:53
  70.3 6.0 %collective-permute-done.9.refs_9_ = bf16[2,2,64,256]{3,2,1,0:T(8,128)(2,1)S(1)} collective-permute-done((bf16[2,2,64,256]{3,2,1,0:T(8,128)(2,1)S(1)}, bf16[2,2,64,256]{3,2,1,0:T(8,128)(2,1)S(1)}, u32[]{:S(2)}, u32[]{:S(2)}) %collective-permute-start.9) | collective-permute-done | bytes 131104 | tf_op jit(solution)/shard_map/ppermute | solution.py:49
  76.3 0.0 collective-permute-start.11
  76.3 3.2 %collective-permute-start.12 = (bf16[2,2,64,256]{3,2,1,0:T(8,128)(2,1)S(1)}, bf16[2,2,64,256]{3,2,1,0:T(8,128)(2,1)S(1)}, u32[]{:S(2)}, u32[]{:S(2)}) collective-permute-start(bf16[2,2,64,256]{3,2,1,0:T(8,128)(2,1)S(1)} %collective-permute-done.10.refs_10_), channel_id=1, source_target_pairs={{0,120},{4,124},{8,0},{12,4},{16,8},{20,12},{24,16},{28,20},{32,24... | collective-permute-start | bytes 393224 | tf_op jit(solution)/shard_map/ppermute | solution.py:53
  79.5 5.8 %collective-permute-done.11.refs_11_ = bf16[2,2,64,256]{3,2,1,0:T(8,128)(2,1)S(1)} collective-permute-done((bf16[2,2,64,256]{3,2,1,0:T(8,128)(2,1)S(1)}, bf16[2,2,64,256]{3,2,1,0:T(8,128)(2,1)S(1)}, u32[]{:S(2)}, u32[]{:S(2)}) %collective-permute-start.11) | collective-permute-done | bytes 131104 | tf_op jit(solution)/shard_map/ppermute | solution.py:49
  85.3 3.4 %collective-permute-start.14 = (bf16[2,2,64,256]{3,2,1,0:T(8,128)(2,1)S(1)}, bf16[2,2,64,256]{3,2,1,0:T(8,128)(2,1)S(1)}, u32[]{:S(2)}, u32[]{:S(2)}) collective-permute-start(bf16[2,2,64,256]{3,2,1,0:T(8,128)(2,1)S(1)} %collective-permute-done.12.refs_12_), channel_id=1, source_target_pairs={{0,120},{4,124},{8,0},{12,4},{16,8},{20,12},{24,16},{28,20},{32,24... | collective-permute-start | bytes 393224 | tf_op jit(solution)/shard_map/ppermute | solution.py:53
  88.8 6.0 %collective-permute-done.13.refs_13_ = bf16[2,2,64,256]{3,2,1,0:T(8,128)(2,1)S(1)} collective-permute-done((bf16[2,2,64,256]{3,2,1,0:T(8,128)(2,1)S(1)}, bf16[2,2,64,256]{3,2,1,0:T(8,128)(2,1)S(1)}, u32[]{:S(2)}, u32[]{:S(2)}) %collective-permute-start.13) | collective-permute-done | bytes 131104 | tf_op jit(solution)/shard_map/ppermute | solution.py:49
  94.8 0.0 collective-permute-start.15
  94.8 0.0 collective-permute-done.14.refs_14_
  94.8 9.1 %collective-permute-done.15.refs_15_ = bf16[2,2,64,256]{3,2,1,0:T(8,128)(2,1)S(1)} collective-permute-done((bf16[2,2,64,256]{3,2,1,0:T(8,128)(2,1)S(1)}, bf16[2,2,64,256]{3,2,1,0:T(8,128)(2,1)S(1)}, u32[]{:S(2)}, u32[]{:S(2)}) %collective-permute-start.15) | collective-permute-done | bytes 131104 | tf_op jit(solution)/shard_map/ppermute | solution.py:49
  103.9 0.1 stack.31.refs_0_
  104.0 0.1 collective-permute-start.17
  104.3 0.1 pad_maximum_fusion.2.lam_ref
  104.4 11.5 %all-gather.4.cloned.1.call-done.kv_ref = bf16[8192,640]{1,0:T(8,128)(2,1)} async-done(((bf16[256,640]{1,0:T(8,128)(2,1)}), bf16[8192,640]{1,0:T(8,128)(2,1)}) %all-gather.4.cloned.1.call-update) | async-done | bytes 10485776 | tf_op jit(solution)/shard_map/all_gather | solution.py:318
  115.9 4.0 %copy-done.3 = bf16[8192,640]{1,0:T(8,128)(2,1)S(1)} copy-done((bf16[8192,640]{1,0:T(8,128)(2,1)S(1)}, bf16[8192,640]{1,0:T(8,128)(2,1)}, u32[]{:S(2)}) %copy-start.3) | copy-done | bytes 10485784
  119.8 27.8 %attend.1 = bf16[256,512]{1,0:T(8,128)(2,1)S(1)} custom-call(bf16[256,256]{1,0:T(8,128)(2,1)S(1)} %bitcast.29, bf16[256,512]{1,0:T(8,128)(2,1)S(1)} %bitcast.28, bf16[8192,640]{1,0:T(8,128)(2,1)S(1)} %copy-done.3, f32[4]{0:T(128)S(1)} %pad_maximum_fusion.2.lam_ref, f32[1,128]{1,0:T(1,128)S(1)} %bitcast.30), custom_call_target="tpu_custom_call" | custom-call | flops 8589934592 | bytes 10485760 | tf_op jit(solution)/shard_map/attend/pallas_call | solution.py:142
  147.6 1.7 convolution_convert_fusion
  149.4 4.2 %all-to-all-start = ((bf16[4,64,2048]{2,1,0:T(8,128)(2,1)}), bf16[4,64,2048]{2,1,0:T(8,128)(2,1)S(1)}, u32[]{:S(2)}, u32[]{:S(2)}) async-start(bf16[4,64,2048]{2,1,0:T(8,128)(2,1)} %bitcast.35), calls=%async_computation | async-start | bytes 2097152 | tf_op jit(solution)/shard_map/all_to_all | solution.py:28
  153.6 0.5 collective-permute-start.18
  154.2 15.0 %all-to-all-done = bf16[4,64,2048]{2,1,0:T(8,128)(2,1)S(1)} async-done(((bf16[4,64,2048]{2,1,0:T(8,128)(2,1)}), bf16[4,64,2048]{2,1,0:T(8,128)(2,1)S(1)}, u32[]{:S(2)}, u32[]{:S(2)}) %all-to-all-start) | async-done | bytes 1048608 | tf_op jit(solution)/shard_map/all_to_all | solution.py:28
  169.1 0.2 convert_reduce_fusion.1
  169.3 0.2 fusion.3
  169.5 0.1 fusion.5
  169.6 1.1 broadcast_in_dim.2
  170.8 3.6 %all-to-all-start.1 = ((bf16[4,64,2048]{2,1,0:T(8,128)(2,1)}), bf16[4,64,2048]{2,1,0:T(8,128)(2,1)S(1)}, u32[]{:S(2)}, u32[]{:S(2)}) async-start(bf16[4,64,2048]{2,1,0:T(8,128)(2,1)} %broadcast_in_dim.2), calls=%async_computation.1 | async-start | bytes 2097152 | tf_op jit(solution)/shard_map/all_to_all | solution.py:38
  174.4 0.0 collective-permute-done.16.refs_1_
  174.4 14.5 %all-to-all-done.1 = bf16[4,64,2048]{2,1,0:T(8,128)(2,1)S(1)} async-done(((bf16[4,64,2048]{2,1,0:T(8,128)(2,1)}), bf16[4,64,2048]{2,1,0:T(8,128)(2,1)S(1)}, u32[]{:S(2)}, u32[]{:S(2)}) %all-to-all-start.1) | async-done | bytes 1048608 | tf_op jit(solution)/shard_map/all_to_all | solution.py:38
  188.9 7.8 %early_mixer.1.early_ref = f32[256,2048]{1,0:T(8,128)S(1)} custom-call(s32[1]{0:T(128)} %bitcast.13.chip_ref, bf16[256,2048]{1,0:T(8,128)(2,1)S(1)} %bitcast.24, bf16[16,2,2,64,256]{4,3,2,1,0:T(8,128)(2,1)S(1)} %stack.31.refs_0_, bf16[16,2,2,64,256]{4,3,2,1,0:T(8,128)(2,1)} %collective-permute-done.16.refs_1_, ...), custom_call_target="tpu_custom_call" | custom-call | flops 2147483648 | bytes 8388608 | tf_op jit(solution)/shard_map/early_mixer/pallas_call | solution.py:210
  196.8 1.3 copy-done.1
  198.1 3.4 %copy-done = bf16[64,64,1024]{2,1,0:T(8,128)(2,1)S(1)} copy-done((bf16[64,64,1024]{2,1,0:T(8,128)(2,1)S(1)}, bf16[64,64,1024]{2,1,0:T(8,128)(2,1)}, u32[]{:S(2)}) %copy-start) | copy-done | bytes 8388632
  201.5 1.6 copy-done.2
  203.1 5.7 %mixer.1 = bf16[256,2048]{1,0:T(8,128)(2,1)S(1)} custom-call(bf16[256,2048]{1,0:T(8,128)(2,1)S(1)} %bitcast.25, bf16[32,2,64,1024]{3,2,1,0:T(8,128)(2,1)S(1)} %bitcast.26, f32[256,2048]{1,0:T(8,128)S(1)} %copy-done.2), custom_call_target="tpu_custom_call" | custom-call | flops 2147483648 | bytes 8388608 | tf_op jit(solution)/shard_map/mixer/pallas_call | solution.py:269
  208.8 16.2 %all_to_all.15 = bf16[4,64,2048]{2,1,0:T(8,128)(2,1)S(1)} all-to-all(bf16[4,64,2048]{2,1,0:T(8,128)(2,1)S(1)} %bitcast.27), channel_id=1, replica_groups=mesh['grp'=2,'sp'=32,'tp'=4] {'tp'}, dimensions={0} | all-to-all | bytes 2097152 | tf_op jit(solution)/shard_map/all_to_all | solution.py:28
  225.0 0.2 convert_reduce_fusion
  225.2 0.8 fusion.6
  (35 shorter events, 0.2 us)
Async XLA Ops:
  6.5 3.7 %copy-start.6 = (bf16[64,2048]{1,0:T(8,128)(2,1)S(1)}, bf16[64,2048]{1,0:T(8,128)(2,1)}, u32[]{:S(2)}) copy-start(bf16[64,2048]{1,0:T(8,128)(2,1)} %param.28) | copy-start | bytes 786436
  6.5 3.7 %copy-start.5 = (bf16[2048,64]{0,1:T(8,128)(2,1)S(1)}, bf16[2048,64]{0,1:T(8,128)(2,1)}, u32[]{:S(2)}) copy-start(bf16[2048,64]{0,1:T(8,128)(2,1)} %param.29) | copy-start | bytes 786436
  6.6 109.3 %all-gather.4.cloned.1.call-start = ((), (), s32[]{:S(2)}) async-start(), calls=%async_computation.3 | async-start | bytes 10813440 | tf_op jit(solution)/shard_map/all_gather | solution.py:318
  8.4 189.7 %all-gather.6.cloned.1.call-start = ((), (), s32[]{:S(2)}) async-start(), calls=%async_computation.4 | async-start | bytes 8650752 | tf_op jit(solution)/shard_map/all_gather | solution.py:323
  10.3 1.4 collective-permute-start
  11.7 92.5 %copy-start.7 = (bf16[256,2,256]{2,1,0:T(2,128)(2,1)S(1)}, bf16[256,2,256]{2,1,0:T(2,128)(2,1)}, u32[]{:S(2)}) copy-start(bf16[256,2,256]{2,1,0:T(2,128)(2,1)} %param.19) | copy-start | bytes 786436
  11.7 92.5 %copy-start.9 = (bf16[256,2,128]{2,1,0:T(2,128)(2,1)S(1)}, bf16[256,2,128]{2,1,0:T(2,128)(2,1)}, u32[]{:S(2)}) copy-start(bf16[256,2,128]{2,1,0:T(2,128)(2,1)} %param.16) | copy-start | bytes 393220
  11.7 92.5 %copy-start.13 = (f32[2]{0:T(128)S(1)}, f32[2]{0:T(128)}, u32[]{:S(2)}) copy-start(f32[2]{0:T(128)} %param.23) | copy-start | bytes 28
  11.8 92.5 %copy-start.14 = (f32[2]{0:T(128)S(1)}, f32[2]{0:T(128)}, u32[]{:S(2)}) copy-start(f32[2]{0:T(128)} %param.22) | copy-start | bytes 28
  11.8 104.1 %copy-start.4 = (f32[128]{0:T(128)S(1)}, f32[128]{0:T(128)}, u32[]{:S(2)}) copy-start(f32[128]{0:T(128)} %param.24) | copy-start | bytes 1540
  11.8 26.3 %collective-permute-start.1 = (bf16[2,2,64,256]{3,2,1,0:T(8,128)(2,1)S(1)}, bf16[2,2,64,256]{3,2,1,0:T(8,128)(2,1)S(1)}, u32[]{:S(2)}, u32[]{:S(2)}) collective-permute-start(bf16[2,2,64,256]{3,2,1,0:T(8,128)(2,1)S(1)} %maximum_select_fusion.refs_0_), channel_id=1, source_target_pairs={{0,8},{4,12},{8,16},{12,20},{16,24},{20,28},{24,32},{28,36},{32,40... | collective-permute-start | bytes 393224 | tf_op jit(solution)/shard_map/ppermute | solution.py:49
  14.7 23.5 %collective-permute-start.2 = (bf16[2,2,64,256]{3,2,1,0:T(8,128)(2,1)S(1)}, bf16[2,2,64,256]{3,2,1,0:T(8,128)(2,1)S(1)}, u32[]{:S(2)}, u32[]{:S(2)}) collective-permute-start(bf16[2,2,64,256]{3,2,1,0:T(8,128)(2,1)S(1)} %maximum_select_fusion.refs_0_), channel_id=1, source_target_pairs={{0,120},{4,124},{8,0},{12,4},{16,8},{20,12},{24,16},{28,20},{32,24... | collective-permute-start | bytes 393224 | tf_op jit(solution)/shard_map/ppermute | solution.py:53
  38.1 9.9 %collective-permute-start.3 = (bf16[2,2,64,256]{3,2,1,0:T(8,128)(2,1)S(1)}, bf16[2,2,64,256]{3,2,1,0:T(8,128)(2,1)S(1)}, u32[]{:S(2)}, u32[]{:S(2)}) collective-permute-start(bf16[2,2,64,256]{3,2,1,0:T(8,128)(2,1)S(1)} %collective-permute-done.1.refs_1_), channel_id=1, source_target_pairs={{0,8},{4,12},{8,16},{12,20},{16,24},{20,28},{24,32},{28,36},{32,40... | collective-permute-start | bytes 393224 | tf_op jit(solution)/shard_map/ppermute | solution.py:49
  38.2 9.8 %collective-permute-start.4 = (bf16[2,2,64,256]{3,2,1,0:T(8,128)(2,1)S(1)}, bf16[2,2,64,256]{3,2,1,0:T(8,128)(2,1)S(1)}, u32[]{:S(2)}, u32[]{:S(2)}) collective-permute-start(bf16[2,2,64,256]{3,2,1,0:T(8,128)(2,1)S(1)} %collective-permute-done.2.refs_2_), channel_id=1, source_target_pairs={{0,120},{4,124},{8,0},{12,4},{16,8},{20,12},{24,16},{28,20},{32,24... | collective-permute-start | bytes 393224 | tf_op jit(solution)/shard_map/ppermute | solution.py:53
  48.0 9.6 %collective-permute-start.5 = (bf16[2,2,64,256]{3,2,1,0:T(8,128)(2,1)S(1)}, bf16[2,2,64,256]{3,2,1,0:T(8,128)(2,1)S(1)}, u32[]{:S(2)}, u32[]{:S(2)}) collective-permute-start(bf16[2,2,64,256]{3,2,1,0:T(8,128)(2,1)S(1)} %collective-permute-done.3.refs_3_), channel_id=1, source_target_pairs={{0,8},{4,12},{8,16},{12,20},{16,24},{20,28},{24,32},{28,36},{32,40... | collective-permute-start | bytes 393224 | tf_op jit(solution)/shard_map/ppermute | solution.py:49
  48.0 9.6 %collective-permute-start.6 = (bf16[2,2,64,256]{3,2,1,0:T(8,128)(2,1)S(1)}, bf16[2,2,64,256]{3,2,1,0:T(8,128)(2,1)S(1)}, u32[]{:S(2)}, u32[]{:S(2)}) collective-permute-start(bf16[2,2,64,256]{3,2,1,0:T(8,128)(2,1)S(1)} %collective-permute-done.4.refs_4_), channel_id=1, source_target_pairs={{0,120},{4,124},{8,0},{12,4},{16,8},{20,12},{24,16},{28,20},{32,24... | collective-permute-start | bytes 393224 | tf_op jit(solution)/shard_map/ppermute | solution.py:53
  57.6 9.4 %collective-permute-start.7 = (bf16[2,2,64,256]{3,2,1,0:T(8,128)(2,1)S(1)}, bf16[2,2,64,256]{3,2,1,0:T(8,128)(2,1)S(1)}, u32[]{:S(2)}, u32[]{:S(2)}) collective-permute-start(bf16[2,2,64,256]{3,2,1,0:T(8,128)(2,1)S(1)} %collective-permute-done.5.refs_5_), channel_id=1, source_target_pairs={{0,8},{4,12},{8,16},{12,20},{16,24},{20,28},{24,32},{28,36},{32,40... | collective-permute-start | bytes 393224 | tf_op jit(solution)/shard_map/ppermute | solution.py:49
  57.6 9.4 %collective-permute-start.8 = (bf16[2,2,64,256]{3,2,1,0:T(8,128)(2,1)S(1)}, bf16[2,2,64,256]{3,2,1,0:T(8,128)(2,1)S(1)}, u32[]{:S(2)}, u32[]{:S(2)}) collective-permute-start(bf16[2,2,64,256]{3,2,1,0:T(8,128)(2,1)S(1)} %collective-permute-done.6.refs_6_), channel_id=1, source_target_pairs={{0,120},{4,124},{8,0},{12,4},{16,8},{20,12},{24,16},{28,20},{32,24... | collective-permute-start | bytes 393224 | tf_op jit(solution)/shard_map/ppermute | solution.py:53
  67.0 9.2 %collective-permute-start.9 = (bf16[2,2,64,256]{3,2,1,0:T(8,128)(2,1)S(1)}, bf16[2,2,64,256]{3,2,1,0:T(8,128)(2,1)S(1)}, u32[]{:S(2)}, u32[]{:S(2)}) collective-permute-start(bf16[2,2,64,256]{3,2,1,0:T(8,128)(2,1)S(1)} %collective-permute-done.7.refs_7_), channel_id=1, source_target_pairs={{0,8},{4,12},{8,16},{12,20},{16,24},{20,28},{24,32},{28,36},{32,40... | collective-permute-start | bytes 393224 | tf_op jit(solution)/shard_map/ppermute | solution.py:49
  67.1 9.2 %collective-permute-start.10 = (bf16[2,2,64,256]{3,2,1,0:T(8,128)(2,1)S(1)}, bf16[2,2,64,256]{3,2,1,0:T(8,128)(2,1)S(1)}, u32[]{:S(2)}, u32[]{:S(2)}) collective-permute-start(bf16[2,2,64,256]{3,2,1,0:T(8,128)(2,1)S(1)} %collective-permute-done.8.refs_8_), channel_id=1, source_target_pairs={{0,120},{4,124},{8,0},{12,4},{16,8},{20,12},{24,16},{28,20},{32,24... | collective-permute-start | bytes 393224 | tf_op jit(solution)/shard_map/ppermute | solution.py:53
  76.3 9.1 %collective-permute-start.11 = (bf16[2,2,64,256]{3,2,1,0:T(8,128)(2,1)S(1)}, bf16[2,2,64,256]{3,2,1,0:T(8,128)(2,1)S(1)}, u32[]{:S(2)}, u32[]{:S(2)}) collective-permute-start(bf16[2,2,64,256]{3,2,1,0:T(8,128)(2,1)S(1)} %collective-permute-done.9.refs_9_), channel_id=1, source_target_pairs={{0,8},{4,12},{8,16},{12,20},{16,24},{20,28},{24,32},{28,36},{32,40... | collective-permute-start | bytes 393224 | tf_op jit(solution)/shard_map/ppermute | solution.py:49
  76.3 9.1 %collective-permute-start.12 = (bf16[2,2,64,256]{3,2,1,0:T(8,128)(2,1)S(1)}, bf16[2,2,64,256]{3,2,1,0:T(8,128)(2,1)S(1)}, u32[]{:S(2)}, u32[]{:S(2)}) collective-permute-start(bf16[2,2,64,256]{3,2,1,0:T(8,128)(2,1)S(1)} %collective-permute-done.10.refs_10_), channel_id=1, source_target_pairs={{0,120},{4,124},{8,0},{12,4},{16,8},{20,12},{24,16},{28,20},{32,24... | collective-permute-start | bytes 393224 | tf_op jit(solution)/shard_map/ppermute | solution.py:53
  85.3 9.4 %collective-permute-start.13 = (bf16[2,2,64,256]{3,2,1,0:T(8,128)(2,1)S(1)}, bf16[2,2,64,256]{3,2,1,0:T(8,128)(2,1)S(1)}, u32[]{:S(2)}, u32[]{:S(2)}) collective-permute-start(bf16[2,2,64,256]{3,2,1,0:T(8,128)(2,1)S(1)} %collective-permute-done.11.refs_11_), channel_id=1, source_target_pairs={{0,8},{4,12},{8,16},{12,20},{16,24},{20,28},{24,32},{28,36},{32,40... | collective-permute-start | bytes 393224 | tf_op jit(solution)/shard_map/ppermute | solution.py:49
  85.3 9.4 %collective-permute-start.14 = (bf16[2,2,64,256]{3,2,1,0:T(8,128)(2,1)S(1)}, bf16[2,2,64,256]{3,2,1,0:T(8,128)(2,1)S(1)}, u32[]{:S(2)}, u32[]{:S(2)}) collective-permute-start(bf16[2,2,64,256]{3,2,1,0:T(8,128)(2,1)S(1)} %collective-permute-done.12.refs_12_), channel_id=1, source_target_pairs={{0,120},{4,124},{8,0},{12,4},{16,8},{20,12},{24,16},{28,20},{32,24... | collective-permute-start | bytes 393224 | tf_op jit(solution)/shard_map/ppermute | solution.py:53
  94.8 9.1 %collective-permute-start.15 = (bf16[2,2,64,256]{3,2,1,0:T(8,128)(2,1)S(1)}, bf16[2,2,64,256]{3,2,1,0:T(8,128)(2,1)S(1)}, u32[]{:S(2)}, u32[]{:S(2)}) collective-permute-start(bf16[2,2,64,256]{3,2,1,0:T(8,128)(2,1)S(1)} %collective-permute-done.13.refs_13_), channel_id=1, source_target_pairs={{0,8},{4,12},{8,16},{12,20},{16,24},{20,28},{24,32},{28,36},{32,40... | collective-permute-start | bytes 393224 | tf_op jit(solution)/shard_map/ppermute | solution.py:49
  104.0 49.6 %collective-permute-start.17 = (bf16[16,2,2,64,256]{4,3,2,1,0:T(8,128)(2,1)S(1)}, bf16[16,2,2,64,256]{4,3,2,1,0:T(8,128)(2,1)}, u32[]{:S(2)}, u32[]{:S(2)}) collective-permute-start(bf16[16,2,2,64,256]{4,3,2,1,0:T(8,128)(2,1)S(1)} %stack.31.refs_0_), channel_id=1, source_target_pairs={{0,128},{128,0},{1,129},{129,1},{2,130},{130,2},{3,131},{131,3},{4... | collective-permute-start | bytes 6291464 | tf_op jit(solution)/shard_map/ppermute | solution.py:331
  115.9 4.0 %copy-start.3 = (bf16[8192,640]{1,0:T(8,128)(2,1)S(1)}, bf16[8192,640]{1,0:T(8,128)(2,1)}, u32[]{:S(2)}) copy-start(bf16[8192,640]{1,0:T(8,128)(2,1)} %all-gather.4.cloned.1.call-done.kv_ref) | copy-start | bytes 31457284
  119.8 27.8 %copy-start.11 = (bf16[256,2048]{1,0:T(8,128)(2,1)S(1)}, bf16[256,2048]{1,0:T(8,128)(2,1)}, u32[]{:S(2)}) copy-start(bf16[256,2048]{1,0:T(8,128)(2,1)} %param.26) | copy-start | bytes 3145732
  119.8 27.8 %copy-start.12 = (bf16[256,2048]{1,0:T(8,128)(2,1)S(1)}, bf16[256,2048]{1,0:T(8,128)(2,1)}, u32[]{:S(2)}) copy-start(bf16[256,2048]{1,0:T(8,128)(2,1)} %param.25) | copy-start | bytes 3145732
  149.4 4.8 %copy-start.10 = (bf16[2048]{0:T(1024)(128)(2,1)S(1)}, bf16[2048]{0:T(1024)(128)(2,1)}, u32[]{:S(2)}) copy-start(bf16[2048]{0:T(1024)(128)(2,1)} %param.27) | copy-start | bytes 12292
  149.4 19.9 %copy-start.8 = (bf16[64,2048]{1,0:T(8,128)(2,1)S(1)}, bf16[64,2048]{1,0:T(8,128)(2,1)}, u32[]{:S(2)}) copy-start(bf16[64,2048]{1,0:T(8,128)(2,1)} %param.15) | copy-start | bytes 786436
  149.4 19.7 %all-to-all-start = ((bf16[4,64,2048]{2,1,0:T(8,128)(2,1)}), bf16[4,64,2048]{2,1,0:T(8,128)(2,1)S(1)}, u32[]{:S(2)}, u32[]{:S(2)}) async-start(bf16[4,64,2048]{2,1,0:T(8,128)(2,1)} %bitcast.35), calls=%async_computation | async-start | bytes 2097152 | tf_op jit(solution)/shard_map/all_to_all | solution.py:28
  153.6 20.8 %collective-permute-start.16 = (bf16[16,2,2,64,256]{4,3,2,1,0:T(8,128)(2,1)S(1)}, bf16[16,2,2,64,256]{4,3,2,1,0:T(8,128)(2,1)}, u32[]{:S(2)}, u32[]{:S(2)}) collective-permute-start(bf16[16,2,2,64,256]{4,3,2,1,0:T(8,128)(2,1)S(1)} %stack.31.refs_0_), channel_id=1, source_target_pairs={{0,4},{4,0},{8,12},{12,8},{16,20},{20,16},{24,28},{28,24},{32,36},... | collective-permute-start | bytes 6291464 | tf_op jit(solution)/shard_map/ppermute | solution.py:332
  153.6 20.8 %collective-permute-start.18 = (bf16[16,2,2,64,256]{4,3,2,1,0:T(8,128)(2,1)}, bf16[16,2,2,64,256]{4,3,2,1,0:T(8,128)(2,1)}, u32[]{:S(2)}, u32[]{:S(2)}) collective-permute-start(bf16[16,2,2,64,256]{4,3,2,1,0:T(8,128)(2,1)} %collective-permute-done.17.refs_2_), channel_id=1, source_target_pairs={{0,4},{4,0},{8,12},{12,8},{16,20},{20,16},{24,28},{28,24},{32,36},... | collective-permute-start | bytes 6291464 | tf_op jit(solution)/shard_map/ppermute | solution.py:333
  170.8 18.2 %all-to-all-start.1 = ((bf16[4,64,2048]{2,1,0:T(8,128)(2,1)}), bf16[4,64,2048]{2,1,0:T(8,128)(2,1)S(1)}, u32[]{:S(2)}, u32[]{:S(2)}) async-start(bf16[4,64,2048]{2,1,0:T(8,128)(2,1)} %broadcast_in_dim.2), calls=%async_computation.1 | async-start | bytes 2097152 | tf_op jit(solution)/shard_map/all_to_all | solution.py:38
  196.7 1.4 copy-start.1
  198.1 3.4 %copy-start = (bf16[64,64,1024]{2,1,0:T(8,128)(2,1)S(1)}, bf16[64,64,1024]{2,1,0:T(8,128)(2,1)}, u32[]{:S(2)}) copy-start(bf16[64,64,1024]{2,1,0:T(8,128)(2,1)} %all-gather.6.cloned.1.call-done) | copy-start | bytes 25165828
  201.5 1.6 copy-start.2
Sparse Core Ops, SparseCore 0:
  9.2 106.6 all-gather.3
  117.7 72.4 all-gather.5

commit v3 on v2

--- a/solution.py
+++ b/solution.py
@@ -13,7 +13,7 @@
 OUT_SCALE = 0.8
 LOG2E = math.log2(math.e)
 LAST_DIMS = (((1,), (1,)), ((), ()))
-VMEM_LIMIT = 28 * 2**20
+VMEM_LIMIT = 58 * 2**20
 EARLY = 8
 BATCHES = ()
 
@@ -140,8 +140,8 @@
     block = math.gcd(keys, 2048)
     steps = keys // block
     return pl.pallas_call(
-        functools.partial(attend_kernel, dn=dn, dw=dw, dv=dv, steps=steps, parts=2),
-        grid=(steps, 2),
+        functools.partial(attend_kernel, dn=dn, dw=dw, dv=dv, steps=steps, parts=1),
+        grid=(steps, 1),
         in_specs=[
             pl.BlockSpec(qn.shape, lambda i, j: (0, 0)),
             pl.BlockSpec(qw.shape, lambda i, j: (0, 0)),
@@ -222,7 +222,7 @@
             pltpu.VMEM((rows // 2, d), jnp.float32),
         ],
         compiler_params=pltpu.CompilerParams(
-            dimension_semantics=("arbitrary",), vmem_limit_bytes=30 * 2**20
+            dimension_semantics=("arbitrary",), vmem_limit_bytes=50 * 2**20
         ),
         cost_estimate=pl.CostEstimate(
             flops=4 * rows * d * hidden, bytes_accessed=4 * d * hidden, transcendentals=0
@@ -281,7 +281,7 @@
             pltpu.VMEM((rows, hidden), jnp.bfloat16),
         ],
         compiler_params=pltpu.CompilerParams(
-            dimension_semantics=("arbitrary",), vmem_limit_bytes=20 * 2**20
+            dimension_semantics=("arbitrary",), vmem_limit_bytes=50 * 2**20
         ),
         cost_estimate=pl.CostEstimate(
             flops=4 * rows * d * hidden, bytes_accessed=4 * d * hidden, transcendentals=0

time: 233 us -> 228 us (0.979)
  local copies, waits for them, and re-layouts: 11.6 us -> 4.18 us
  Pallas kernels: 41.4 us -> 44.2 us
  waiting for transfers between devices: 91.7 us -> 89.3 us
    unnamed x32 -> x26, local copies, waits for them, and re-layouts: 10.4 us -> 3.02 us
    pallas_call x1, Pallas kernels: 5.72 us -> 8.76 us  [mixer(): pl.pallas_call(functools.partial(mixer_kernel, half=half), grid=(2 * half...]
  transfers between devices with their start and end apart: 23 -> 23, of which waited for: 13 -> 13; matrix products, arithmetic and copies ran while one was open for 2% -> 4% of each run, Pallas kernels for 15% -> 16%
where the time goes in v3:
time: 228 us; the launch traced here: 227 us
  waiting for transfers between devices  89.3 us (39%)
  starting transfers between devices  51.6 us (23%)
  Pallas kernels  44.2 us (19%)
  blocking collectives  16.1 us (7%)
  between operations  13.7 us (6%)
  other arithmetic  5.59 us (2%)
  local copies, waits for them, and re-layouts  4.18 us (2%)
  matrix products  2.71 us (1%)
    ppermute x8, waiting for transfers between devices, ring(): ahead = lax.ppermute(ahead, 'sp', onward)  49.3 us
    ppermute x7, starting transfers between devices, ring(): behind = lax.ppermute(behind, 'sp', backward)  39.8 us
    pallas_call x1, Pallas kernels, attention(): pl.pallas_call(functools.partial(attend_kernel, dn=dn, dw=dw, dv=dv, step...  26.9 us
    all_to_all x1, blocking collectives, sent_and_summed(): parts = lax.all_to_all(split_up(array, dim, peers), axis, 0, 0, tiled=True)  16.1 us
    all_to_all x1, waiting for transfers between devices, sent_and_summed(): parts = lax.all_to_all(split_up(array, dim, peers), axis, 0, 0, tiled=True)  15 us
    all_to_all x1, waiting for transfers between devices, copy_for_each(): return lax.all_to_all(copies, axis, split_axis=0, concat_axis=0, tiled=True)  14.3 us
    all_gather x1, waiting for transfers between devices, shards(): kv = lax.all_gather(own, 'sp', axis=0, tiled=True)  9.38 us
    pallas_call x1, Pallas kernels, mixer(): pl.pallas_call(functools.partial(mixer_kernel, half=half), grid=(2 * half...  8.76 us
  transfers between devices with their start and end apart: 23, of which 13 were waited for; matrix products, arithmetic and copies ran while one was open for 4% of the time, Pallas kernels for 16%

profile of v3, /device:TPU:40, one launch (start us, length us, event | category | flops | bytes accessed | tf_op | source)
XLA Modules:
  0.0 227.5 jit_solution(14319529133528121892)
XLA Ops:
  6.6 1.8 pad_maximum_fusion
  8.3 0.1 all-gather.4.cloned.1.call-update
  8.4 0.1 all-gather.6.cloned.1.call-start
  8.5 1.7 pad_maximum_fusion.1
  10.2 0.1 all-gather.6.cloned.1.call-update
  10.3 0.1 collective-permute-start
  10.5 1.2 collective-permute-done
  11.7 0.0 copy-start.4
  11.7 0.0 copy-start.6
  11.7 0.0 copy-start.10
  11.8 0.0 copy-start.11
  11.8 2.9 %collective-permute-start.1 = (bf16[2,2,64,256]{3,2,1,0:T(8,128)(2,1)S(1)}, bf16[2,2,64,256]{3,2,1,0:T(8,128)(2,1)S(1)}, u32[]{:S(2)}, u32[]{:S(2)}) collective-permute-start(bf16[2,2,64,256]{3,2,1,0:T(8,128)(2,1)S(1)} %maximum_select_fusion.refs_0_), channel_id=1, source_target_pairs={{0,8},{4,12},{8,16},{12,20},{16,24},{20,28},{24,32},{28,36},{32,40... | collective-permute-start | bytes 393224 | tf_op jit(solution)/shard_map/ppermute | solution.py:49
  14.7 19.7 %collective-permute-start.2 = (bf16[2,2,64,256]{3,2,1,0:T(8,128)(2,1)S(1)}, bf16[2,2,64,256]{3,2,1,0:T(8,128)(2,1)S(1)}, u32[]{:S(2)}, u32[]{:S(2)}) collective-permute-start(bf16[2,2,64,256]{3,2,1,0:T(8,128)(2,1)S(1)} %maximum_select_fusion.refs_0_), channel_id=1, source_target_pairs={{0,120},{4,124},{8,0},{12,4},{16,8},{20,12},{24,16},{28,20},{32,24... | collective-permute-start | bytes 393224 | tf_op jit(solution)/shard_map/ppermute | solution.py:53
  34.4 3.7 %collective-permute-done.1.refs_1_ = bf16[2,2,64,256]{3,2,1,0:T(8,128)(2,1)S(1)} collective-permute-done((bf16[2,2,64,256]{3,2,1,0:T(8,128)(2,1)S(1)}, bf16[2,2,64,256]{3,2,1,0:T(8,128)(2,1)S(1)}, u32[]{:S(2)}, u32[]{:S(2)}) %collective-permute-start.1) | collective-permute-done | bytes 131104 | tf_op jit(solution)/shard_map/ppermute | solution.py:49
  38.1 0.0 collective-permute-start.3
  38.1 0.1 collective-permute-done.2.refs_2_
  38.2 3.7 %collective-permute-start.4 = (bf16[2,2,64,256]{3,2,1,0:T(8,128)(2,1)S(1)}, bf16[2,2,64,256]{3,2,1,0:T(8,128)(2,1)S(1)}, u32[]{:S(2)}, u32[]{:S(2)}) collective-permute-start(bf16[2,2,64,256]{3,2,1,0:T(8,128)(2,1)S(1)} %collective-permute-done.2.refs_2_), channel_id=1, source_target_pairs={{0,120},{4,124},{8,0},{12,4},{16,8},{20,12},{24,16},{28,20},{32,24... | collective-permute-start | bytes 393224 | tf_op jit(solution)/shard_map/ppermute | solution.py:53
  41.9 6.1 %collective-permute-done.3.refs_3_ = bf16[2,2,64,256]{3,2,1,0:T(8,128)(2,1)S(1)} collective-permute-done((bf16[2,2,64,256]{3,2,1,0:T(8,128)(2,1)S(1)}, bf16[2,2,64,256]{3,2,1,0:T(8,128)(2,1)S(1)}, u32[]{:S(2)}, u32[]{:S(2)}) %collective-permute-start.3) | collective-permute-done | bytes 131104 | tf_op jit(solution)/shard_map/ppermute | solution.py:49
  47.9 0.0 collective-permute-start.5
  47.9 0.0 collective-permute-done.4.refs_4_
  48.0 3.2 %collective-permute-start.6 = (bf16[2,2,64,256]{3,2,1,0:T(8,128)(2,1)S(1)}, bf16[2,2,64,256]{3,2,1,0:T(8,128)(2,1)S(1)}, u32[]{:S(2)}, u32[]{:S(2)}) collective-permute-start(bf16[2,2,64,256]{3,2,1,0:T(8,128)(2,1)S(1)} %collective-permute-done.4.refs_4_), channel_id=1, source_target_pairs={{0,120},{4,124},{8,0},{12,4},{16,8},{20,12},{24,16},{28,20},{32,24... | collective-permute-start | bytes 393224 | tf_op jit(solution)/shard_map/ppermute | solution.py:53
  51.2 6.4 %collective-permute-done.5.refs_5_ = bf16[2,2,64,256]{3,2,1,0:T(8,128)(2,1)S(1)} collective-permute-done((bf16[2,2,64,256]{3,2,1,0:T(8,128)(2,1)S(1)}, bf16[2,2,64,256]{3,2,1,0:T(8,128)(2,1)S(1)}, u32[]{:S(2)}, u32[]{:S(2)}) %collective-permute-start.5) | collective-permute-done | bytes 131104 | tf_op jit(solution)/shard_map/ppermute | solution.py:49
  57.6 0.0 collective-permute-start.7
  57.6 0.0 collective-permute-done.6.refs_6_
  57.6 3.2 %collective-permute-start.8 = (bf16[2,2,64,256]{3,2,1,0:T(8,128)(2,1)S(1)}, bf16[2,2,64,256]{3,2,1,0:T(8,128)(2,1)S(1)}, u32[]{:S(2)}, u32[]{:S(2)}) collective-permute-start(bf16[2,2,64,256]{3,2,1,0:T(8,128)(2,1)S(1)} %collective-permute-done.6.refs_6_), channel_id=1, source_target_pairs={{0,120},{4,124},{8,0},{12,4},{16,8},{20,12},{24,16},{28,20},{32,24... | collective-permute-start | bytes 393224 | tf_op jit(solution)/shard_map/ppermute | solution.py:53
  60.8 6.2 %collective-permute-done.7.refs_7_ = bf16[2,2,64,256]{3,2,1,0:T(8,128)(2,1)S(1)} collective-permute-done((bf16[2,2,64,256]{3,2,1,0:T(8,128)(2,1)S(1)}, bf16[2,2,64,256]{3,2,1,0:T(8,128)(2,1)S(1)}, u32[]{:S(2)}, u32[]{:S(2)}) %collective-permute-start.7) | collective-permute-done | bytes 131104 | tf_op jit(solution)/shard_map/ppermute | solution.py:49
  67.0 0.0 collective-permute-start.9
  67.0 0.0 collective-permute-done.8.refs_8_
  67.0 3.2 %collective-permute-start.10 = (bf16[2,2,64,256]{3,2,1,0:T(8,128)(2,1)S(1)}, bf16[2,2,64,256]{3,2,1,0:T(8,128)(2,1)S(1)}, u32[]{:S(2)}, u32[]{:S(2)}) collective-permute-start(bf16[2,2,64,256]{3,2,1,0:T(8,128)(2,1)S(1)} %collective-permute-done.8.refs_8_), channel_id=1, source_target_pairs={{0,120},{4,124},{8,0},{12,4},{16,8},{20,12},{24,16},{28,20},{32,24... | collective-permute-start | bytes 393224 | tf_op jit(solution)/shard_map/ppermute | solution.py:53
  70.3 6.0 %collective-permute-done.9.refs_9_ = bf16[2,2,64,256]{3,2,1,0:T(8,128)(2,1)S(1)} collective-permute-done((bf16[2,2,64,256]{3,2,1,0:T(8,128)(2,1)S(1)}, bf16[2,2,64,256]{3,2,1,0:T(8,128)(2,1)S(1)}, u32[]{:S(2)}, u32[]{:S(2)}) %collective-permute-start.9) | collective-permute-done | bytes 131104 | tf_op jit(solution)/shard_map/ppermute | solution.py:49
  76.3 0.0 collective-permute-start.11
  76.3 3.2 %collective-permute-start.12 = (bf16[2,2,64,256]{3,2,1,0:T(8,128)(2,1)S(1)}, bf16[2,2,64,256]{3,2,1,0:T(8,128)(2,1)S(1)}, u32[]{:S(2)}, u32[]{:S(2)}) collective-permute-start(bf16[2,2,64,256]{3,2,1,0:T(8,128)(2,1)S(1)} %collective-permute-done.10.refs_10_), channel_id=1, source_target_pairs={{0,120},{4,124},{8,0},{12,4},{16,8},{20,12},{24,16},{28,20},{32,24... | collective-permute-start | bytes 393224 | tf_op jit(solution)/shard_map/ppermute | solution.py:53
  79.5 5.8 %collective-permute-done.11.refs_11_ = bf16[2,2,64,256]{3,2,1,0:T(8,128)(2,1)S(1)} collective-permute-done((bf16[2,2,64,256]{3,2,1,0:T(8,128)(2,1)S(1)}, bf16[2,2,64,256]{3,2,1,0:T(8,128)(2,1)S(1)}, u32[]{:S(2)}, u32[]{:S(2)}) %collective-permute-start.11) | collective-permute-done | bytes 131104 | tf_op jit(solution)/shard_map/ppermute | solution.py:49
  85.3 0.0 collective-permute-start.13
  85.3 0.0 collective-permute-done.12.refs_12_
  85.3 3.4 %collective-permute-start.14 = (bf16[2,2,64,256]{3,2,1,0:T(8,128)(2,1)S(1)}, bf16[2,2,64,256]{3,2,1,0:T(8,128)(2,1)S(1)}, u32[]{:S(2)}, u32[]{:S(2)}) collective-permute-start(bf16[2,2,64,256]{3,2,1,0:T(8,128)(2,1)S(1)} %collective-permute-done.12.refs_12_), channel_id=1, source_target_pairs={{0,120},{4,124},{8,0},{12,4},{16,8},{20,12},{24,16},{28,20},{32,24... | collective-permute-start | bytes 393224 | tf_op jit(solution)/shard_map/ppermute | solution.py:53
  88.8 6.0 %collective-permute-done.13.refs_13_ = bf16[2,2,64,256]{3,2,1,0:T(8,128)(2,1)S(1)} collective-permute-done((bf16[2,2,64,256]{3,2,1,0:T(8,128)(2,1)S(1)}, bf16[2,2,64,256]{3,2,1,0:T(8,128)(2,1)S(1)}, u32[]{:S(2)}, u32[]{:S(2)}) %collective-permute-start.13) | collective-permute-done | bytes 131104 | tf_op jit(solution)/shard_map/ppermute | solution.py:49
  94.8 0.0 collective-permute-done.14.refs_14_
  94.8 9.1 %collective-permute-done.15.refs_15_ = bf16[2,2,64,256]{3,2,1,0:T(8,128)(2,1)S(1)} collective-permute-done((bf16[2,2,64,256]{3,2,1,0:T(8,128)(2,1)S(1)}, bf16[2,2,64,256]{3,2,1,0:T(8,128)(2,1)S(1)}, u32[]{:S(2)}, u32[]{:S(2)}) %collective-permute-start.15) | collective-permute-done | bytes 131104 | tf_op jit(solution)/shard_map/ppermute | solution.py:49
  103.9 0.1 stack.31.refs_0_
  104.0 0.1 collective-permute-start.17
  104.2 1.0 copy.17
  105.1 0.7 copy.19
  105.8 0.7 pad_maximum_fusion.2.lam_ref
  106.5 9.4 %all-gather.4.cloned.1.call-done.kv_ref = bf16[8192,640]{1,0:T(8,128)(2,1)} async-done(((bf16[256,640]{1,0:T(8,128)(2,1)}), bf16[8192,640]{1,0:T(8,128)(2,1)}) %all-gather.4.cloned.1.call-update) | async-done | bytes 10485776 | tf_op jit(solution)/shard_map/all_gather | solution.py:318
  115.9 26.9 %attend.1 = bf16[256,512]{1,0:T(8,128)(2,1)} custom-call(bf16[256,256]{1,0:T(8,128)(2,1)} %bitcast.37, bf16[256,512]{1,0:T(8,128)(2,1)} %bitcast.34, bf16[8192,640]{1,0:T(8,128)(2,1)} %all-gather.4.cloned.1.call-done.kv_ref, f32[4]{0:T(128)} %pad_maximum_fusion.2.lam_ref, f32[1,128]{1,0:T(1,128)} %bitcast.42), custom_call_target="tpu_custom_call" | custom-call | flops 8589934592 | bytes 10485760 | tf_op jit(solution)/shard_map/attend/pallas_call | solution.py:142
  142.7 2.7 %convolution_convert_fusion = bf16[256,2048]{1,0:T(8,128)(2,1)} fusion(bf16[256,512]{1,0:T(8,128)(2,1)} %attend.1, bf16[256,2048]{1,0:T(8,128)(2,1)S(1)} %copy-done.8, bf16[256,2048]{1,0:T(8,128)(2,1)S(1)} %copy-done.9), kind=kOutput, calls=%fused_computation | convolution fusion | flops 541589504 | bytes 3407872 | tf_op jit(solution)/shard_map/dot_general | solution.py:345
  145.4 4.2 %all-to-all-start = ((bf16[4,64,2048]{2,1,0:T(8,128)(2,1)}), bf16[4,64,2048]{2,1,0:T(8,128)(2,1)S(1)}, u32[]{:S(2)}, u32[]{:S(2)}) async-start(bf16[4,64,2048]{2,1,0:T(8,128)(2,1)} %bitcast.32), calls=%async_computation | async-start | bytes 2097152 | tf_op jit(solution)/shard_map/all_to_all | solution.py:28
  149.7 0.0 collective-permute-done.17.refs_2_
  149.7 0.5 collective-permute-start.18
  150.2 15.0 %all-to-all-done = bf16[4,64,2048]{2,1,0:T(8,128)(2,1)S(1)} async-done(((bf16[4,64,2048]{2,1,0:T(8,128)(2,1)}), bf16[4,64,2048]{2,1,0:T(8,128)(2,1)S(1)}, u32[]{:S(2)}, u32[]{:S(2)}) %all-to-all-start) | async-done | bytes 1048608 | tf_op jit(solution)/shard_map/all_to_all | solution.py:28
  165.2 0.2 convert_reduce_fusion.1
  165.3 0.2 fusion.3
  165.5 0.1 fusion.5
  165.7 1.2 broadcast_in_dim.2
  166.8 3.8 %all-to-all-start.1 = ((bf16[4,64,2048]{2,1,0:T(8,128)(2,1)}), bf16[4,64,2048]{2,1,0:T(8,128)(2,1)S(1)}, u32[]{:S(2)}, u32[]{:S(2)}) async-start(bf16[4,64,2048]{2,1,0:T(8,128)(2,1)} %broadcast_in_dim.2), calls=%async_computation.1 | async-start | bytes 2097152 | tf_op jit(solution)/shard_map/all_to_all | solution.py:38
  170.7 0.0 collective-permute-done.18.refs_3_
  170.7 14.3 %all-to-all-done.1 = bf16[4,64,2048]{2,1,0:T(8,128)(2,1)S(1)} async-done(((bf16[4,64,2048]{2,1,0:T(8,128)(2,1)}), bf16[4,64,2048]{2,1,0:T(8,128)(2,1)S(1)}, u32[]{:S(2)}, u32[]{:S(2)}) %all-to-all-start.1) | async-done | bytes 1048608 | tf_op jit(solution)/shard_map/all_to_all | solution.py:38
  185.0 8.5 %early_mixer.1.early_ref = f32[256,2048]{1,0:T(8,128)S(1)} custom-call(s32[1]{0:T(128)} %bitcast.13.chip_ref, bf16[256,2048]{1,0:T(8,128)(2,1)S(1)} %bitcast.24, bf16[16,2,2,64,256]{4,3,2,1,0:T(8,128)(2,1)} %copy-done, bf16[16,2,2,64,256]{4,3,2,1,0:T(8,128)(2,1)} %collective-permute-done.16.refs_1_, ...), custom_call_target="tpu_custom_call" | custom-call | flops 2147483648 | bytes 8388608 | tf_op jit(solution)/shard_map/early_mixer/pallas_call | solution.py:210
  193.4 1.3 copy-done.1
  194.8 8.8 %mixer.1 = bf16[256,2048]{1,0:T(8,128)(2,1)S(1)} custom-call(bf16[256,2048]{1,0:T(8,128)(2,1)S(1)} %bitcast.25, bf16[32,2,64,1024]{3,2,1,0:T(8,128)(2,1)} %bitcast.27, f32[256,2048]{1,0:T(8,128)} %copy-done.1), custom_call_target="tpu_custom_call" | custom-call | flops 2147483648 | bytes 8388608 | tf_op jit(solution)/shard_map/mixer/pallas_call | solution.py:269
  203.6 16.1 %all_to_all.15 = bf16[4,64,2048]{2,1,0:T(8,128)(2,1)S(1)} all-to-all(bf16[4,64,2048]{2,1,0:T(8,128)(2,1)S(1)} %bitcast.26), channel_id=1, replica_groups=mesh['grp'=2,'sp'=32,'tp'=4] {'tp'}, dimensions={0} | all-to-all | bytes 2097152 | tf_op jit(solution)/shard_map/all_to_all | solution.py:28
  219.7 0.2 convert_reduce_fusion
  219.9 0.8 fusion.6
  (29 shorter events, 0.1 us)
Async XLA Ops:
  6.5 3.7 %copy-start.3 = (bf16[64,2048]{1,0:T(8,128)(2,1)S(1)}, bf16[64,2048]{1,0:T(8,128)(2,1)}, u32[]{:S(2)}) copy-start(bf16[64,2048]{1,0:T(8,128)(2,1)} %param.28) | copy-start | bytes 786436
  6.5 3.7 %copy-start.2 = (bf16[2048,64]{0,1:T(8,128)(2,1)S(1)}, bf16[2048,64]{0,1:T(8,128)(2,1)}, u32[]{:S(2)}) copy-start(bf16[2048,64]{0,1:T(8,128)(2,1)} %param.29) | copy-start | bytes 786436
  6.6 109.3 %all-gather.4.cloned.1.call-start = ((), (), s32[]{:S(2)}) async-start(), calls=%async_computation.3 | async-start | bytes 10813440 | tf_op jit(solution)/shard_map/all_gather | solution.py:318
  8.4 186.4 %all-gather.6.cloned.1.call-start = ((), (), s32[]{:S(2)}) async-start(), calls=%async_computation.4 | async-start | bytes 8650752 | tf_op jit(solution)/shard_map/all_gather | solution.py:323
  10.3 1.4 collective-permute-start
  11.7 92.4 %copy-start.4 = (bf16[256,2,256]{2,1,0:T(2,128)(2,1)S(1)}, bf16[256,2,256]{2,1,0:T(2,128)(2,1)}, u32[]{:S(2)}) copy-start(bf16[256,2,256]{2,1,0:T(2,128)(2,1)} %param.19) | copy-start | bytes 786436
  11.7 93.4 %copy-start.6 = (bf16[256,2,128]{2,1,0:T(2,128)(2,1)S(1)}, bf16[256,2,128]{2,1,0:T(2,128)(2,1)}, u32[]{:S(2)}) copy-start(bf16[256,2,128]{2,1,0:T(2,128)(2,1)} %param.16) | copy-start | bytes 393220
  11.7 94.1 %copy-start.10 = (f32[2]{0:T(128)S(1)}, f32[2]{0:T(128)}, u32[]{:S(2)}) copy-start(f32[2]{0:T(128)} %param.23) | copy-start | bytes 28
  11.8 94.0 %copy-start.11 = (f32[2]{0:T(128)S(1)}, f32[2]{0:T(128)}, u32[]{:S(2)}) copy-start(f32[2]{0:T(128)} %param.22) | copy-start | bytes 28
  11.8 26.3 %collective-permute-start.1 = (bf16[2,2,64,256]{3,2,1,0:T(8,128)(2,1)S(1)}, bf16[2,2,64,256]{3,2,1,0:T(8,128)(2,1)S(1)}, u32[]{:S(2)}, u32[]{:S(2)}) collective-permute-start(bf16[2,2,64,256]{3,2,1,0:T(8,128)(2,1)S(1)} %maximum_select_fusion.refs_0_), channel_id=1, source_target_pairs={{0,8},{4,12},{8,16},{12,20},{16,24},{20,28},{24,32},{28,36},{32,40... | collective-permute-start | bytes 393224 | tf_op jit(solution)/shard_map/ppermute | solution.py:49
  14.7 23.5 %collective-permute-start.2 = (bf16[2,2,64,256]{3,2,1,0:T(8,128)(2,1)S(1)}, bf16[2,2,64,256]{3,2,1,0:T(8,128)(2,1)S(1)}, u32[]{:S(2)}, u32[]{:S(2)}) collective-permute-start(bf16[2,2,64,256]{3,2,1,0:T(8,128)(2,1)S(1)} %maximum_select_fusion.refs_0_), channel_id=1, source_target_pairs={{0,120},{4,124},{8,0},{12,4},{16,8},{20,12},{24,16},{28,20},{32,24... | collective-permute-start | bytes 393224 | tf_op jit(solution)/shard_map/ppermute | solution.py:53
  38.1 9.9 %collective-permute-start.3 = (bf16[2,2,64,256]{3,2,1,0:T(8,128)(2,1)S(1)}, bf16[2,2,64,256]{3,2,1,0:T(8,128)(2,1)S(1)}, u32[]{:S(2)}, u32[]{:S(2)}) collective-permute-start(bf16[2,2,64,256]{3,2,1,0:T(8,128)(2,1)S(1)} %collective-permute-done.1.refs_1_), channel_id=1, source_target_pairs={{0,8},{4,12},{8,16},{12,20},{16,24},{20,28},{24,32},{28,36},{32,40... | collective-permute-start | bytes 393224 | tf_op jit(solution)/shard_map/ppermute | solution.py:49
  38.2 9.8 %collective-permute-start.4 = (bf16[2,2,64,256]{3,2,1,0:T(8,128)(2,1)S(1)}, bf16[2,2,64,256]{3,2,1,0:T(8,128)(2,1)S(1)}, u32[]{:S(2)}, u32[]{:S(2)}) collective-permute-start(bf16[2,2,64,256]{3,2,1,0:T(8,128)(2,1)S(1)} %collective-permute-done.2.refs_2_), channel_id=1, source_target_pairs={{0,120},{4,124},{8,0},{12,4},{16,8},{20,12},{24,16},{28,20},{32,24... | collective-permute-start | bytes 393224 | tf_op jit(solution)/shard_map/ppermute | solution.py:53
  47.9 9.6 %collective-permute-start.5 = (bf16[2,2,64,256]{3,2,1,0:T(8,128)(2,1)S(1)}, bf16[2,2,64,256]{3,2,1,0:T(8,128)(2,1)S(1)}, u32[]{:S(2)}, u32[]{:S(2)}) collective-permute-start(bf16[2,2,64,256]{3,2,1,0:T(8,128)(2,1)S(1)} %collective-permute-done.3.refs_3_), channel_id=1, source_target_pairs={{0,8},{4,12},{8,16},{12,20},{16,24},{20,28},{24,32},{28,36},{32,40... | collective-permute-start | bytes 393224 | tf_op jit(solution)/shard_map/ppermute | solution.py:49
  48.0 9.6 %collective-permute-start.6 = (bf16[2,2,64,256]{3,2,1,0:T(8,128)(2,1)S(1)}, bf16[2,2,64,256]{3,2,1,0:T(8,128)(2,1)S(1)}, u32[]{:S(2)}, u32[]{:S(2)}) collective-permute-start(bf16[2,2,64,256]{3,2,1,0:T(8,128)(2,1)S(1)} %collective-permute-done.4.refs_4_), channel_id=1, source_target_pairs={{0,120},{4,124},{8,0},{12,4},{16,8},{20,12},{24,16},{28,20},{32,24... | collective-permute-start | bytes 393224 | tf_op jit(solution)/shard_map/ppermute | solution.py:53
  57.6 9.4 %collective-permute-start.7 = (bf16[2,2,64,256]{3,2,1,0:T(8,128)(2,1)S(1)}, bf16[2,2,64,256]{3,2,1,0:T(8,128)(2,1)S(1)}, u32[]{:S(2)}, u32[]{:S(2)}) collective-permute-start(bf16[2,2,64,256]{3,2,1,0:T(8,128)(2,1)S(1)} %collective-permute-done.5.refs_5_), channel_id=1, source_target_pairs={{0,8},{4,12},{8,16},{12,20},{16,24},{20,28},{24,32},{28,36},{32,40... | collective-permute-start | bytes 393224 | tf_op jit(solution)/shard_map/ppermute | solution.py:49
  57.6 9.4 %collective-permute-start.8 = (bf16[2,2,64,256]{3,2,1,0:T(8,128)(2,1)S(1)}, bf16[2,2,64,256]{3,2,1,0:T(8,128)(2,1)S(1)}, u32[]{:S(2)}, u32[]{:S(2)}) collective-permute-start(bf16[2,2,64,256]{3,2,1,0:T(8,128)(2,1)S(1)} %collective-permute-done.6.refs_6_), channel_id=1, source_target_pairs={{0,120},{4,124},{8,0},{12,4},{16,8},{20,12},{24,16},{28,20},{32,24... | collective-permute-start | bytes 393224 | tf_op jit(solution)/shard_map/ppermute | solution.py:53
  67.0 9.2 %collective-permute-start.9 = (bf16[2,2,64,256]{3,2,1,0:T(8,128)(2,1)S(1)}, bf16[2,2,64,256]{3,2,1,0:T(8,128)(2,1)S(1)}, u32[]{:S(2)}, u32[]{:S(2)}) collective-permute-start(bf16[2,2,64,256]{3,2,1,0:T(8,128)(2,1)S(1)} %collective-permute-done.7.refs_7_), channel_id=1, source_target_pairs={{0,8},{4,12},{8,16},{12,20},{16,24},{20,28},{24,32},{28,36},{32,40... | collective-permute-start | bytes 393224 | tf_op jit(solution)/shard_map/ppermute | solution.py:49
  67.0 9.2 %collective-permute-start.10 = (bf16[2,2,64,256]{3,2,1,0:T(8,128)(2,1)S(1)}, bf16[2,2,64,256]{3,2,1,0:T(8,128)(2,1)S(1)}, u32[]{:S(2)}, u32[]{:S(2)}) collective-permute-start(bf16[2,2,64,256]{3,2,1,0:T(8,128)(2,1)S(1)} %collective-permute-done.8.refs_8_), channel_id=1, source_target_pairs={{0,120},{4,124},{8,0},{12,4},{16,8},{20,12},{24,16},{28,20},{32,24... | collective-permute-start | bytes 393224 | tf_op jit(solution)/shard_map/ppermute | solution.py:53
  76.3 9.1 %collective-permute-start.11 = (bf16[2,2,64,256]{3,2,1,0:T(8,128)(2,1)S(1)}, bf16[2,2,64,256]{3,2,1,0:T(8,128)(2,1)S(1)}, u32[]{:S(2)}, u32[]{:S(2)}) collective-permute-start(bf16[2,2,64,256]{3,2,1,0:T(8,128)(2,1)S(1)} %collective-permute-done.9.refs_9_), channel_id=1, source_target_pairs={{0,8},{4,12},{8,16},{12,20},{16,24},{20,28},{24,32},{28,36},{32,40... | collective-permute-start | bytes 393224 | tf_op jit(solution)/shard_map/ppermute | solution.py:49
  76.3 9.1 %collective-permute-start.12 = (bf16[2,2,64,256]{3,2,1,0:T(8,128)(2,1)S(1)}, bf16[2,2,64,256]{3,2,1,0:T(8,128)(2,1)S(1)}, u32[]{:S(2)}, u32[]{:S(2)}) collective-permute-start(bf16[2,2,64,256]{3,2,1,0:T(8,128)(2,1)S(1)} %collective-permute-done.10.refs_10_), channel_id=1, source_target_pairs={{0,120},{4,124},{8,0},{12,4},{16,8},{20,12},{24,16},{28,20},{32,24... | collective-permute-start | bytes 393224 | tf_op jit(solution)/shard_map/ppermute | solution.py:53
  85.3 9.4 %collective-permute-start.13 = (bf16[2,2,64,256]{3,2,1,0:T(8,128)(2,1)S(1)}, bf16[2,2,64,256]{3,2,1,0:T(8,128)(2,1)S(1)}, u32[]{:S(2)}, u32[]{:S(2)}) collective-permute-start(bf16[2,2,64,256]{3,2,1,0:T(8,128)(2,1)S(1)} %collective-permute-done.11.refs_11_), channel_id=1, source_target_pairs={{0,8},{4,12},{8,16},{12,20},{16,24},{20,28},{24,32},{28,36},{32,40... | collective-permute-start | bytes 393224 | tf_op jit(solution)/shard_map/ppermute | solution.py:49
  85.3 9.4 %collective-permute-start.14 = (bf16[2,2,64,256]{3,2,1,0:T(8,128)(2,1)S(1)}, bf16[2,2,64,256]{3,2,1,0:T(8,128)(2,1)S(1)}, u32[]{:S(2)}, u32[]{:S(2)}) collective-permute-start(bf16[2,2,64,256]{3,2,1,0:T(8,128)(2,1)S(1)} %collective-permute-done.12.refs_12_), channel_id=1, source_target_pairs={{0,120},{4,124},{8,0},{12,4},{16,8},{20,12},{24,16},{28,20},{32,24... | collective-permute-start | bytes 393224 | tf_op jit(solution)/shard_map/ppermute | solution.py:53
  94.8 9.1 %collective-permute-start.15 = (bf16[2,2,64,256]{3,2,1,0:T(8,128)(2,1)S(1)}, bf16[2,2,64,256]{3,2,1,0:T(8,128)(2,1)S(1)}, u32[]{:S(2)}, u32[]{:S(2)}) collective-permute-start(bf16[2,2,64,256]{3,2,1,0:T(8,128)(2,1)S(1)} %collective-permute-done.13.refs_13_), channel_id=1, source_target_pairs={{0,8},{4,12},{8,16},{12,20},{16,24},{20,28},{24,32},{28,36},{32,40... | collective-permute-start | bytes 393224 | tf_op jit(solution)/shard_map/ppermute | solution.py:49
  104.0 45.7 %copy-start = (bf16[16,2,2,64,256]{4,3,2,1,0:T(8,128)(2,1)}, bf16[16,2,2,64,256]{4,3,2,1,0:T(8,128)(2,1)S(1)}, u32[]{:S(2)}) copy-start(bf16[16,2,2,64,256]{4,3,2,1,0:T(8,128)(2,1)S(1)} %stack.31.refs_0_) | copy-start | bytes 6291460
  104.0 45.7 %collective-permute-start.17 = (bf16[16,2,2,64,256]{4,3,2,1,0:T(8,128)(2,1)S(1)}, bf16[16,2,2,64,256]{4,3,2,1,0:T(8,128)(2,1)}, u32[]{:S(2)}, u32[]{:S(2)}) collective-permute-start(bf16[16,2,2,64,256]{4,3,2,1,0:T(8,128)(2,1)S(1)} %stack.31.refs_0_), channel_id=1, source_target_pairs={{0,128},{128,0},{1,129},{129,1},{2,130},{130,2},{3,131},{131,3},{4... | collective-permute-start | bytes 6291464 | tf_op jit(solution)/shard_map/ppermute | solution.py:331
  115.9 26.9 %copy-start.8 = (bf16[256,2048]{1,0:T(8,128)(2,1)S(1)}, bf16[256,2048]{1,0:T(8,128)(2,1)}, u32[]{:S(2)}) copy-start(bf16[256,2048]{1,0:T(8,128)(2,1)} %param.26) | copy-start | bytes 3145732
  115.9 26.9 %copy-start.9 = (bf16[256,2048]{1,0:T(8,128)(2,1)S(1)}, bf16[256,2048]{1,0:T(8,128)(2,1)}, u32[]{:S(2)}) copy-start(bf16[256,2048]{1,0:T(8,128)(2,1)} %param.25) | copy-start | bytes 3145732
  145.4 4.8 %copy-start.7 = (bf16[2048]{0:T(1024)(128)(2,1)S(1)}, bf16[2048]{0:T(1024)(128)(2,1)}, u32[]{:S(2)}) copy-start(bf16[2048]{0:T(1024)(128)(2,1)} %param.27) | copy-start | bytes 12292
  145.4 19.9 %copy-start.5 = (bf16[64,2048]{1,0:T(8,128)(2,1)S(1)}, bf16[64,2048]{1,0:T(8,128)(2,1)}, u32[]{:S(2)}) copy-start(bf16[64,2048]{1,0:T(8,128)(2,1)} %param.15) | copy-start | bytes 786436
  145.4 19.7 %all-to-all-start = ((bf16[4,64,2048]{2,1,0:T(8,128)(2,1)}), bf16[4,64,2048]{2,1,0:T(8,128)(2,1)S(1)}, u32[]{:S(2)}, u32[]{:S(2)}) async-start(bf16[4,64,2048]{2,1,0:T(8,128)(2,1)} %bitcast.32), calls=%async_computation | async-start | bytes 2097152 | tf_op jit(solution)/shard_map/all_to_all | solution.py:28
  149.7 21.0 %collective-permute-start.16 = (bf16[16,2,2,64,256]{4,3,2,1,0:T(8,128)(2,1)S(1)}, bf16[16,2,2,64,256]{4,3,2,1,0:T(8,128)(2,1)}, u32[]{:S(2)}, u32[]{:S(2)}) collective-permute-start(bf16[16,2,2,64,256]{4,3,2,1,0:T(8,128)(2,1)S(1)} %stack.31.refs_0_), channel_id=1, source_target_pairs={{0,4},{4,0},{8,12},{12,8},{16,20},{20,16},{24,28},{28,24},{32,36},... | collective-permute-start | bytes 6291464 | tf_op jit(solution)/shard_map/ppermute | solution.py:332
  149.7 21.0 %collective-permute-start.18 = (bf16[16,2,2,64,256]{4,3,2,1,0:T(8,128)(2,1)}, bf16[16,2,2,64,256]{4,3,2,1,0:T(8,128)(2,1)}, u32[]{:S(2)}, u32[]{:S(2)}) collective-permute-start(bf16[16,2,2,64,256]{4,3,2,1,0:T(8,128)(2,1)} %collective-permute-done.17.refs_2_), channel_id=1, source_target_pairs={{0,4},{4,0},{8,12},{12,8},{16,20},{20,16},{24,28},{28,24},{32,36},... | collective-permute-start | bytes 6291464 | tf_op jit(solution)/shard_map/ppermute | solution.py:333
  166.8 18.1 %all-to-all-start.1 = ((bf16[4,64,2048]{2,1,0:T(8,128)(2,1)}), bf16[4,64,2048]{2,1,0:T(8,128)(2,1)S(1)}, u32[]{:S(2)}, u32[]{:S(2)}) async-start(bf16[4,64,2048]{2,1,0:T(8,128)(2,1)} %broadcast_in_dim.2), calls=%async_computation.1 | async-start | bytes 2097152 | tf_op jit(solution)/shard_map/all_to_all | solution.py:38
  193.4 1.4 copy-start.1
Sparse Core Ops, SparseCore 0:
  9.2 106.6 all-gather.3
  117.7 72.4 all-gather.5

commit v4 on v3

--- a/solution.py
+++ b/solution.py
@@ -15,7 +15,6 @@
 LAST_DIMS = (((1,), (1,)), ((), ()))
 VMEM_LIMIT = 58 * 2**20
 EARLY = 8
-BATCHES = ()
 
 
 def split_up(array, dim, peers):
@@ -38,25 +37,22 @@
     return lax.all_to_all(copies, axis, split_axis=0, concat_axis=0, tiled=True)
 
 
-def ring(block, batches):
+def ring(block):
     peers = lax.axis_size("sp")
     chips = peers // 2
     onward = [(i, (i + 2) % peers) for i in range(peers)]
     backward = [(i, (i - 2) % peers) for i in range(peers)]
     ahead, behind = block, block
-    waiting, stacks, places = [block], [], [0]
+    blocks, places = [block], [0]
     for step in range(1, chips // 2 + 1):
         ahead = lax.ppermute(ahead, "sp", onward)
-        waiting.append(ahead)
+        blocks.append(ahead)
         places.append(-step % chips)
         if step < chips - chips // 2:
             behind = lax.ppermute(behind, "sp", backward)
-            waiting.append(behind)
+            blocks.append(behind)
             places.append(step)
-        if step in batches or step == chips // 2:
-            stacks.append(stacked(waiting))
-            waiting = []
-    return stacks, places
+    return stacked(blocks), places
 
 
 def stack_kernel(*refs):
@@ -167,10 +163,13 @@
     )(qn, qw, kv, lam, gain)
 
 
-def early_mixer_kernel(chip_ref, x_ref, *refs, places, batches):
-    weights, (out_ref, x_s, out_s) = refs[:-3], refs[-3:]
+def early_mixer_kernel(chip_ref, x_ref, *refs, places):
+    arrays, (out_ref, w_s, x_s, out_s, sem) = refs[:-5], refs[-5:]
     chips = len(places)
     each = x_ref.shape[1] // chips
+    copies = [pltpu.make_async_copy(w, w_s.at[i], sem.at[i]) for i, w in enumerate(arrays)]
+    for copy in copies:
+        copy.start()
 
     def columns(at):
         chip = lax.rem(chip_ref[0] + at, chips)
@@ -178,52 +177,43 @@
 
     for i, at in enumerate(places):
         x_s[:, i * each : (i + 1) * each] = x_ref[:, columns(at)]
-    for first in range(0, len(weights), batches):
-        some = weights[first : first + batches]
-        lifted, start = 0.0, 0
-        for w in some:
-            up = w[:, :, 0].reshape(-1, w.shape[4])
-            lifted += jnp.dot(
-                x_s[:, start : start + up.shape[0]], up, preferred_element_type=jnp.float32
-            )
-            start += up.shape[0]
-        lifted = jnp.maximum(lifted, 0.0)
-        activated = (lifted * lifted).astype(jnp.bfloat16)
-        start = 0
-        for w in some:
-            down = w[:, :, 1].reshape(-1, w.shape[4])
-            part = lax.dot_general(
-                activated, down, LAST_DIMS, preferred_element_type=jnp.float32
-            )
-            to = slice(start, start + down.shape[0])
-            out_s[:, to] = part if first == 0 else out_s[:, to] + part
-            start += down.shape[0]
+    for k, copy in enumerate(copies):
+        copy.wait()
+        up = w_s[k, :, :, 0].reshape(x_ref.shape[1], w_s.shape[5])
+        down = w_s[k, :, :, 1].reshape(x_ref.shape[1], w_s.shape[5])
+        lifted = jnp.maximum(jnp.dot(x_s[...], up, preferred_element_type=jnp.float32), 0.0)
+        part = lax.dot_general(
+            (lifted * lifted).astype(jnp.bfloat16),
+            down,
+            LAST_DIMS,
+            preferred_element_type=jnp.float32,
+        )
+        out_s[...] = part if k == 0 else out_s[...] + part
     for i, at in enumerate(places):
         out_ref[:, columns(at)] = out_s[:, i * each : (i + 1) * each]
 
 
-def early_mixer(x, weights, places, batches):
+def early_mixer(x, weights, places):
     rows, d = x.shape
-    half = pl.BlockSpec((rows // 2, d), lambda i: (i, 0))
-    hidden = sum(w.shape[4] for w in weights[::batches])
+    hidden = sum(w.shape[4] for w in weights)
     chip = (lax.axis_index("sp") // 2).astype(jnp.int32).reshape(1)
+    vmem = pl.BlockSpec(memory_space=pltpu.VMEM)
     return pl.pallas_call(
-        functools.partial(early_mixer_kernel, places=places, batches=batches),
-        grid=(2,),
+        functools.partial(early_mixer_kernel, places=places),
         in_specs=[
             pl.BlockSpec(memory_space=pltpu.SMEM),
-            half,
-            *(pl.BlockSpec(memory_space=pltpu.VMEM) for _ in weights),
-        ],
-        out_specs=half,
+            vmem,
+            *(pl.BlockSpec(memory_space=pl.ANY) for _ in weights),
+        ],
+        out_specs=vmem,
         out_shape=jax.ShapeDtypeStruct((rows, d), jnp.float32),
         scratch_shapes=[
-            pltpu.VMEM((rows // 2, d), jnp.bfloat16),
-            pltpu.VMEM((rows // 2, d), jnp.float32),
-        ],
-        compiler_params=pltpu.CompilerParams(
-            dimension_semantics=("arbitrary",), vmem_limit_bytes=50 * 2**20
-        ),
+            pltpu.VMEM((len(weights), *weights[0].shape), weights[0].dtype),
+            pltpu.VMEM((rows, d), jnp.bfloat16),
+            pltpu.VMEM((rows, d), jnp.float32),
+            pltpu.SemaphoreType.DMA((len(weights),)),
+        ],
+        compiler_params=pltpu.CompilerParams(vmem_limit_bytes=50 * 2**20),
         cost_estimate=pl.CostEstimate(
             flops=4 * rows * d * hidden, bytes_accessed=4 * d * hidden, transcendentals=0
         ),
@@ -263,7 +253,7 @@
 def mixer(x, w, early):
     rows, d = x.shape
     shards, _, each, hidden = w.shape
-    group = math.gcd(shards, 8)
+    group = math.gcd(shards, 32)
     half = shards // group
     depth = group * each
     return pl.pallas_call(
@@ -325,15 +315,12 @@
     theirs = lax.dynamic_slice_in_dim(own_weights, (2 * side + 1 - core) * each, each, 2)
     theirs = lax.ppermute(theirs, "sp", other_core)
     chip = jnp.where(core == 0, jnp.stack([mine, theirs]), jnp.stack([theirs, mine]))
-    stacks, places = ring(chip, BATCHES)
-    early_weights = [[], [], [], []]
-    for stack in stacks:
-        swapped = lax.ppermute(stack, "grp", other_group)
-        first = lax.ppermute(stack, "sp", other_core)
-        second = lax.ppermute(swapped, "sp", other_core)
-        for kind, array in zip(early_weights, (stack, first, swapped, second)):
-            kind.append(array)
-    kv = after(kv, *stacks)
+    stack, places = ring(chip)
+    swapped = lax.ppermute(stack, "grp", other_group)
+    first = lax.ppermute(stack, "sp", other_core)
+    second = lax.ppermute(swapped, "sp", other_core)
+    early_weights = (stack, first, swapped, second)
+    kv = after(kv, stack)
     attended = attention(
         query_narrow.reshape(rows, -1),
         query_wide.reshape(rows, -1),
@@ -351,7 +338,7 @@
     )
     normed = (normed * norm_gain.astype(jnp.float32)).astype(jnp.bfloat16)
     normed = copy_for_each(normed, "tp").reshape(-1, normed.shape[1])
-    early = early_mixer(normed, sum(early_weights, []), places, len(stacks))
+    early = early_mixer(normed, early_weights, places)
     mixer_out = sent_and_summed(mixer(normed, late_weights, early), "tp", 0)
     return (middle_f32 + mixer_out).astype(jnp.bfloat16)
 

time: 228 us -> 224 us (0.982)
  Pallas kernels: 44.2 us -> 39.8 us
    pallas_call x1, Pallas kernels: 8.76 us -> 6.12 us  [mixer(): pl.pallas_call(functools.partial(mixer_kernel, half=half), grid=(2 * half...]
  transfers between devices with their start and end apart: 23 -> 23, of which waited for: 13 -> 13; matrix products, arithmetic and copies ran while one was open for 4% -> 4% of each run, Pallas kernels for 16% -> 15%
where the time goes in v4:
time: 224 us
  waiting for transfers between devices  89.3 us (40%)
  starting transfers between devices  51.6 us (23%)
  Pallas kernels  39.8 us (18%)
  blocking collectives  16.8 us (8%)
  between operations  13.7 us (6%)
  other arithmetic  5.59 us (2%)
  local copies, waits for them, and re-layouts  4.18 us (2%)
  matrix products  2.71 us (1%)
    ppermute x8, waiting for transfers between devices, ring(): ahead = lax.ppermute(ahead, 'sp', onward)  49.3 us
    ppermute x7, starting transfers between devices, ring(): behind = lax.ppermute(behind, 'sp', backward)  39.8 us
    pallas_call x1, Pallas kernels, attention(): pl.pallas_call(functools.partial(attend_kernel, dn=dn, dw=dw, dv=dv, step...  26.9 us
    all_to_all x1, blocking collectives, sent_and_summed(): parts = lax.all_to_all(split_up(array, dim, peers), axis, 0, 0, tiled=True)  16.8 us
    all_to_all x1, waiting for transfers between devices, sent_and_summed(): parts = lax.all_to_all(split_up(array, dim, peers), axis, 0, 0, tiled=True)  15 us
    all_to_all x1, waiting for transfers between devices, copy_for_each(): return lax.all_to_all(copies, axis, split_axis=0, concat_axis=0, tiled=True)  14.3 us
    all_gather x1, waiting for transfers between devices, shards(): kv = lax.all_gather(own, 'sp', axis=0, tiled=True)  9.38 us
    pallas_call x1, Pallas kernels, early_mixer(): pl.pallas_call(functools.partial(early_mixer_kernel, places=places), in_s...  6.72 us
  transfers between devices with their start and end apart: 23, of which 13 were waited for; matrix products, arithmetic and copies ran while one was open for 4% of the time, Pallas kernels for 15%

profile of v4, /device:TPU:40, one launch (start us, length us, event | category | flops | bytes accessed | tf_op | source)
XLA Modules:
  0.0 223.7 jit_solution(12159129308875343983)
XLA Ops:
  6.6 1.8 pad_maximum_fusion
  8.3 0.1 all-gather.4.cloned.1.call-update
  8.4 0.1 all-gather.6.cloned.1.call-start
  8.5 1.7 pad_maximum_fusion.1
  10.2 0.1 all-gather.6.cloned.1.call-update
  10.3 0.1 collective-permute-start
  10.5 1.2 collective-permute-done
  11.7 0.0 copy-start.4
  11.7 0.0 copy-start.6
  11.7 0.0 copy-start.10
  11.8 0.0 copy-start.11
  11.8 2.9 %collective-permute-start.1 = (bf16[2,2,64,256]{3,2,1,0:T(8,128)(2,1)S(1)}, bf16[2,2,64,256]{3,2,1,0:T(8,128)(2,1)S(1)}, u32[]{:S(2)}, u32[]{:S(2)}) collective-permute-start(bf16[2,2,64,256]{3,2,1,0:T(8,128)(2,1)S(1)} %maximum_select_fusion.refs_0_), channel_id=1, source_target_pairs={{0,8},{4,12},{8,16},{12,20},{16,24},{20,28},{24,32},{28,36},{32,40... | collective-permute-start | bytes 393224 | tf_op jit(solution)/shard_map/ppermute | solution.py:48
  14.7 19.7 %collective-permute-start.2 = (bf16[2,2,64,256]{3,2,1,0:T(8,128)(2,1)S(1)}, bf16[2,2,64,256]{3,2,1,0:T(8,128)(2,1)S(1)}, u32[]{:S(2)}, u32[]{:S(2)}) collective-permute-start(bf16[2,2,64,256]{3,2,1,0:T(8,128)(2,1)S(1)} %maximum_select_fusion.refs_0_), channel_id=1, source_target_pairs={{0,120},{4,124},{8,0},{12,4},{16,8},{20,12},{24,16},{28,20},{32,24... | collective-permute-start | bytes 393224 | tf_op jit(solution)/shard_map/ppermute | solution.py:52
  34.4 3.7 %collective-permute-done.1.refs_1_ = bf16[2,2,64,256]{3,2,1,0:T(8,128)(2,1)S(1)} collective-permute-done((bf16[2,2,64,256]{3,2,1,0:T(8,128)(2,1)S(1)}, bf16[2,2,64,256]{3,2,1,0:T(8,128)(2,1)S(1)}, u32[]{:S(2)}, u32[]{:S(2)}) %collective-permute-start.1) | collective-permute-done | bytes 131104 | tf_op jit(solution)/shard_map/ppermute | solution.py:48
  38.1 0.0 collective-permute-start.3
  38.1 0.1 collective-permute-done.2.refs_2_
  38.2 3.7 %collective-permute-start.4 = (bf16[2,2,64,256]{3,2,1,0:T(8,128)(2,1)S(1)}, bf16[2,2,64,256]{3,2,1,0:T(8,128)(2,1)S(1)}, u32[]{:S(2)}, u32[]{:S(2)}) collective-permute-start(bf16[2,2,64,256]{3,2,1,0:T(8,128)(2,1)S(1)} %collective-permute-done.2.refs_2_), channel_id=1, source_target_pairs={{0,120},{4,124},{8,0},{12,4},{16,8},{20,12},{24,16},{28,20},{32,24... | collective-permute-start | bytes 393224 | tf_op jit(solution)/shard_map/ppermute | solution.py:52
  41.9 6.1 %collective-permute-done.3.refs_3_ = bf16[2,2,64,256]{3,2,1,0:T(8,128)(2,1)S(1)} collective-permute-done((bf16[2,2,64,256]{3,2,1,0:T(8,128)(2,1)S(1)}, bf16[2,2,64,256]{3,2,1,0:T(8,128)(2,1)S(1)}, u32[]{:S(2)}, u32[]{:S(2)}) %collective-permute-start.3) | collective-permute-done | bytes 131104 | tf_op jit(solution)/shard_map/ppermute | solution.py:48
  47.9 0.0 collective-permute-start.5
  47.9 0.0 collective-permute-done.4.refs_4_
  48.0 3.2 %collective-permute-start.6 = (bf16[2,2,64,256]{3,2,1,0:T(8,128)(2,1)S(1)}, bf16[2,2,64,256]{3,2,1,0:T(8,128)(2,1)S(1)}, u32[]{:S(2)}, u32[]{:S(2)}) collective-permute-start(bf16[2,2,64,256]{3,2,1,0:T(8,128)(2,1)S(1)} %collective-permute-done.4.refs_4_), channel_id=1, source_target_pairs={{0,120},{4,124},{8,0},{12,4},{16,8},{20,12},{24,16},{28,20},{32,24... | collective-permute-start | bytes 393224 | tf_op jit(solution)/shard_map/ppermute | solution.py:52
  51.2 6.4 %collective-permute-done.5.refs_5_ = bf16[2,2,64,256]{3,2,1,0:T(8,128)(2,1)S(1)} collective-permute-done((bf16[2,2,64,256]{3,2,1,0:T(8,128)(2,1)S(1)}, bf16[2,2,64,256]{3,2,1,0:T(8,128)(2,1)S(1)}, u32[]{:S(2)}, u32[]{:S(2)}) %collective-permute-start.5) | collective-permute-done | bytes 131104 | tf_op jit(solution)/shard_map/ppermute | solution.py:48
  57.6 0.0 collective-permute-start.7
  57.6 0.0 collective-permute-done.6.refs_6_
  57.6 3.2 %collective-permute-start.8 = (bf16[2,2,64,256]{3,2,1,0:T(8,128)(2,1)S(1)}, bf16[2,2,64,256]{3,2,1,0:T(8,128)(2,1)S(1)}, u32[]{:S(2)}, u32[]{:S(2)}) collective-permute-start(bf16[2,2,64,256]{3,2,1,0:T(8,128)(2,1)S(1)} %collective-permute-done.6.refs_6_), channel_id=1, source_target_pairs={{0,120},{4,124},{8,0},{12,4},{16,8},{20,12},{24,16},{28,20},{32,24... | collective-permute-start | bytes 393224 | tf_op jit(solution)/shard_map/ppermute | solution.py:52
  60.8 6.2 %collective-permute-done.7.refs_7_ = bf16[2,2,64,256]{3,2,1,0:T(8,128)(2,1)S(1)} collective-permute-done((bf16[2,2,64,256]{3,2,1,0:T(8,128)(2,1)S(1)}, bf16[2,2,64,256]{3,2,1,0:T(8,128)(2,1)S(1)}, u32[]{:S(2)}, u32[]{:S(2)}) %collective-permute-start.7) | collective-permute-done | bytes 131104 | tf_op jit(solution)/shard_map/ppermute | solution.py:48
  67.0 0.0 collective-permute-start.9
  67.0 0.0 collective-permute-done.8.refs_8_
  67.0 3.2 %collective-permute-start.10 = (bf16[2,2,64,256]{3,2,1,0:T(8,128)(2,1)S(1)}, bf16[2,2,64,256]{3,2,1,0:T(8,128)(2,1)S(1)}, u32[]{:S(2)}, u32[]{:S(2)}) collective-permute-start(bf16[2,2,64,256]{3,2,1,0:T(8,128)(2,1)S(1)} %collective-permute-done.8.refs_8_), channel_id=1, source_target_pairs={{0,120},{4,124},{8,0},{12,4},{16,8},{20,12},{24,16},{28,20},{32,24... | collective-permute-start | bytes 393224 | tf_op jit(solution)/shard_map/ppermute | solution.py:52
  70.3 6.0 %collective-permute-done.9.refs_9_ = bf16[2,2,64,256]{3,2,1,0:T(8,128)(2,1)S(1)} collective-permute-done((bf16[2,2,64,256]{3,2,1,0:T(8,128)(2,1)S(1)}, bf16[2,2,64,256]{3,2,1,0:T(8,128)(2,1)S(1)}, u32[]{:S(2)}, u32[]{:S(2)}) %collective-permute-start.9) | collective-permute-done | bytes 131104 | tf_op jit(solution)/shard_map/ppermute | solution.py:48
  76.3 0.0 collective-permute-start.11
  76.3 3.2 %collective-permute-start.12 = (bf16[2,2,64,256]{3,2,1,0:T(8,128)(2,1)S(1)}, bf16[2,2,64,256]{3,2,1,0:T(8,128)(2,1)S(1)}, u32[]{:S(2)}, u32[]{:S(2)}) collective-permute-start(bf16[2,2,64,256]{3,2,1,0:T(8,128)(2,1)S(1)} %collective-permute-done.10.refs_10_), channel_id=1, source_target_pairs={{0,120},{4,124},{8,0},{12,4},{16,8},{20,12},{24,16},{28,20},{32,24... | collective-permute-start | bytes 393224 | tf_op jit(solution)/shard_map/ppermute | solution.py:52
  79.5 5.8 %collective-permute-done.11.refs_11_ = bf16[2,2,64,256]{3,2,1,0:T(8,128)(2,1)S(1)} collective-permute-done((bf16[2,2,64,256]{3,2,1,0:T(8,128)(2,1)S(1)}, bf16[2,2,64,256]{3,2,1,0:T(8,128)(2,1)S(1)}, u32[]{:S(2)}, u32[]{:S(2)}) %collective-permute-start.11) | collective-permute-done | bytes 131104 | tf_op jit(solution)/shard_map/ppermute | solution.py:48
  85.3 0.0 collective-permute-start.13
  85.3 0.0 collective-permute-done.12.refs_12_
  85.3 3.4 %collective-permute-start.14 = (bf16[2,2,64,256]{3,2,1,0:T(8,128)(2,1)S(1)}, bf16[2,2,64,256]{3,2,1,0:T(8,128)(2,1)S(1)}, u32[]{:S(2)}, u32[]{:S(2)}) collective-permute-start(bf16[2,2,64,256]{3,2,1,0:T(8,128)(2,1)S(1)} %collective-permute-done.12.refs_12_), channel_id=1, source_target_pairs={{0,120},{4,124},{8,0},{12,4},{16,8},{20,12},{24,16},{28,20},{32,24... | collective-permute-start | bytes 393224 | tf_op jit(solution)/shard_map/ppermute | solution.py:52
  88.8 6.0 %collective-permute-done.13.refs_13_ = bf16[2,2,64,256]{3,2,1,0:T(8,128)(2,1)S(1)} collective-permute-done((bf16[2,2,64,256]{3,2,1,0:T(8,128)(2,1)S(1)}, bf16[2,2,64,256]{3,2,1,0:T(8,128)(2,1)S(1)}, u32[]{:S(2)}, u32[]{:S(2)}) %collective-permute-start.13) | collective-permute-done | bytes 131104 | tf_op jit(solution)/shard_map/ppermute | solution.py:48
  94.8 0.0 collective-permute-done.14.refs_14_
  94.8 9.1 %collective-permute-done.15.refs_15_ = bf16[2,2,64,256]{3,2,1,0:T(8,128)(2,1)S(1)} collective-permute-done((bf16[2,2,64,256]{3,2,1,0:T(8,128)(2,1)S(1)}, bf16[2,2,64,256]{3,2,1,0:T(8,128)(2,1)S(1)}, u32[]{:S(2)}, u32[]{:S(2)}) %collective-permute-start.15) | collective-permute-done | bytes 131104 | tf_op jit(solution)/shard_map/ppermute | solution.py:48
  103.9 0.1 stack.31.refs_0_
  104.0 0.1 collective-permute-start.17
  104.2 1.0 copy.17
  105.1 0.7 copy.19
  105.8 0.7 pad_maximum_fusion.2.lam_ref
  106.5 9.4 %all-gather.4.cloned.1.call-done.kv_ref = bf16[8192,640]{1,0:T(8,128)(2,1)} async-done(((bf16[256,640]{1,0:T(8,128)(2,1)}), bf16[8192,640]{1,0:T(8,128)(2,1)}) %all-gather.4.cloned.1.call-update) | async-done | bytes 10485776 | tf_op jit(solution)/shard_map/all_gather | solution.py:308
  115.9 26.9 %attend.1 = bf16[256,512]{1,0:T(8,128)(2,1)} custom-call(bf16[256,256]{1,0:T(8,128)(2,1)} %bitcast.37, bf16[256,512]{1,0:T(8,128)(2,1)} %bitcast.34, bf16[8192,640]{1,0:T(8,128)(2,1)} %all-gather.4.cloned.1.call-done.kv_ref, f32[4]{0:T(128)} %pad_maximum_fusion.2.lam_ref, f32[1,128]{1,0:T(1,128)} %bitcast.42), custom_call_target="tpu_custom_call" | custom-call | flops 8589934592 | bytes 10485760 | tf_op jit(solution)/shard_map/attend/pallas_call | solution.py:138
  142.7 2.7 %convolution_convert_fusion = bf16[256,2048]{1,0:T(8,128)(2,1)} fusion(bf16[256,512]{1,0:T(8,128)(2,1)} %attend.1, bf16[256,2048]{1,0:T(8,128)(2,1)S(1)} %copy-done.8, bf16[256,2048]{1,0:T(8,128)(2,1)S(1)} %copy-done.9), kind=kOutput, calls=%fused_computation | convolution fusion | flops 541589504 | bytes 3407872 | tf_op jit(solution)/shard_map/dot_general | solution.py:332
  145.4 4.2 %all-to-all-start = ((bf16[4,64,2048]{2,1,0:T(8,128)(2,1)}), bf16[4,64,2048]{2,1,0:T(8,128)(2,1)S(1)}, u32[]{:S(2)}, u32[]{:S(2)}) async-start(bf16[4,64,2048]{2,1,0:T(8,128)(2,1)} %bitcast.32), calls=%async_computation | async-start | bytes 2097152 | tf_op jit(solution)/shard_map/all_to_all | solution.py:27
  149.7 0.0 collective-permute-done.17.refs_2_
  149.7 0.5 collective-permute-start.18
  150.2 15.0 %all-to-all-done = bf16[4,64,2048]{2,1,0:T(8,128)(2,1)S(1)} async-done(((bf16[4,64,2048]{2,1,0:T(8,128)(2,1)}), bf16[4,64,2048]{2,1,0:T(8,128)(2,1)S(1)}, u32[]{:S(2)}, u32[]{:S(2)}) %all-to-all-start) | async-done | bytes 1048608 | tf_op jit(solution)/shard_map/all_to_all | solution.py:27
  165.2 0.2 convert_reduce_fusion.1
  165.3 0.2 fusion.3
  165.5 0.1 fusion.5
  165.7 1.2 broadcast_in_dim.2
  166.8 3.8 %all-to-all-start.1 = ((bf16[4,64,2048]{2,1,0:T(8,128)(2,1)}), bf16[4,64,2048]{2,1,0:T(8,128)(2,1)S(1)}, u32[]{:S(2)}, u32[]{:S(2)}) async-start(bf16[4,64,2048]{2,1,0:T(8,128)(2,1)} %broadcast_in_dim.2), calls=%async_computation.1 | async-start | bytes 2097152 | tf_op jit(solution)/shard_map/all_to_all | solution.py:37
  170.7 0.0 collective-permute-done.18.refs_3_
  170.7 14.3 %all-to-all-done.1 = bf16[4,64,2048]{2,1,0:T(8,128)(2,1)S(1)} async-done(((bf16[4,64,2048]{2,1,0:T(8,128)(2,1)}), bf16[4,64,2048]{2,1,0:T(8,128)(2,1)S(1)}, u32[]{:S(2)}, u32[]{:S(2)}) %all-to-all-start.1) | async-done | bytes 1048608 | tf_op jit(solution)/shard_map/all_to_all | solution.py:37
  185.0 6.7 %early_mixer.1.early_ref = f32[256,2048]{1,0:T(8,128)S(1)} custom-call(s32[1]{0:T(128)} %bitcast.13.chip_ref, bf16[256,2048]{1,0:T(8,128)(2,1)S(1)} %bitcast.24, bf16[16,2,2,64,256]{4,3,2,1,0:T(8,128)(2,1)} %copy-done, bf16[16,2,2,64,256]{4,3,2,1,0:T(8,128)(2,1)} %collective-permute-done.16.refs_1_, ...), custom_call_target="tpu_custom_call" | custom-call | flops 2147483648 | bytes 8388608 | tf_op jit(solution)/shard_map/early_mixer/pallas_call | solution.py:201
  191.7 1.3 copy-done.1
  193.1 6.1 %mixer.1 = bf16[256,2048]{1,0:T(8,128)(2,1)S(1)} custom-call(bf16[256,2048]{1,0:T(8,128)(2,1)S(1)} %bitcast.25, bf16[32,2,64,1024]{3,2,1,0:T(8,128)(2,1)} %bitcast.27, f32[256,2048]{1,0:T(8,128)} %copy-done.1), custom_call_target="tpu_custom_call" | custom-call | flops 2147483648 | bytes 8388608 | tf_op jit(solution)/shard_map/mixer/pallas_call | solution.py:259
  199.2 16.8 %all_to_all.15 = bf16[4,64,2048]{2,1,0:T(8,128)(2,1)S(1)} all-to-all(bf16[4,64,2048]{2,1,0:T(8,128)(2,1)S(1)} %bitcast.26), channel_id=1, replica_groups=mesh['grp'=2,'sp'=32,'tp'=4] {'tp'}, dimensions={0} | all-to-all | bytes 2097152 | tf_op jit(solution)/shard_map/all_to_all | solution.py:27
  216.0 0.2 convert_reduce_fusion
  216.1 0.8 fusion.6
  (29 shorter events, 0.1 us)
Async XLA Ops:
  6.5 3.7 %copy-start.3 = (bf16[64,2048]{1,0:T(8,128)(2,1)S(1)}, bf16[64,2048]{1,0:T(8,128)(2,1)}, u32[]{:S(2)}) copy-start(bf16[64,2048]{1,0:T(8,128)(2,1)} %param.28) | copy-start | bytes 786436
  6.5 3.7 %copy-start.2 = (bf16[2048,64]{0,1:T(8,128)(2,1)S(1)}, bf16[2048,64]{0,1:T(8,128)(2,1)}, u32[]{:S(2)}) copy-start(bf16[2048,64]{0,1:T(8,128)(2,1)} %param.29) | copy-start | bytes 786436
  6.6 109.3 %all-gather.4.cloned.1.call-start = ((), (), s32[]{:S(2)}) async-start(), calls=%async_computation.3 | async-start | bytes 10813440 | tf_op jit(solution)/shard_map/all_gather | solution.py:308
  8.4 184.7 %all-gather.6.cloned.1.call-start = ((), (), s32[]{:S(2)}) async-start(), calls=%async_computation.4 | async-start | bytes 8650752 | tf_op jit(solution)/shard_map/all_gather | solution.py:313
  10.3 1.4 collective-permute-start
  11.7 92.4 %copy-start.4 = (bf16[256,2,256]{2,1,0:T(2,128)(2,1)S(1)}, bf16[256,2,256]{2,1,0:T(2,128)(2,1)}, u32[]{:S(2)}) copy-start(bf16[256,2,256]{2,1,0:T(2,128)(2,1)} %param.19) | copy-start | bytes 786436
  11.7 93.4 %copy-start.6 = (bf16[256,2,128]{2,1,0:T(2,128)(2,1)S(1)}, bf16[256,2,128]{2,1,0:T(2,128)(2,1)}, u32[]{:S(2)}) copy-start(bf16[256,2,128]{2,1,0:T(2,128)(2,1)} %param.16) | copy-start | bytes 393220
  11.7 94.1 %copy-start.10 = (f32[2]{0:T(128)S(1)}, f32[2]{0:T(128)}, u32[]{:S(2)}) copy-start(f32[2]{0:T(128)} %param.23) | copy-start | bytes 28
  11.8 94.0 %copy-start.11 = (f32[2]{0:T(128)S(1)}, f32[2]{0:T(128)}, u32[]{:S(2)}) copy-start(f32[2]{0:T(128)} %param.22) | copy-start | bytes 28
  11.8 26.3 %collective-permute-start.1 = (bf16[2,2,64,256]{3,2,1,0:T(8,128)(2,1)S(1)}, bf16[2,2,64,256]{3,2,1,0:T(8,128)(2,1)S(1)}, u32[]{:S(2)}, u32[]{:S(2)}) collective-permute-start(bf16[2,2,64,256]{3,2,1,0:T(8,128)(2,1)S(1)} %maximum_select_fusion.refs_0_), channel_id=1, source_target_pairs={{0,8},{4,12},{8,16},{12,20},{16,24},{20,28},{24,32},{28,36},{32,40... | collective-permute-start | bytes 393224 | tf_op jit(solution)/shard_map/ppermute | solution.py:48
  14.7 23.5 %collective-permute-start.2 = (bf16[2,2,64,256]{3,2,1,0:T(8,128)(2,1)S(1)}, bf16[2,2,64,256]{3,2,1,0:T(8,128)(2,1)S(1)}, u32[]{:S(2)}, u32[]{:S(2)}) collective-permute-start(bf16[2,2,64,256]{3,2,1,0:T(8,128)(2,1)S(1)} %maximum_select_fusion.refs_0_), channel_id=1, source_target_pairs={{0,120},{4,124},{8,0},{12,4},{16,8},{20,12},{24,16},{28,20},{32,24... | collective-permute-start | bytes 393224 | tf_op jit(solution)/shard_map/ppermute | solution.py:52
  38.1 9.9 %collective-permute-start.3 = (bf16[2,2,64,256]{3,2,1,0:T(8,128)(2,1)S(1)}, bf16[2,2,64,256]{3,2,1,0:T(8,128)(2,1)S(1)}, u32[]{:S(2)}, u32[]{:S(2)}) collective-permute-start(bf16[2,2,64,256]{3,2,1,0:T(8,128)(2,1)S(1)} %collective-permute-done.1.refs_1_), channel_id=1, source_target_pairs={{0,8},{4,12},{8,16},{12,20},{16,24},{20,28},{24,32},{28,36},{32,40... | collective-permute-start | bytes 393224 | tf_op jit(solution)/shard_map/ppermute | solution.py:48
  38.2 9.8 %collective-permute-start.4 = (bf16[2,2,64,256]{3,2,1,0:T(8,128)(2,1)S(1)}, bf16[2,2,64,256]{3,2,1,0:T(8,128)(2,1)S(1)}, u32[]{:S(2)}, u32[]{:S(2)}) collective-permute-start(bf16[2,2,64,256]{3,2,1,0:T(8,128)(2,1)S(1)} %collective-permute-done.2.refs_2_), channel_id=1, source_target_pairs={{0,120},{4,124},{8,0},{12,4},{16,8},{20,12},{24,16},{28,20},{32,24... | collective-permute-start | bytes 393224 | tf_op jit(solution)/shard_map/ppermute | solution.py:52
  47.9 9.6 %collective-permute-start.5 = (bf16[2,2,64,256]{3,2,1,0:T(8,128)(2,1)S(1)}, bf16[2,2,64,256]{3,2,1,0:T(8,128)(2,1)S(1)}, u32[]{:S(2)}, u32[]{:S(2)}) collective-permute-start(bf16[2,2,64,256]{3,2,1,0:T(8,128)(2,1)S(1)} %collective-permute-done.3.refs_3_), channel_id=1, source_target_pairs={{0,8},{4,12},{8,16},{12,20},{16,24},{20,28},{24,32},{28,36},{32,40... | collective-permute-start | bytes 393224 | tf_op jit(solution)/shard_map/ppermute | solution.py:48
  48.0 9.6 %collective-permute-start.6 = (bf16[2,2,64,256]{3,2,1,0:T(8,128)(2,1)S(1)}, bf16[2,2,64,256]{3,2,1,0:T(8,128)(2,1)S(1)}, u32[]{:S(2)}, u32[]{:S(2)}) collective-permute-start(bf16[2,2,64,256]{3,2,1,0:T(8,128)(2,1)S(1)} %collective-permute-done.4.refs_4_), channel_id=1, source_target_pairs={{0,120},{4,124},{8,0},{12,4},{16,8},{20,12},{24,16},{28,20},{32,24... | collective-permute-start | bytes 393224 | tf_op jit(solution)/shard_map/ppermute | solution.py:52
  57.6 9.4 %collective-permute-start.7 = (bf16[2,2,64,256]{3,2,1,0:T(8,128)(2,1)S(1)}, bf16[2,2,64,256]{3,2,1,0:T(8,128)(2,1)S(1)}, u32[]{:S(2)}, u32[]{:S(2)}) collective-permute-start(bf16[2,2,64,256]{3,2,1,0:T(8,128)(2,1)S(1)} %collective-permute-done.5.refs_5_), channel_id=1, source_target_pairs={{0,8},{4,12},{8,16},{12,20},{16,24},{20,28},{24,32},{28,36},{32,40... | collective-permute-start | bytes 393224 | tf_op jit(solution)/shard_map/ppermute | solution.py:48
  57.6 9.4 %collective-permute-start.8 = (bf16[2,2,64,256]{3,2,1,0:T(8,128)(2,1)S(1)}, bf16[2,2,64,256]{3,2,1,0:T(8,128)(2,1)S(1)}, u32[]{:S(2)}, u32[]{:S(2)}) collective-permute-start(bf16[2,2,64,256]{3,2,1,0:T(8,128)(2,1)S(1)} %collective-permute-done.6.refs_6_), channel_id=1, source_target_pairs={{0,120},{4,124},{8,0},{12,4},{16,8},{20,12},{24,16},{28,20},{32,24... | collective-permute-start | bytes 393224 | tf_op jit(solution)/shard_map/ppermute | solution.py:52
  67.0 9.2 %collective-permute-start.9 = (bf16[2,2,64,256]{3,2,1,0:T(8,128)(2,1)S(1)}, bf16[2,2,64,256]{3,2,1,0:T(8,128)(2,1)S(1)}, u32[]{:S(2)}, u32[]{:S(2)}) collective-permute-start(bf16[2,2,64,256]{3,2,1,0:T(8,128)(2,1)S(1)} %collective-permute-done.7.refs_7_), channel_id=1, source_target_pairs={{0,8},{4,12},{8,16},{12,20},{16,24},{20,28},{24,32},{28,36},{32,40... | collective-permute-start | bytes 393224 | tf_op jit(solution)/shard_map/ppermute | solution.py:48
  67.0 9.2 %collective-permute-start.10 = (bf16[2,2,64,256]{3,2,1,0:T(8,128)(2,1)S(1)}, bf16[2,2,64,256]{3,2,1,0:T(8,128)(2,1)S(1)}, u32[]{:S(2)}, u32[]{:S(2)}) collective-permute-start(bf16[2,2,64,256]{3,2,1,0:T(8,128)(2,1)S(1)} %collective-permute-done.8.refs_8_), channel_id=1, source_target_pairs={{0,120},{4,124},{8,0},{12,4},{16,8},{20,12},{24,16},{28,20},{32,24... | collective-permute-start | bytes 393224 | tf_op jit(solution)/shard_map/ppermute | solution.py:52
  76.3 9.1 %collective-permute-start.11 = (bf16[2,2,64,256]{3,2,1,0:T(8,128)(2,1)S(1)}, bf16[2,2,64,256]{3,2,1,0:T(8,128)(2,1)S(1)}, u32[]{:S(2)}, u32[]{:S(2)}) collective-permute-start(bf16[2,2,64,256]{3,2,1,0:T(8,128)(2,1)S(1)} %collective-permute-done.9.refs_9_), channel_id=1, source_target_pairs={{0,8},{4,12},{8,16},{12,20},{16,24},{20,28},{24,32},{28,36},{32,40... | collective-permute-start | bytes 393224 | tf_op jit(solution)/shard_map/ppermute | solution.py:48
  76.3 9.1 %collective-permute-start.12 = (bf16[2,2,64,256]{3,2,1,0:T(8,128)(2,1)S(1)}, bf16[2,2,64,256]{3,2,1,0:T(8,128)(2,1)S(1)}, u32[]{:S(2)}, u32[]{:S(2)}) collective-permute-start(bf16[2,2,64,256]{3,2,1,0:T(8,128)(2,1)S(1)} %collective-permute-done.10.refs_10_), channel_id=1, source_target_pairs={{0,120},{4,124},{8,0},{12,4},{16,8},{20,12},{24,16},{28,20},{32,24... | collective-permute-start | bytes 393224 | tf_op jit(solution)/shard_map/ppermute | solution.py:52
  85.3 9.4 %collective-permute-start.13 = (bf16[2,2,64,256]{3,2,1,0:T(8,128)(2,1)S(1)}, bf16[2,2,64,256]{3,2,1,0:T(8,128)(2,1)S(1)}, u32[]{:S(2)}, u32[]{:S(2)}) collective-permute-start(bf16[2,2,64,256]{3,2,1,0:T(8,128)(2,1)S(1)} %collective-permute-done.11.refs_11_), channel_id=1, source_target_pairs={{0,8},{4,12},{8,16},{12,20},{16,24},{20,28},{24,32},{28,36},{32,40... | collective-permute-start | bytes 393224 | tf_op jit(solution)/shard_map/ppermute | solution.py:48
  85.3 9.4 %collective-permute-start.14 = (bf16[2,2,64,256]{3,2,1,0:T(8,128)(2,1)S(1)}, bf16[2,2,64,256]{3,2,1,0:T(8,128)(2,1)S(1)}, u32[]{:S(2)}, u32[]{:S(2)}) collective-permute-start(bf16[2,2,64,256]{3,2,1,0:T(8,128)(2,1)S(1)} %collective-permute-done.12.refs_12_), channel_id=1, source_target_pairs={{0,120},{4,124},{8,0},{12,4},{16,8},{20,12},{24,16},{28,20},{32,24... | collective-permute-start | bytes 393224 | tf_op jit(solution)/shard_map/ppermute | solution.py:52
  94.8 9.1 %collective-permute-start.15 = (bf16[2,2,64,256]{3,2,1,0:T(8,128)(2,1)S(1)}, bf16[2,2,64,256]{3,2,1,0:T(8,128)(2,1)S(1)}, u32[]{:S(2)}, u32[]{:S(2)}) collective-permute-start(bf16[2,2,64,256]{3,2,1,0:T(8,128)(2,1)S(1)} %collective-permute-done.13.refs_13_), channel_id=1, source_target_pairs={{0,8},{4,12},{8,16},{12,20},{16,24},{20,28},{24,32},{28,36},{32,40... | collective-permute-start | bytes 393224 | tf_op jit(solution)/shard_map/ppermute | solution.py:48
  104.0 45.7 %copy-start = (bf16[16,2,2,64,256]{4,3,2,1,0:T(8,128)(2,1)}, bf16[16,2,2,64,256]{4,3,2,1,0:T(8,128)(2,1)S(1)}, u32[]{:S(2)}) copy-start(bf16[16,2,2,64,256]{4,3,2,1,0:T(8,128)(2,1)S(1)} %stack.31.refs_0_) | copy-start | bytes 6291460
  104.0 45.7 %collective-permute-start.17 = (bf16[16,2,2,64,256]{4,3,2,1,0:T(8,128)(2,1)S(1)}, bf16[16,2,2,64,256]{4,3,2,1,0:T(8,128)(2,1)}, u32[]{:S(2)}, u32[]{:S(2)}) collective-permute-start(bf16[16,2,2,64,256]{4,3,2,1,0:T(8,128)(2,1)S(1)} %stack.31.refs_0_), channel_id=1, source_target_pairs={{0,128},{128,0},{1,129},{129,1},{2,130},{130,2},{3,131},{131,3},{4... | collective-permute-start | bytes 6291464 | tf_op jit(solution)/shard_map/ppermute | solution.py:319
  115.9 26.9 %copy-start.8 = (bf16[256,2048]{1,0:T(8,128)(2,1)S(1)}, bf16[256,2048]{1,0:T(8,128)(2,1)}, u32[]{:S(2)}) copy-start(bf16[256,2048]{1,0:T(8,128)(2,1)} %param.26) | copy-start | bytes 3145732
  115.9 26.9 %copy-start.9 = (bf16[256,2048]{1,0:T(8,128)(2,1)S(1)}, bf16[256,2048]{1,0:T(8,128)(2,1)}, u32[]{:S(2)}) copy-start(bf16[256,2048]{1,0:T(8,128)(2,1)} %param.25) | copy-start | bytes 3145732
  145.4 4.8 %copy-start.7 = (bf16[2048]{0:T(1024)(128)(2,1)S(1)}, bf16[2048]{0:T(1024)(128)(2,1)}, u32[]{:S(2)}) copy-start(bf16[2048]{0:T(1024)(128)(2,1)} %param.27) | copy-start | bytes 12292
  145.4 19.9 %copy-start.5 = (bf16[64,2048]{1,0:T(8,128)(2,1)S(1)}, bf16[64,2048]{1,0:T(8,128)(2,1)}, u32[]{:S(2)}) copy-start(bf16[64,2048]{1,0:T(8,128)(2,1)} %param.15) | copy-start | bytes 786436
  145.4 19.7 %all-to-all-start = ((bf16[4,64,2048]{2,1,0:T(8,128)(2,1)}), bf16[4,64,2048]{2,1,0:T(8,128)(2,1)S(1)}, u32[]{:S(2)}, u32[]{:S(2)}) async-start(bf16[4,64,2048]{2,1,0:T(8,128)(2,1)} %bitcast.32), calls=%async_computation | async-start | bytes 2097152 | tf_op jit(solution)/shard_map/all_to_all | solution.py:27
  149.7 21.0 %collective-permute-start.16 = (bf16[16,2,2,64,256]{4,3,2,1,0:T(8,128)(2,1)S(1)}, bf16[16,2,2,64,256]{4,3,2,1,0:T(8,128)(2,1)}, u32[]{:S(2)}, u32[]{:S(2)}) collective-permute-start(bf16[16,2,2,64,256]{4,3,2,1,0:T(8,128)(2,1)S(1)} %stack.31.refs_0_), channel_id=1, source_target_pairs={{0,4},{4,0},{8,12},{12,8},{16,20},{20,16},{24,28},{28,24},{32,36},... | collective-permute-start | bytes 6291464 | tf_op jit(solution)/shard_map/ppermute | solution.py:320
  149.7 21.0 %collective-permute-start.18 = (bf16[16,2,2,64,256]{4,3,2,1,0:T(8,128)(2,1)}, bf16[16,2,2,64,256]{4,3,2,1,0:T(8,128)(2,1)}, u32[]{:S(2)}, u32[]{:S(2)}) collective-permute-start(bf16[16,2,2,64,256]{4,3,2,1,0:T(8,128)(2,1)} %collective-permute-done.17.refs_2_), channel_id=1, source_target_pairs={{0,4},{4,0},{8,12},{12,8},{16,20},{20,16},{24,28},{28,24},{32,36},... | collective-permute-start | bytes 6291464 | tf_op jit(solution)/shard_map/ppermute | solution.py:321
  166.8 18.1 %all-to-all-start.1 = ((bf16[4,64,2048]{2,1,0:T(8,128)(2,1)}), bf16[4,64,2048]{2,1,0:T(8,128)(2,1)S(1)}, u32[]{:S(2)}, u32[]{:S(2)}) async-start(bf16[4,64,2048]{2,1,0:T(8,128)(2,1)} %broadcast_in_dim.2), calls=%async_computation.1 | async-start | bytes 2097152 | tf_op jit(solution)/shard_map/all_to_all | solution.py:37
  191.7 1.4 copy-start.1
Sparse Core Ops, SparseCore 0:
  9.2 106.6 all-gather.3
  117.7 72.4 all-gather.5

commit v5 on v4

--- a/solution.py
+++ b/solution.py
@@ -73,7 +73,25 @@
 
 
 def attend_kernel(
-    qn_ref, qw_ref, kv_ref, lam_ref, gain_ref, out_ref, q_s, m_s, acc_s, v_s, *, dn, dw, dv, steps, parts
+    qn_ref,
+    qw_ref,
+    kv_ref,
+    lam_ref,
+    gain_ref,
+    rows_n_ref,
+    rows_w_ref,
+    out_ref,
+    q_s,
+    m_s,
+    acc_s,
+    v_s,
+    att_s,
+    *,
+    dn,
+    dw,
+    dv,
+    steps,
+    parts,
 ):
     step, part = pl.program_id(0), pl.program_id(1)
     rows = qn_ref.shape[0]
@@ -125,10 +143,14 @@
             o = first[:, :dv] / first[:, dv:] - lam_ref[h] * (second[:, :dv] / second[:, dv:])
             square = jnp.mean(o * o, axis=-1, keepdims=True)
             o = o * lax.rsqrt(square + NORM_EPS) * gain_ref[...] * OUT_SCALE
-            out_ref[:, h * dv : (h + 1) * dv] = o.astype(out_ref.dtype)
-
-
-def attention(qn, qw, kv, lam, gain):
+            att_s[:, h * dv : (h + 1) * dv] = o.astype(att_s.dtype)
+        cut = rows_n_ref.shape[0]
+        total = jnp.dot(att_s[:, :cut], rows_n_ref[...], preferred_element_type=jnp.float32)
+        total += jnp.dot(att_s[:, cut:], rows_w_ref[...], preferred_element_type=jnp.float32)
+        out_ref[...] = total.astype(out_ref.dtype)
+
+
+def attention(qn, qw, kv, lam, gain, rows_n, rows_w):
     rows = qn.shape[0]
     keys, width = kv.shape
     dv = gain.shape[1]
@@ -144,14 +166,17 @@
             pl.BlockSpec((block, width), lambda i, j: (i, 0)),
             pl.BlockSpec(memory_space=pltpu.SMEM),
             pl.BlockSpec(gain.shape, lambda i, j: (0, 0)),
-        ],
-        out_specs=pl.BlockSpec((rows, 4 * dv), lambda i, j: (0, 0)),
-        out_shape=jax.ShapeDtypeStruct((rows, 4 * dv), jnp.bfloat16),
+            pl.BlockSpec(rows_n.shape, lambda i, j: (0, 0)),
+            pl.BlockSpec(rows_w.shape, lambda i, j: (0, 0)),
+        ],
+        out_specs=pl.BlockSpec((rows, rows_n.shape[1]), lambda i, j: (0, 0)),
+        out_shape=jax.ShapeDtypeStruct((rows, rows_n.shape[1]), jnp.bfloat16),
         scratch_shapes=[
             pltpu.VMEM((8, rows, 128), jnp.bfloat16),
             pltpu.VMEM((8, rows, 1), jnp.float32),
             pltpu.VMEM((8, rows, 2 * dv), jnp.float32),
             pltpu.VMEM((2, block, 2 * dv), jnp.bfloat16),
+            pltpu.VMEM((rows, 4 * dv), jnp.bfloat16),
         ],
         compiler_params=pltpu.CompilerParams(
             dimension_semantics=("arbitrary", "arbitrary"), vmem_limit_bytes=VMEM_LIMIT
@@ -160,7 +185,7 @@
             flops=16 * rows * keys * 256, bytes_accessed=keys * width * 2, transcendentals=8 * rows * keys
         ),
         name="attend",
-    )(qn, qw, kv, lam, gain)
+    )(qn, qw, kv, lam, gain, rows_n, rows_w)
 
 
 def early_mixer_kernel(chip_ref, x_ref, *refs, places):
@@ -321,16 +346,16 @@
     second = lax.ppermute(swapped, "sp", other_core)
     early_weights = (stack, first, swapped, second)
     kv = after(kv, stack)
-    attended = attention(
+    projected = attention(
         query_narrow.reshape(rows, -1),
         query_wide.reshape(rows, -1),
         kv,
         jnp.concatenate([lambda_narrow, lambda_wide]),
         head_gain.reshape(1, -1),
-    )
-    out_rows = jnp.concatenate([out_narrow, out_wide], axis=0)
-    projected = jnp.dot(attended, out_rows, preferred_element_type=jnp.float32)
-    projected = sent_and_summed(projected.astype(jnp.bfloat16), "tp", 0)
+        out_narrow,
+        out_wide,
+    )
+    projected = sent_and_summed(projected, "tp", 0)
     middle = (resid_in.astype(jnp.float32) + projected).astype(jnp.bfloat16)
     middle_f32 = middle.astype(jnp.float32)
     normed = middle_f32 * lax.rsqrt(

time: 224 us -> 225 us (level)
  matrix products: 2.71 us -> 0 us
    dot_general x1 -> x0, matrix products: 2.71 us -> none  [shards(): projected = jnp.dot(attended, out_rows, preferred_element_type=jnp.float32)]
  transfers between devices with their start and end apart: 23 -> 23, of which waited for: 13 -> 13; matrix products, arithmetic and copies ran while one was open for 4% -> 2% of each run, Pallas kernels for 15% -> 16%
where the time goes in v5:
time: 225 us; the launch traced here: 224 us
  waiting for transfers between devices  89.4 us (40%)
  starting transfers between devices  51.6 us (23%)
  Pallas kernels  41.2 us (18%)
  blocking collectives  18 us (8%)
  between operations  13.7 us (6%)
  other arithmetic  5.5 us (2%)
  local copies, waits for them, and re-layouts  4.16 us (2%)
    ppermute x8, waiting for transfers between devices, ring(): ahead = lax.ppermute(ahead, 'sp', onward)  49.3 us
    ppermute x7, starting transfers between devices, ring(): behind = lax.ppermute(behind, 'sp', backward)  39.8 us
    pallas_call x1, Pallas kernels, attention(): pl.pallas_call(functools.partial(attend_kernel, dn=dn, dw=dw, dv=dv, step...  28.2 us
    all_to_all x1, blocking collectives, sent_and_summed(): parts = lax.all_to_all(split_up(array, dim, peers), axis, 0, 0, tiled=True)  18 us
    all_to_all x1, waiting for transfers between devices, sent_and_summed(): parts = lax.all_to_all(split_up(array, dim, peers), axis, 0, 0, tiled=True)  15 us
    all_to_all x1, waiting for transfers between devices, copy_for_each(): return lax.all_to_all(copies, axis, split_axis=0, concat_axis=0, tiled=True)  14.3 us
    all_gather x1, waiting for transfers between devices, shards(): kv = lax.all_gather(own, 'sp', axis=0, tiled=True)  9.47 us
    pallas_call x1, Pallas kernels, early_mixer(): pl.pallas_call(functools.partial(early_mixer_kernel, places=places), in_s...  6.75 us
  transfers between devices with their start and end apart: 23, of which 13 were waited for; matrix products, arithmetic and copies ran while one was open for 2% of the time, Pallas kernels for 16%

profile of v5, /device:TPU:40, one launch (start us, length us, event | category | flops | bytes accessed | tf_op | source)
XLA Modules:
  0.0 223.6 jit_solution(5673191694358948700)
XLA Ops:
  6.6 1.8 pad_maximum_fusion
  8.3 0.1 all-gather.4.cloned.1.call-update
  8.4 0.1 all-gather.6.cloned.1.call-start
  8.5 1.7 pad_maximum_fusion.1
  10.2 0.1 all-gather.6.cloned.1.call-update
  10.3 0.1 collective-permute-start
  10.5 1.2 collective-permute-done
  11.7 0.0 copy-start.4
  11.7 0.0 copy-start.6
  11.7 0.0 copy-start.8
  11.8 0.0 copy-start.9
  11.8 2.9 %collective-permute-start.1 = (bf16[2,2,64,256]{3,2,1,0:T(8,128)(2,1)S(1)}, bf16[2,2,64,256]{3,2,1,0:T(8,128)(2,1)S(1)}, u32[]{:S(2)}, u32[]{:S(2)}) collective-permute-start(bf16[2,2,64,256]{3,2,1,0:T(8,128)(2,1)S(1)} %maximum_select_fusion.refs_0_), channel_id=1, source_target_pairs={{0,8},{4,12},{8,16},{12,20},{16,24},{20,28},{24,32},{28,36},{32,40... | collective-permute-start | bytes 393224 | tf_op jit(solution)/shard_map/ppermute | solution.py:48
  14.7 19.7 %collective-permute-start.2 = (bf16[2,2,64,256]{3,2,1,0:T(8,128)(2,1)S(1)}, bf16[2,2,64,256]{3,2,1,0:T(8,128)(2,1)S(1)}, u32[]{:S(2)}, u32[]{:S(2)}) collective-permute-start(bf16[2,2,64,256]{3,2,1,0:T(8,128)(2,1)S(1)} %maximum_select_fusion.refs_0_), channel_id=1, source_target_pairs={{0,120},{4,124},{8,0},{12,4},{16,8},{20,12},{24,16},{28,20},{32,24... | collective-permute-start | bytes 393224 | tf_op jit(solution)/shard_map/ppermute | solution.py:52
  34.4 3.7 %collective-permute-done.1.refs_1_ = bf16[2,2,64,256]{3,2,1,0:T(8,128)(2,1)S(1)} collective-permute-done((bf16[2,2,64,256]{3,2,1,0:T(8,128)(2,1)S(1)}, bf16[2,2,64,256]{3,2,1,0:T(8,128)(2,1)S(1)}, u32[]{:S(2)}, u32[]{:S(2)}) %collective-permute-start.1) | collective-permute-done | bytes 131104 | tf_op jit(solution)/shard_map/ppermute | solution.py:48
  38.1 0.0 collective-permute-start.3
  38.1 0.1 collective-permute-done.2.refs_2_
  38.2 3.7 %collective-permute-start.4 = (bf16[2,2,64,256]{3,2,1,0:T(8,128)(2,1)S(1)}, bf16[2,2,64,256]{3,2,1,0:T(8,128)(2,1)S(1)}, u32[]{:S(2)}, u32[]{:S(2)}) collective-permute-start(bf16[2,2,64,256]{3,2,1,0:T(8,128)(2,1)S(1)} %collective-permute-done.2.refs_2_), channel_id=1, source_target_pairs={{0,120},{4,124},{8,0},{12,4},{16,8},{20,12},{24,16},{28,20},{32,24... | collective-permute-start | bytes 393224 | tf_op jit(solution)/shard_map/ppermute | solution.py:52
  41.8 6.1 %collective-permute-done.3.refs_3_ = bf16[2,2,64,256]{3,2,1,0:T(8,128)(2,1)S(1)} collective-permute-done((bf16[2,2,64,256]{3,2,1,0:T(8,128)(2,1)S(1)}, bf16[2,2,64,256]{3,2,1,0:T(8,128)(2,1)S(1)}, u32[]{:S(2)}, u32[]{:S(2)}) %collective-permute-start.3) | collective-permute-done | bytes 131104 | tf_op jit(solution)/shard_map/ppermute | solution.py:48
  47.9 0.0 collective-permute-start.5
  47.9 0.0 collective-permute-done.4.refs_4_
  47.9 3.2 %collective-permute-start.6 = (bf16[2,2,64,256]{3,2,1,0:T(8,128)(2,1)S(1)}, bf16[2,2,64,256]{3,2,1,0:T(8,128)(2,1)S(1)}, u32[]{:S(2)}, u32[]{:S(2)}) collective-permute-start(bf16[2,2,64,256]{3,2,1,0:T(8,128)(2,1)S(1)} %collective-permute-done.4.refs_4_), channel_id=1, source_target_pairs={{0,120},{4,124},{8,0},{12,4},{16,8},{20,12},{24,16},{28,20},{32,24... | collective-permute-start | bytes 393224 | tf_op jit(solution)/shard_map/ppermute | solution.py:52
  51.2 6.4 %collective-permute-done.5.refs_5_ = bf16[2,2,64,256]{3,2,1,0:T(8,128)(2,1)S(1)} collective-permute-done((bf16[2,2,64,256]{3,2,1,0:T(8,128)(2,1)S(1)}, bf16[2,2,64,256]{3,2,1,0:T(8,128)(2,1)S(1)}, u32[]{:S(2)}, u32[]{:S(2)}) %collective-permute-start.5) | collective-permute-done | bytes 131104 | tf_op jit(solution)/shard_map/ppermute | solution.py:48
  57.6 0.0 collective-permute-start.7
  57.6 0.0 collective-permute-done.6.refs_6_
  57.6 3.2 %collective-permute-start.8 = (bf16[2,2,64,256]{3,2,1,0:T(8,128)(2,1)S(1)}, bf16[2,2,64,256]{3,2,1,0:T(8,128)(2,1)S(1)}, u32[]{:S(2)}, u32[]{:S(2)}) collective-permute-start(bf16[2,2,64,256]{3,2,1,0:T(8,128)(2,1)S(1)} %collective-permute-done.6.refs_6_), channel_id=1, source_target_pairs={{0,120},{4,124},{8,0},{12,4},{16,8},{20,12},{24,16},{28,20},{32,24... | collective-permute-start | bytes 393224 | tf_op jit(solution)/shard_map/ppermute | solution.py:52
  60.8 6.2 %collective-permute-done.7.refs_7_ = bf16[2,2,64,256]{3,2,1,0:T(8,128)(2,1)S(1)} collective-permute-done((bf16[2,2,64,256]{3,2,1,0:T(8,128)(2,1)S(1)}, bf16[2,2,64,256]{3,2,1,0:T(8,128)(2,1)S(1)}, u32[]{:S(2)}, u32[]{:S(2)}) %collective-permute-start.7) | collective-permute-done | bytes 131104 | tf_op jit(solution)/shard_map/ppermute | solution.py:48
  67.0 0.0 collective-permute-start.9
  67.0 0.0 collective-permute-done.8.refs_8_
  67.0 3.2 %collective-permute-start.10 = (bf16[2,2,64,256]{3,2,1,0:T(8,128)(2,1)S(1)}, bf16[2,2,64,256]{3,2,1,0:T(8,128)(2,1)S(1)}, u32[]{:S(2)}, u32[]{:S(2)}) collective-permute-start(bf16[2,2,64,256]{3,2,1,0:T(8,128)(2,1)S(1)} %collective-permute-done.8.refs_8_), channel_id=1, source_target_pairs={{0,120},{4,124},{8,0},{12,4},{16,8},{20,12},{24,16},{28,20},{32,24... | collective-permute-start | bytes 393224 | tf_op jit(solution)/shard_map/ppermute | solution.py:52
  70.3 6.0 %collective-permute-done.9.refs_9_ = bf16[2,2,64,256]{3,2,1,0:T(8,128)(2,1)S(1)} collective-permute-done((bf16[2,2,64,256]{3,2,1,0:T(8,128)(2,1)S(1)}, bf16[2,2,64,256]{3,2,1,0:T(8,128)(2,1)S(1)}, u32[]{:S(2)}, u32[]{:S(2)}) %collective-permute-start.9) | collective-permute-done | bytes 131104 | tf_op jit(solution)/shard_map/ppermute | solution.py:48
  76.3 0.0 collective-permute-start.11
  76.3 0.0 collective-permute-done.10.refs_10_
  76.3 3.2 %collective-permute-start.12 = (bf16[2,2,64,256]{3,2,1,0:T(8,128)(2,1)S(1)}, bf16[2,2,64,256]{3,2,1,0:T(8,128)(2,1)S(1)}, u32[]{:S(2)}, u32[]{:S(2)}) collective-permute-start(bf16[2,2,64,256]{3,2,1,0:T(8,128)(2,1)S(1)} %collective-permute-done.10.refs_10_), channel_id=1, source_target_pairs={{0,120},{4,124},{8,0},{12,4},{16,8},{20,12},{24,16},{28,20},{32,24... | collective-permute-start | bytes 393224 | tf_op jit(solution)/shard_map/ppermute | solution.py:52
  79.5 5.8 %collective-permute-done.11.refs_11_ = bf16[2,2,64,256]{3,2,1,0:T(8,128)(2,1)S(1)} collective-permute-done((bf16[2,2,64,256]{3,2,1,0:T(8,128)(2,1)S(1)}, bf16[2,2,64,256]{3,2,1,0:T(8,128)(2,1)S(1)}, u32[]{:S(2)}, u32[]{:S(2)}) %collective-permute-start.11) | collective-permute-done | bytes 131104 | tf_op jit(solution)/shard_map/ppermute | solution.py:48
  85.3 0.0 collective-permute-start.13
  85.3 0.0 collective-permute-done.12.refs_12_
  85.3 3.4 %collective-permute-start.14 = (bf16[2,2,64,256]{3,2,1,0:T(8,128)(2,1)S(1)}, bf16[2,2,64,256]{3,2,1,0:T(8,128)(2,1)S(1)}, u32[]{:S(2)}, u32[]{:S(2)}) collective-permute-start(bf16[2,2,64,256]{3,2,1,0:T(8,128)(2,1)S(1)} %collective-permute-done.12.refs_12_), channel_id=1, source_target_pairs={{0,120},{4,124},{8,0},{12,4},{16,8},{20,12},{24,16},{28,20},{32,24... | collective-permute-start | bytes 393224 | tf_op jit(solution)/shard_map/ppermute | solution.py:52
  88.8 6.0 %collective-permute-done.13.refs_13_ = bf16[2,2,64,256]{3,2,1,0:T(8,128)(2,1)S(1)} collective-permute-done((bf16[2,2,64,256]{3,2,1,0:T(8,128)(2,1)S(1)}, bf16[2,2,64,256]{3,2,1,0:T(8,128)(2,1)S(1)}, u32[]{:S(2)}, u32[]{:S(2)}) %collective-permute-start.13) | collective-permute-done | bytes 131104 | tf_op jit(solution)/shard_map/ppermute | solution.py:48
  94.7 0.0 collective-permute-start.15
  94.7 9.1 %collective-permute-done.15.refs_15_ = bf16[2,2,64,256]{3,2,1,0:T(8,128)(2,1)S(1)} collective-permute-done((bf16[2,2,64,256]{3,2,1,0:T(8,128)(2,1)S(1)}, bf16[2,2,64,256]{3,2,1,0:T(8,128)(2,1)S(1)}, u32[]{:S(2)}, u32[]{:S(2)}) %collective-permute-start.15) | collective-permute-done | bytes 131104 | tf_op jit(solution)/shard_map/ppermute | solution.py:48
  103.9 0.1 stack.31.refs_0_
  104.0 0.1 collective-permute-start.17
  104.2 0.9 copy.17
  105.1 0.7 copy.19
  105.8 0.6 pad_maximum_fusion.2.lam_ref
  106.4 9.5 %all-gather.4.cloned.1.call-done.kv_ref = bf16[8192,640]{1,0:T(8,128)(2,1)} async-done(((bf16[256,640]{1,0:T(8,128)(2,1)}), bf16[8192,640]{1,0:T(8,128)(2,1)}) %all-gather.4.cloned.1.call-update) | async-done | bytes 10485776 | tf_op jit(solution)/shard_map/all_gather | solution.py:333
  115.9 28.2 %attend.1 = bf16[256,2048]{1,0:T(8,128)(2,1)} custom-call(bf16[256,256]{1,0:T(8,128)(2,1)} %bitcast.36, bf16[256,512]{1,0:T(8,128)(2,1)} %bitcast.33, bf16[8192,640]{1,0:T(8,128)(2,1)} %all-gather.4.cloned.1.call-done.kv_ref, f32[4]{0:T(128)} %pad_maximum_fusion.2.lam_ref, f32[1,128]{1,0:T(1,128)} %bitcast.41, bf16[256,2048]{1,0:T(8,128)(2,1)} %rows_n_ref.1, ...), custom_call_target="tpu_custom_call" | custom-call | flops 8589934592 | bytes 10485760 | tf_op jit(solution)/shard_map/attend/pallas_call | solution.py:160
  144.1 4.2 %all-to-all-start = ((bf16[4,64,2048]{2,1,0:T(8,128)(2,1)}), bf16[4,64,2048]{2,1,0:T(8,128)(2,1)S(1)}, u32[]{:S(2)}, u32[]{:S(2)}) async-start(bf16[4,64,2048]{2,1,0:T(8,128)(2,1)} %bitcast.31), calls=%async_computation | async-start | bytes 2097152 | tf_op jit(solution)/shard_map/all_to_all | solution.py:27
  148.3 0.0 collective-permute-start.16
  148.3 0.5 collective-permute-start.18
  148.8 15.0 %all-to-all-done = bf16[4,64,2048]{2,1,0:T(8,128)(2,1)S(1)} async-done(((bf16[4,64,2048]{2,1,0:T(8,128)(2,1)}), bf16[4,64,2048]{2,1,0:T(8,128)(2,1)S(1)}, u32[]{:S(2)}, u32[]{:S(2)}) %all-to-all-start) | async-done | bytes 1048608 | tf_op jit(solution)/shard_map/all_to_all | solution.py:27
  163.8 0.2 convert_reduce_fusion.1
  163.9 0.2 fusion
  164.1 0.1 fusion.2
  164.3 1.1 broadcast_in_dim.2
  165.4 3.8 %all-to-all-start.1 = ((bf16[4,64,2048]{2,1,0:T(8,128)(2,1)}), bf16[4,64,2048]{2,1,0:T(8,128)(2,1)S(1)}, u32[]{:S(2)}, u32[]{:S(2)}) async-start(bf16[4,64,2048]{2,1,0:T(8,128)(2,1)} %broadcast_in_dim.2), calls=%async_computation.1 | async-start | bytes 2097152 | tf_op jit(solution)/shard_map/all_to_all | solution.py:37
  169.3 0.0 collective-permute-done.16.refs_1_
  169.3 14.3 %all-to-all-done.1 = bf16[4,64,2048]{2,1,0:T(8,128)(2,1)S(1)} async-done(((bf16[4,64,2048]{2,1,0:T(8,128)(2,1)}), bf16[4,64,2048]{2,1,0:T(8,128)(2,1)S(1)}, u32[]{:S(2)}, u32[]{:S(2)}) %all-to-all-start.1) | async-done | bytes 1048608 | tf_op jit(solution)/shard_map/all_to_all | solution.py:37
  183.6 6.8 %early_mixer.1.early_ref = f32[256,2048]{1,0:T(8,128)S(1)} custom-call(s32[1]{0:T(128)} %bitcast.13.chip_ref, bf16[256,2048]{1,0:T(8,128)(2,1)S(1)} %bitcast.23, bf16[16,2,2,64,256]{4,3,2,1,0:T(8,128)(2,1)} %copy-done, bf16[16,2,2,64,256]{4,3,2,1,0:T(8,128)(2,1)} %collective-permute-done.16.refs_1_, ...), custom_call_target="tpu_custom_call" | custom-call | flops 2147483648 | bytes 8388608 | tf_op jit(solution)/shard_map/early_mixer/pallas_call | solution.py:226
  190.3 1.4 copy-done.1
  191.7 6.1 %mixer.1 = bf16[256,2048]{1,0:T(8,128)(2,1)S(1)} custom-call(bf16[256,2048]{1,0:T(8,128)(2,1)S(1)} %bitcast.24, bf16[32,2,64,1024]{3,2,1,0:T(8,128)(2,1)} %bitcast.26, f32[256,2048]{1,0:T(8,128)} %copy-done.1), custom_call_target="tpu_custom_call" | custom-call | flops 2147483648 | bytes 8388608 | tf_op jit(solution)/shard_map/mixer/pallas_call | solution.py:284
  197.8 18.0 %all_to_all.15 = bf16[4,64,2048]{2,1,0:T(8,128)(2,1)S(1)} all-to-all(bf16[4,64,2048]{2,1,0:T(8,128)(2,1)S(1)} %bitcast.25), channel_id=1, replica_groups=mesh['grp'=2,'sp'=32,'tp'=4] {'tp'}, dimensions={0} | all-to-all | bytes 2097152 | tf_op jit(solution)/shard_map/all_to_all | solution.py:27
  215.8 0.2 convert_reduce_fusion
  216.0 0.8 fusion.3
  (24 shorter events, 0.1 us)
Async XLA Ops:
  6.5 3.7 %copy-start.3 = (bf16[64,2048]{1,0:T(8,128)(2,1)S(1)}, bf16[64,2048]{1,0:T(8,128)(2,1)}, u32[]{:S(2)}) copy-start(bf16[64,2048]{1,0:T(8,128)(2,1)} %param.28) | copy-start | bytes 786436
  6.5 3.7 %copy-start.2 = (bf16[2048,64]{0,1:T(8,128)(2,1)S(1)}, bf16[2048,64]{0,1:T(8,128)(2,1)}, u32[]{:S(2)}) copy-start(bf16[2048,64]{0,1:T(8,128)(2,1)} %param.29) | copy-start | bytes 786436
  6.6 109.3 %all-gather.4.cloned.1.call-start = ((), (), s32[]{:S(2)}) async-start(), calls=%async_computation.3 | async-start | bytes 10813440 | tf_op jit(solution)/shard_map/all_gather | solution.py:333
  8.4 183.3 %all-gather.6.cloned.1.call-start = ((), (), s32[]{:S(2)}) async-start(), calls=%async_computation.4 | async-start | bytes 8650752 | tf_op jit(solution)/shard_map/all_gather | solution.py:338
  10.3 1.4 collective-permute-start
  11.7 92.4 %copy-start.4 = (bf16[256,2,256]{2,1,0:T(2,128)(2,1)S(1)}, bf16[256,2,256]{2,1,0:T(2,128)(2,1)}, u32[]{:S(2)}) copy-start(bf16[256,2,256]{2,1,0:T(2,128)(2,1)} %param.19) | copy-start | bytes 786436
  11.7 93.4 %copy-start.6 = (bf16[256,2,128]{2,1,0:T(2,128)(2,1)S(1)}, bf16[256,2,128]{2,1,0:T(2,128)(2,1)}, u32[]{:S(2)}) copy-start(bf16[256,2,128]{2,1,0:T(2,128)(2,1)} %param.16) | copy-start | bytes 393220
  11.7 94.1 %copy-start.8 = (f32[2]{0:T(128)S(1)}, f32[2]{0:T(128)}, u32[]{:S(2)}) copy-start(f32[2]{0:T(128)} %param.23) | copy-start | bytes 28
  11.8 94.0 %copy-start.9 = (f32[2]{0:T(128)S(1)}, f32[2]{0:T(128)}, u32[]{:S(2)}) copy-start(f32[2]{0:T(128)} %param.22) | copy-start | bytes 28
  11.8 26.3 %collective-permute-start.1 = (bf16[2,2,64,256]{3,2,1,0:T(8,128)(2,1)S(1)}, bf16[2,2,64,256]{3,2,1,0:T(8,128)(2,1)S(1)}, u32[]{:S(2)}, u32[]{:S(2)}) collective-permute-start(bf16[2,2,64,256]{3,2,1,0:T(8,128)(2,1)S(1)} %maximum_select_fusion.refs_0_), channel_id=1, source_target_pairs={{0,8},{4,12},{8,16},{12,20},{16,24},{20,28},{24,32},{28,36},{32,40... | collective-permute-start | bytes 393224 | tf_op jit(solution)/shard_map/ppermute | solution.py:48
  14.7 23.5 %collective-permute-start.2 = (bf16[2,2,64,256]{3,2,1,0:T(8,128)(2,1)S(1)}, bf16[2,2,64,256]{3,2,1,0:T(8,128)(2,1)S(1)}, u32[]{:S(2)}, u32[]{:S(2)}) collective-permute-start(bf16[2,2,64,256]{3,2,1,0:T(8,128)(2,1)S(1)} %maximum_select_fusion.refs_0_), channel_id=1, source_target_pairs={{0,120},{4,124},{8,0},{12,4},{16,8},{20,12},{24,16},{28,20},{32,24... | collective-permute-start | bytes 393224 | tf_op jit(solution)/shard_map/ppermute | solution.py:52
  38.1 9.8 %collective-permute-start.3 = (bf16[2,2,64,256]{3,2,1,0:T(8,128)(2,1)S(1)}, bf16[2,2,64,256]{3,2,1,0:T(8,128)(2,1)S(1)}, u32[]{:S(2)}, u32[]{:S(2)}) collective-permute-start(bf16[2,2,64,256]{3,2,1,0:T(8,128)(2,1)S(1)} %collective-permute-done.1.refs_1_), channel_id=1, source_target_pairs={{0,8},{4,12},{8,16},{12,20},{16,24},{20,28},{24,32},{28,36},{32,40... | collective-permute-start | bytes 393224 | tf_op jit(solution)/shard_map/ppermute | solution.py:48
  38.2 9.8 %collective-permute-start.4 = (bf16[2,2,64,256]{3,2,1,0:T(8,128)(2,1)S(1)}, bf16[2,2,64,256]{3,2,1,0:T(8,128)(2,1)S(1)}, u32[]{:S(2)}, u32[]{:S(2)}) collective-permute-start(bf16[2,2,64,256]{3,2,1,0:T(8,128)(2,1)S(1)} %collective-permute-done.2.refs_2_), channel_id=1, source_target_pairs={{0,120},{4,124},{8,0},{12,4},{16,8},{20,12},{24,16},{28,20},{32,24... | collective-permute-start | bytes 393224 | tf_op jit(solution)/shard_map/ppermute | solution.py:52
  47.9 9.6 %collective-permute-start.5 = (bf16[2,2,64,256]{3,2,1,0:T(8,128)(2,1)S(1)}, bf16[2,2,64,256]{3,2,1,0:T(8,128)(2,1)S(1)}, u32[]{:S(2)}, u32[]{:S(2)}) collective-permute-start(bf16[2,2,64,256]{3,2,1,0:T(8,128)(2,1)S(1)} %collective-permute-done.3.refs_3_), channel_id=1, source_target_pairs={{0,8},{4,12},{8,16},{12,20},{16,24},{20,28},{24,32},{28,36},{32,40... | collective-permute-start | bytes 393224 | tf_op jit(solution)/shard_map/ppermute | solution.py:48
  47.9 9.6 %collective-permute-start.6 = (bf16[2,2,64,256]{3,2,1,0:T(8,128)(2,1)S(1)}, bf16[2,2,64,256]{3,2,1,0:T(8,128)(2,1)S(1)}, u32[]{:S(2)}, u32[]{:S(2)}) collective-permute-start(bf16[2,2,64,256]{3,2,1,0:T(8,128)(2,1)S(1)} %collective-permute-done.4.refs_4_), channel_id=1, source_target_pairs={{0,120},{4,124},{8,0},{12,4},{16,8},{20,12},{24,16},{28,20},{32,24... | collective-permute-start | bytes 393224 | tf_op jit(solution)/shard_map/ppermute | solution.py:52
  57.6 9.4 %collective-permute-start.7 = (bf16[2,2,64,256]{3,2,1,0:T(8,128)(2,1)S(1)}, bf16[2,2,64,256]{3,2,1,0:T(8,128)(2,1)S(1)}, u32[]{:S(2)}, u32[]{:S(2)}) collective-permute-start(bf16[2,2,64,256]{3,2,1,0:T(8,128)(2,1)S(1)} %collective-permute-done.5.refs_5_), channel_id=1, source_target_pairs={{0,8},{4,12},{8,16},{12,20},{16,24},{20,28},{24,32},{28,36},{32,40... | collective-permute-start | bytes 393224 | tf_op jit(solution)/shard_map/ppermute | solution.py:48
  57.6 9.4 %collective-permute-start.8 = (bf16[2,2,64,256]{3,2,1,0:T(8,128)(2,1)S(1)}, bf16[2,2,64,256]{3,2,1,0:T(8,128)(2,1)S(1)}, u32[]{:S(2)}, u32[]{:S(2)}) collective-permute-start(bf16[2,2,64,256]{3,2,1,0:T(8,128)(2,1)S(1)} %collective-permute-done.6.refs_6_), channel_id=1, source_target_pairs={{0,120},{4,124},{8,0},{12,4},{16,8},{20,12},{24,16},{28,20},{32,24... | collective-permute-start | bytes 393224 | tf_op jit(solution)/shard_map/ppermute | solution.py:52
  67.0 9.2 %collective-permute-start.9 = (bf16[2,2,64,256]{3,2,1,0:T(8,128)(2,1)S(1)}, bf16[2,2,64,256]{3,2,1,0:T(8,128)(2,1)S(1)}, u32[]{:S(2)}, u32[]{:S(2)}) collective-permute-start(bf16[2,2,64,256]{3,2,1,0:T(8,128)(2,1)S(1)} %collective-permute-done.7.refs_7_), channel_id=1, source_target_pairs={{0,8},{4,12},{8,16},{12,20},{16,24},{20,28},{24,32},{28,36},{32,40... | collective-permute-start | bytes 393224 | tf_op jit(solution)/shard_map/ppermute | solution.py:48
  67.0 9.2 %collective-permute-start.10 = (bf16[2,2,64,256]{3,2,1,0:T(8,128)(2,1)S(1)}, bf16[2,2,64,256]{3,2,1,0:T(8,128)(2,1)S(1)}, u32[]{:S(2)}, u32[]{:S(2)}) collective-permute-start(bf16[2,2,64,256]{3,2,1,0:T(8,128)(2,1)S(1)} %collective-permute-done.8.refs_8_), channel_id=1, source_target_pairs={{0,120},{4,124},{8,0},{12,4},{16,8},{20,12},{24,16},{28,20},{32,24... | collective-permute-start | bytes 393224 | tf_op jit(solution)/shard_map/ppermute | solution.py:52
  76.3 9.1 %collective-permute-start.11 = (bf16[2,2,64,256]{3,2,1,0:T(8,128)(2,1)S(1)}, bf16[2,2,64,256]{3,2,1,0:T(8,128)(2,1)S(1)}, u32[]{:S(2)}, u32[]{:S(2)}) collective-permute-start(bf16[2,2,64,256]{3,2,1,0:T(8,128)(2,1)S(1)} %collective-permute-done.9.refs_9_), channel_id=1, source_target_pairs={{0,8},{4,12},{8,16},{12,20},{16,24},{20,28},{24,32},{28,36},{32,40... | collective-permute-start | bytes 393224 | tf_op jit(solution)/shard_map/ppermute | solution.py:48
  76.3 9.1 %collective-permute-start.12 = (bf16[2,2,64,256]{3,2,1,0:T(8,128)(2,1)S(1)}, bf16[2,2,64,256]{3,2,1,0:T(8,128)(2,1)S(1)}, u32[]{:S(2)}, u32[]{:S(2)}) collective-permute-start(bf16[2,2,64,256]{3,2,1,0:T(8,128)(2,1)S(1)} %collective-permute-done.10.refs_10_), channel_id=1, source_target_pairs={{0,120},{4,124},{8,0},{12,4},{16,8},{20,12},{24,16},{28,20},{32,24... | collective-permute-start | bytes 393224 | tf_op jit(solution)/shard_map/ppermute | solution.py:52
  85.3 9.4 %collective-permute-start.13 = (bf16[2,2,64,256]{3,2,1,0:T(8,128)(2,1)S(1)}, bf16[2,2,64,256]{3,2,1,0:T(8,128)(2,1)S(1)}, u32[]{:S(2)}, u32[]{:S(2)}) collective-permute-start(bf16[2,2,64,256]{3,2,1,0:T(8,128)(2,1)S(1)} %collective-permute-done.11.refs_11_), channel_id=1, source_target_pairs={{0,8},{4,12},{8,16},{12,20},{16,24},{20,28},{24,32},{28,36},{32,40... | collective-permute-start | bytes 393224 | tf_op jit(solution)/shard_map/ppermute | solution.py:48
  85.3 9.4 %collective-permute-start.14 = (bf16[2,2,64,256]{3,2,1,0:T(8,128)(2,1)S(1)}, bf16[2,2,64,256]{3,2,1,0:T(8,128)(2,1)S(1)}, u32[]{:S(2)}, u32[]{:S(2)}) collective-permute-start(bf16[2,2,64,256]{3,2,1,0:T(8,128)(2,1)S(1)} %collective-permute-done.12.refs_12_), channel_id=1, source_target_pairs={{0,120},{4,124},{8,0},{12,4},{16,8},{20,12},{24,16},{28,20},{32,24... | collective-permute-start | bytes 393224 | tf_op jit(solution)/shard_map/ppermute | solution.py:52
  94.7 9.1 %collective-permute-start.15 = (bf16[2,2,64,256]{3,2,1,0:T(8,128)(2,1)S(1)}, bf16[2,2,64,256]{3,2,1,0:T(8,128)(2,1)S(1)}, u32[]{:S(2)}, u32[]{:S(2)}) collective-permute-start(bf16[2,2,64,256]{3,2,1,0:T(8,128)(2,1)S(1)} %collective-permute-done.13.refs_13_), channel_id=1, source_target_pairs={{0,8},{4,12},{8,16},{12,20},{16,24},{20,28},{24,32},{28,36},{32,40... | collective-permute-start | bytes 393224 | tf_op jit(solution)/shard_map/ppermute | solution.py:48
  104.0 44.3 %copy-start = (bf16[16,2,2,64,256]{4,3,2,1,0:T(8,128)(2,1)}, bf16[16,2,2,64,256]{4,3,2,1,0:T(8,128)(2,1)S(1)}, u32[]{:S(2)}) copy-start(bf16[16,2,2,64,256]{4,3,2,1,0:T(8,128)(2,1)S(1)} %stack.31.refs_0_) | copy-start | bytes 6291460
  104.0 44.3 %collective-permute-start.17 = (bf16[16,2,2,64,256]{4,3,2,1,0:T(8,128)(2,1)S(1)}, bf16[16,2,2,64,256]{4,3,2,1,0:T(8,128)(2,1)}, u32[]{:S(2)}, u32[]{:S(2)}) collective-permute-start(bf16[16,2,2,64,256]{4,3,2,1,0:T(8,128)(2,1)S(1)} %stack.31.refs_0_), channel_id=1, source_target_pairs={{0,128},{128,0},{1,129},{129,1},{2,130},{130,2},{3,131},{131,3},{4... | collective-permute-start | bytes 6291464 | tf_op jit(solution)/shard_map/ppermute | solution.py:344
  144.1 4.7 %copy-start.7 = (bf16[2048]{0:T(1024)(128)(2,1)S(1)}, bf16[2048]{0:T(1024)(128)(2,1)}, u32[]{:S(2)}) copy-start(bf16[2048]{0:T(1024)(128)(2,1)} %param.27) | copy-start | bytes 12292
  144.1 19.9 %copy-start.5 = (bf16[64,2048]{1,0:T(8,128)(2,1)S(1)}, bf16[64,2048]{1,0:T(8,128)(2,1)}, u32[]{:S(2)}) copy-start(bf16[64,2048]{1,0:T(8,128)(2,1)} %param.15) | copy-start | bytes 786436
  144.1 19.7 %all-to-all-start = ((bf16[4,64,2048]{2,1,0:T(8,128)(2,1)}), bf16[4,64,2048]{2,1,0:T(8,128)(2,1)S(1)}, u32[]{:S(2)}, u32[]{:S(2)}) async-start(bf16[4,64,2048]{2,1,0:T(8,128)(2,1)} %bitcast.31), calls=%async_computation | async-start | bytes 2097152 | tf_op jit(solution)/shard_map/all_to_all | solution.py:27
  148.3 21.0 %collective-permute-start.16 = (bf16[16,2,2,64,256]{4,3,2,1,0:T(8,128)(2,1)S(1)}, bf16[16,2,2,64,256]{4,3,2,1,0:T(8,128)(2,1)}, u32[]{:S(2)}, u32[]{:S(2)}) collective-permute-start(bf16[16,2,2,64,256]{4,3,2,1,0:T(8,128)(2,1)S(1)} %stack.31.refs_0_), channel_id=1, source_target_pairs={{0,4},{4,0},{8,12},{12,8},{16,20},{20,16},{24,28},{28,24},{32,36},... | collective-permute-start | bytes 6291464 | tf_op jit(solution)/shard_map/ppermute | solution.py:345
  148.3 21.0 %collective-permute-start.18 = (bf16[16,2,2,64,256]{4,3,2,1,0:T(8,128)(2,1)}, bf16[16,2,2,64,256]{4,3,2,1,0:T(8,128)(2,1)}, u32[]{:S(2)}, u32[]{:S(2)}) collective-permute-start(bf16[16,2,2,64,256]{4,3,2,1,0:T(8,128)(2,1)} %collective-permute-done.17.refs_2_), channel_id=1, source_target_pairs={{0,4},{4,0},{8,12},{12,8},{16,20},{20,16},{24,28},{28,24},{32,36},... | collective-permute-start | bytes 6291464 | tf_op jit(solution)/shard_map/ppermute | solution.py:346
  165.4 18.2 %all-to-all-start.1 = ((bf16[4,64,2048]{2,1,0:T(8,128)(2,1)}), bf16[4,64,2048]{2,1,0:T(8,128)(2,1)S(1)}, u32[]{:S(2)}, u32[]{:S(2)}) async-start(bf16[4,64,2048]{2,1,0:T(8,128)(2,1)} %broadcast_in_dim.2), calls=%async_computation.1 | async-start | bytes 2097152 | tf_op jit(solution)/shard_map/all_to_all | solution.py:37
  190.3 1.4 copy-start.1
Sparse Core Ops, SparseCore 0:
  9.2 106.6 all-gather.3
  117.7 72.4 all-gather.5
